TPU v7x, 256 devices: a whole 4x4x8 slice. The times are simulated.
256 devices in a mesh: fs: 32 (over z, x), tp: 8 (over y, core).
Axes of the slice: x: 4, y: 4, z: 8, core: 2. Of those that a mesh axis runs over, the one named last changes fastest.
Arguments:
- tokens: bfloat16 [32768, 2048], P(('fs', 'tp')), may hold values from -6 to 6
- gate_pre: bfloat16 [32768, 5632], P('fs', 'tp'), may hold values from -6 to 6
- value_pre: bfloat16 [32768, 5632], P('fs', 'tp'), may hold values from -6 to 6
- up_gate_w: bfloat16 [2048, 5632], P('fs', 'tp'), may hold values from -0.078125 to 0.078125
- up_value_w: bfloat16 [2048, 5632], P('fs', 'tp'), may hold values from -0.078125 to 0.078125
- conv_weight: float32 [3, 5632], P(None, 'tp'), may hold values from -3 to 3
- conv_bias: float32 [5632], P('tp'), may hold values from -3 to 3
- hidden_grad: bfloat16 [32768, 5632], P('fs', 'tp'), may hold values from -6 to 6
Outputs:
- input_grad: bfloat16 [32768, 2048], P(('fs', 'tp'))
- up_gate_grad: float32 [2048, 5632], P('fs', 'tp')
- up_value_grad: float32 [2048, 5632], P('fs', 'tp')
- conv_weight_grad: float32 [3, 5632], P(None, 'tp')
- conv_bias_grad: float32 [5632], P('tp')
All inputs are finite; a program needn't handle non-finite values.
Results may differ from a plain program's by a relative error of at most 0.013.
Values may be sent and summed in bfloat16 or wider, within the bound.
No kernel may reach another device: no remote copies, remote signals or barrier semaphores. Data moves between devices by JAX's collectives and lax.ppermute only.
A program may use at most 128 MiB of HBM per device.

v0:
```python
import jax
import jax.numpy as jnp
from jax import lax
from jax.sharding import Mesh
from jax.sharding import PartitionSpec as P

FS = ("fs_0", "fs_1")
FS_TP = ("fs_0", "fs_1", "tp")


def copy_for_each(shard, axis):
    peers = lax.axis_size(axis)
    return lax.all_to_all(
        jnp.broadcast_to(shard[None], (peers, *shard.shape)), axis, 0, 0, tiled=True
    )


def taken_together(shard, axis):
    return copy_for_each(shard, axis).sum(axis=0)


def in_one_piece(arrays, axis, dim, along):
    ends, at = ([], 0)
    for a in arrays[:-1]:
        at += a.shape[along]
        ends.append(at)
    both = jnp.concatenate(arrays, axis=along)
    return tuple(jnp.split(lax.all_gather(both, axis, axis=dim, tiled=True), ends, axis=along))


def summed_rows(subtotal, axes):
    for axis in axes:
        subtotal = lax.psum_scatter(subtotal, axis, scatter_dimension=0, tiled=True)
    return subtotal


def in_blocks(shard, dim, peers):
    lengths = shard.shape
    blocks = shard.reshape(*lengths[:dim], peers, lengths[dim] // peers, *lengths[dim + 1 :])
    return jnp.moveaxis(blocks, dim, 0)


def summed_on_arrival(shard, axis, dim):
    blocks = in_blocks(shard, dim, lax.axis_size(axis))
    arrived = lax.all_to_all(blocks, axis, split_axis=0, concat_axis=0, tiled=True)
    return arrived.astype(jnp.float32).sum(axis=0)


def contract_rows(left, right):
    return lax.dot_general(
        left, right, (((0,), (0,)), ((), ())), preferred_element_type=jnp.float32
    )


def contract_cols(left, right):
    return lax.dot_general(
        left, right, (((1,), (1,)), ((), ())), preferred_element_type=jnp.float32
    )


def on_device(
    tokens, gate_pre, value_pre, up_gate_w, up_value_w, conv_weight, conv_bias, hidden_grad
):
    length = gate_pre.shape[0]
    col_count = gate_pre.shape[1]
    scale = float(length * lax.axis_size(FS)) ** (-0.5)
    gate_float = gate_pre.astype(jnp.float32)
    padded = jnp.pad(gate_float, ((2, 0), (0, 0)))
    gate_conv = (
        conv_bias
        + conv_weight[0] * padded[:length]
        + conv_weight[1] * padded[1 : length + 1]
        + conv_weight[2] * padded[2:]
    )
    active, gelu_back = jax.vjp(jax.nn.gelu, gate_conv)
    grad_float = hidden_grad.astype(jnp.float32)
    value_grad = (grad_float * active).astype(jnp.bfloat16)
    conv_grad = gelu_back(grad_float * value_pre.astype(jnp.float32))[0]
    shifted = jnp.pad(conv_grad, ((0, 2), (0, 0)))
    gate_grad = (
        conv_weight[2] * conv_grad
        + conv_weight[1] * shifted[1 : length + 1]
        + conv_weight[0] * shifted[2:]
    ).astype(jnp.bfloat16)
    conv_terms = jnp.stack(
        [
            jnp.sum(conv_grad * padded[:length], axis=0),
            jnp.sum(conv_grad * padded[1 : length + 1], axis=0),
            jnp.sum(conv_grad * padded[2:], axis=0),
            jnp.sum(conv_grad, axis=0),
        ]
    )
    conv_total = taken_together(conv_terms, FS) * scale
    whole_tokens = lax.all_gather(tokens, "tp", axis=0, tiled=True)
    full_gate, full_value = in_one_piece((up_gate_w, up_value_w), FS, 0, 1)
    joined = summed_rows(
        jnp.concatenate(
            [contract_rows(whole_tokens, gate_grad), contract_rows(whole_tokens, value_grad)],
            axis=1,
        ),
        FS,
    )
    gate_out = joined[:, :col_count] * scale
    value_out = joined[:, col_count:] * scale
    input_grad = summed_on_arrival(
        (contract_cols(gate_grad, full_gate) + contract_cols(value_grad, full_value)).astype(
            jnp.bfloat16
        ),
        "tp",
        0,
    ).astype(jnp.bfloat16)
    return (input_grad, gate_out, value_out, conv_total[:3], conv_total[3])


def solution(mesh):
    finer = Mesh(mesh.devices.reshape(8, 4, mesh.shape["tp"]), ("fs_0", "fs_1", "tp"))
    in_specs = (
        P(FS_TP, None),
        P(FS, "tp"),
        P(FS, "tp"),
        P(FS, "tp"),
        P(FS, "tp"),
        P(None, "tp"),
        P("tp"),
        P(FS, "tp"),
    )
    out_specs = (P(FS_TP, None), P(FS, "tp"), P(FS, "tp"), P(None, "tp"), P("tp"))
    return jax.shard_map(
        on_device, mesh=finer, in_specs=in_specs, out_specs=out_specs, check_vma=False
    )
```

profile of v0, /device:TPU:8, one launch (start us, length us, event | category | flops | bytes accessed | tf_op | source)
XLA Modules:
  0.0 301.7 jit_solution(17411305977214108581)
XLA Ops:
  7.2 0.0 all-gather.5.cloned.1.call-start
  7.3 0.7 all-gather.5.cloned.1.call-update
  7.9 0.0 all-gather.3.cloned.1.call-start
  8.0 1.8 pad_maximum_fusion.1
  9.8 0.0 all-gather.3.cloned.1.call-update
  9.8 0.0 reduce-scatter.5.cloned.1.call-start
  9.9 1.8 convert_element_type.26
  11.8 6.5 %multiply_reduce_fusion.2 = (f32[704]{0:T(1024)S(1)}, f32[704]{0:T(1024)S(1)}, f32[704]{0:T(1024)S(1)}, f32[704]{0:T(1024)S(1)}, f32[1024,704]{0,1:T(8,128)S(1)}, /*index=5*/f32[1024,704]{0,1:T(8,128)}) fusion(f32[1024,704]{0,1:T(8,128)S(1)} %convert_element_type.26, bf16[1024,704]{0,1:T(8,128)(2,1)S(1)} %copy-done, bf16[1024,704]{0,1:T(8,128)(2,1)S(1)} %copy-done.2, ...), kind=kLoop, calls=%fused_computation.29 | loop fusion | flops 25949440 | bytes 12998656 | tf_op jit(solution)/shard_map/reduce_sum | solution.py:87
  18.3 3.0 %fusion.6 = bf16[1024,704]{0,1:T(8,128)(2,1)} fusion(f32[1024,704]{0,1:T(8,128)S(1)} %get-tuple-element.32, f32[704]{0:T(1024)S(1)} %get-tuple-element.30, f32[704]{0:T(1024)S(1)} %get-tuple-element.31, f32[704]{0:T(1024)S(1)} %get-tuple-element.29), kind=kLoop, calls=%fused_computation.18 | loop fusion | flops 4325376 | bytes 4333824 | tf_op jit(solution)/shard_map/convert_element_type | solution.py:84
  21.4 25.0 %all-gather.5.cloned.1.call-done = bf16[1024,2048]{1,0:T(8,128)(2,1)} async-done(((bf16[128,2048]{1,0:T(8,128)(2,1)}), bf16[1024,2048]{1,0:T(8,128)(2,1)}) %all-gather.5.cloned.1.call-update) | async-done | bytes 4194320 | tf_op jit(solution)/shard_map/all_gather | solution.py:94
  46.4 8.4 %convolution_bitcast_fusion.1 = f32[2048,704]{0,1:T(8,128)} fusion(bf16[1024,704]{0,1:T(8,128)(2,1)} %fusion.6, bf16[1024,2048]{1,0:T(8,128)(2,1)} %all-gather.5.cloned.1.call-done), kind=kOutput, calls=%fused_computation.5 | convolution fusion | flops 2952790016 | bytes 11403264 | tf_op jit(solution)/shard_map/dot_general | solution.py:50
  54.8 5.3 %convolution_bitcast_fusion = f32[2048,704]{0,1:T(8,128)} fusion(bf16[1024,2048]{1,0:T(8,128)(2,1)S(1)} %copy-done.10, bf16[1024,704]{0,1:T(8,128)(2,1)S(1)} %copy-done.4, f32[1024,704]{0,1:T(8,128)S(1)} %copy-done.1), kind=kOutput, calls=%fused_computation.4 | convolution fusion | flops 2960719872 | bytes 14286848 | tf_op jit(solution)/shard_map/dot_general | solution.py:50
  60.1 10.8 %pad_maximum_fusion = f32[2048,1408]{0,1:T(8,128)} fusion(f32[2048,704]{0,1:T(8,128)} %convolution_bitcast_fusion, f32[2048,704]{0,1:T(8,128)} %convolution_bitcast_fusion.1), kind=kLoop, calls=%fused_computation | loop fusion | flops 2883584 | bytes 23068672 | tf_op jit(solution)/shard_map/concatenate | solution.py:97
  70.9 0.0 reduce-scatter.5.cloned.1.call-update
  71.0 0.8 broadcast_in_dim.2
  71.8 10.0 %all-to-all-start.1 = ((f32[32,4,704]{2,1,0:T(4,128)}), f32[32,4,704]{2,1,0:T(4,128)S(1)}, u32[]{:S(2)}, u32[]{:S(2)}) async-start(f32[32,4,704]{2,1,0:T(4,128)} %broadcast_in_dim.2), calls=%async_computation.2 | async-start | bytes 786432 | tf_op jit(solution)/shard_map/all_to_all | solution.py:13
  81.8 56.8 %all-gather.3.cloned.1.call-done = bf16[2048,1408]{1,0:T(8,128)(2,1)} async-done(((bf16[64,1408]{1,0:T(8,128)(2,1)}), bf16[2048,1408]{1,0:T(8,128)(2,1)}) %all-gather.3.cloned.1.call-update) | async-done | bytes 5767184 | tf_op jit(solution)/shard_map/all_gather | solution.py:28
  138.7 6.0 %fusion.1 = f32[1024,2048]{1,0:T(8,128)S(1)} fusion(bf16[1024,704]{0,1:T(8,128)(2,1)} %fusion.6, bf16[2048,1408]{1,0:T(8,128)(2,1)} %all-gather.3.cloned.1.call-done), kind=kOutput, calls=%fused_computation.13 | convolution fusion | flops 2952790016 | bytes 12976128 | tf_op jit(solution)/shard_map/dot_general | solution.py:56
  144.7 7.6 %add_convert_fusion = bf16[1024,2048]{1,0:T(8,128)(2,1)} fusion(f32[1024,2048]{1,0:T(8,128)S(1)} %fusion.1, bf16[2048,1408]{1,0:T(8,128)(2,1)S(1)} %copy-done.9, bf16[1024,704]{0,1:T(8,128)(2,1)S(1)} %copy-done.5, f32[1024,704]{0,1:T(8,128)S(1)} %copy-done.1), kind=kOutput, calls=%fused_computation.1 | convolution fusion | flops 2964914176 | bytes 20054016 | tf_op jit(solution)/shard_map/dot_general | solution.py:56
  152.3 5.0 %all-to-all-start = ((bf16[8,128,2048]{2,1,0:T(8,128)(2,1)}), bf16[8,128,2048]{2,1,0:T(8,128)(2,1)}, u32[]{:S(2)}, u32[]{:S(2)}) async-start(bf16[8,128,2048]{2,1,0:T(8,128)(2,1)} %bitcast.11), calls=%async_computation | async-start | bytes 8388608 | tf_op jit(solution)/shard_map/all_to_all | solution.py:45
  157.3 105.4 %reduce-scatter.5.cloned.1.call-done = f32[256,1408]{0,1:T(8,128)} async-done(((f32[2048,1408]{0,1:T(8,128)}), f32[256,1408]{0,1:T(8,128)}) %reduce-scatter.5.cloned.1.call-update) | async-done | bytes 1441808 | tf_op jit(solution)/shard_map/reduce_scatter | solution.py:33
  262.6 2.9 copy.22
  265.5 0.0 reduce-scatter.7.cloned.1.call-update
  265.6 0.1 reduce_sum.62
  265.7 0.6 slice_reduce_fusion
  266.3 3.8 %reduce_sum.57 = bf16[128,2048]{1,0:T(8,128)(2,1)} reduce(bf16[8,128,2048]{2,1,0:T(8,128)(2,1)} %all-to-all-done, bf16[]{:T(256)} %constant.19.clone.1), dimensions={0}, to_apply=%region_0.1 | reduce | flops 1835008 | bytes 4718594 | tf_op jit(solution)/shard_map/reduce_sum | solution.py:46
  270.1 21.8 %reduce-scatter.7.cloned.1.call-done = f32[64,1408]{1,0:T(8,128)} async-done(((f32[256,1408]{1,0:T(8,128)}), f32[64,1408]{1,0:T(8,128)}) %reduce-scatter.7.cloned.1.call-update) | async-done | bytes 360464
  292.0 1.1 fusion.18
  293.1 0.2 copy.25
  293.3 0.8 copy.20
  294.1 0.2 copy.26
  294.3 0.8 copy.21
  (34 shorter events, 0.2 us)
Async XLA Ops:
  7.2 4.6 %copy-start = (bf16[1024,704]{0,1:T(8,128)(2,1)S(1)}, bf16[1024,704]{0,1:T(8,128)(2,1)}, u32[]{:S(2)}) copy-start(bf16[1024,704]{0,1:T(8,128)(2,1)} %param.9) | copy-start | bytes 4325380
  7.2 4.5 %copy-start.7 = (f32[3,704]{1,0:T(4,128)S(1)}, f32[3,704]{1,0:T(4,128)}, u32[]{:S(2)}) copy-start(f32[3,704]{1,0:T(4,128)} %param.13) | copy-start | bytes 25348
  7.2 4.6 %copy-start.2 = (bf16[1024,704]{0,1:T(8,128)(2,1)S(1)}, bf16[1024,704]{0,1:T(8,128)(2,1)}, u32[]{:S(2)}) copy-start(bf16[1024,704]{0,1:T(8,128)(2,1)} %param.10) | copy-start | bytes 4325380
  7.2 4.6 %copy-start.8 = (f32[704]{0:T(1024)S(1)}, f32[704]{0:T(1024)}, u32[]{:S(2)}) copy-start(f32[704]{0:T(1024)} %param.14) | copy-start | bytes 8452
  7.2 39.2 %all-gather.5.cloned.1.call-start = ((), (), s32[]{:S(2)}) async-start(), calls=%async_computation.5 | async-start | bytes 4718592 | tf_op jit(solution)/shard_map/all_gather | solution.py:94
  7.9 130.7 %all-gather.3.cloned.1.call-start = ((), (), s32[]{:S(2)}) async-start(), calls=%async_computation.4 | async-start | bytes 5947392 | tf_op jit(solution)/shard_map/all_gather | solution.py:28
  9.8 252.8 %reduce-scatter.5.cloned.1.call-start = ((), (), s32[]{:S(2)}) async-start(), calls=%async_computation.6 | async-start | bytes 12976128 | tf_op jit(solution)/shard_map/reduce_scatter | solution.py:33
  9.9 1.9 copy-start.3
  21.4 33.4 %copy-start.1 = (f32[1024,704]{0,1:T(8,128)S(1)}, f32[1024,704]{0,1:T(8,128)}, u32[]{:S(2)}) copy-start(f32[1024,704]{0,1:T(8,128)} %get-tuple-element.33) | copy-start | bytes 8650756
  46.4 8.4 %copy-start.4 = (bf16[1024,704]{0,1:T(8,128)(2,1)S(1)}, bf16[1024,704]{0,1:T(8,128)(2,1)}, u32[]{:S(2)}) copy-start(bf16[1024,704]{0,1:T(8,128)(2,1)} %param.15) | copy-start | bytes 4325380
  46.4 8.4 %copy-start.10 = (bf16[1024,2048]{1,0:T(8,128)(2,1)S(1)}, bf16[1024,2048]{1,0:T(8,128)(2,1)}, u32[]{:S(2)}) copy-start(bf16[1024,2048]{1,0:T(8,128)(2,1)} %all-gather.5.cloned.1.call-done) | copy-start | bytes 12582916
  71.8 80.4 %all-to-all-start.1 = ((f32[32,4,704]{2,1,0:T(4,128)}), f32[32,4,704]{2,1,0:T(4,128)S(1)}, u32[]{:S(2)}, u32[]{:S(2)}) async-start(f32[32,4,704]{2,1,0:T(4,128)} %broadcast_in_dim.2), calls=%async_computation.2 | async-start | bytes 786432 | tf_op jit(solution)/shard_map/all_to_all | solution.py:13
  138.7 6.0 %copy-start.5 = (bf16[1024,704]{0,1:T(8,128)(2,1)S(1)}, bf16[1024,704]{0,1:T(8,128)(2,1)}, u32[]{:S(2)}) copy-start(bf16[1024,704]{0,1:T(8,128)(2,1)} %param.15) | copy-start | bytes 4325380
  138.7 6.0 %copy-start.9 = (bf16[2048,1408]{1,0:T(8,128)(2,1)S(1)}, bf16[2048,1408]{1,0:T(8,128)(2,1)}, u32[]{:S(2)}) copy-start(bf16[2048,1408]{1,0:T(8,128)(2,1)} %all-gather.3.cloned.1.call-done) | copy-start | bytes 17301508
  152.3 114.0 %all-to-all-start = ((bf16[8,128,2048]{2,1,0:T(8,128)(2,1)}), bf16[8,128,2048]{2,1,0:T(8,128)(2,1)}, u32[]{:S(2)}, u32[]{:S(2)}) async-start(bf16[8,128,2048]{2,1,0:T(8,128)(2,1)} %bitcast.11), calls=%async_computation | async-start | bytes 8388608 | tf_op jit(solution)/shard_map/all_to_all | solution.py:45
  157.3 134.7 %reduce-scatter.7.cloned.1.call-start = ((), (), s32[]{:S(2)}) async-start(), calls=%async_computation.7 | async-start | bytes 1802240
  265.7 27.6 %copy-start.6 = (f32[4,704]{1,0:T(4,128)}, f32[4,704]{1,0:T(4,128)S(1)}, u32[]{:S(2)}) copy-start(f32[4,704]{1,0:T(4,128)S(1)} %broadcast_multiply_fusion.2) | copy-start | bytes 33796
Sparse Core Ops, SparseCore 0:
  9.9 36.4 all-gather.4
  49.5 89.0 all-gather.2
  141.2 121.3 reduce-scatter.4
  265.7 26.2 reduce-scatter.6
where the time goes:
time: 302 us
  waiting for transfers between devices  210 us (70%)
  other arithmetic  28 us (9%)
  matrix products  27.3 us (9%)
  starting transfers between devices  15.1 us (5%)
  between operations  14 us (5%)
  local copies, waits for them, and re-layouts  7.54 us (2%)
    reduce_scatter x1, waiting for transfers between devices, summed_rows(): subtotal = lax.psum_scatter(subtotal, axis, scatter_dimension=0, tiled=True)  105 us
    all_gather x1, waiting for transfers between devices, in_one_piece(): lax.all_gather(both, axis, axis=dim, tiled=True)  56.8 us
    all_gather x1, waiting for transfers between devices, on_device(): whole_tokens = lax.all_gather(tokens, 'tp', axis=0, tiled=True)  25 us
    unnamed x5, waiting for transfers between devices  22.5 us
    dot_general x2, matrix products, contract_rows(): lax.dot_general(left, right, (((0,), (0,)), ((), ())), preferred_element_...  13.7 us
    dot_general x2, matrix products, contract_cols(): lax.dot_general(left, right, (((1,), (1,)), ((), ())), preferred_element_...  13.6 us
    concatenate x1, other arithmetic, on_device(): jnp.concatenate([contract_rows(whole_tokens, gate_grad), contract_rows(wh...  10.8 us
    all_to_all x1, starting transfers between devices, copy_for_each(): lax.all_to_all(jnp.broadcast_to(shard[None], (peers, *shard.shape)), axis...  10 us
  transfers between devices with their start and end apart: 6, of which 4 were waited for; matrix products, arithmetic and copies ran while one was open for 20% of the time, Pallas kernels for 0%

commit v1 on v0

--- a/solution.py
+++ b/solution.py
@@ -29,9 +29,9 @@
 
 
 def summed_rows(subtotal, axes):
-    for axis in axes:
-        subtotal = lax.psum_scatter(subtotal, axis, scatter_dimension=0, tiled=True)
-    return subtotal
+    return lax.psum_scatter(
+        subtotal.astype(jnp.bfloat16), axes, scatter_dimension=0, tiled=True
+    ).astype(jnp.float32)
 
 
 def in_blocks(shard, dim, peers):

time: 302 us -> 377 us (1.25)
  waiting for transfers between devices: 210 us -> 291 us
  other arithmetic: 28 us -> 20.5 us
  local copies, waits for them, and re-layouts: 7.54 us -> 12.7 us
  matrix products: 27.3 us -> 23.3 us
    unnamed x5 -> x4, waiting for transfers between devices: 22.5 us -> 158 us
    reduce_scatter x1 -> x0, waiting for transfers between devices: 105 us -> none  [summed_rows(): subtotal = lax.psum_scatter(subtotal, axis, scatter_dimension=0, tiled=True)]
    all_to_all x1, waiting for transfers between devices: 0.01 us -> 47.6 us  [summed_on_arrival(): lax.all_to_all(blocks, axis, split_axis=0, concat_axis=0, tiled=True)]
    concatenate x1, other arithmetic: 10.8 us -> 3.15 us  [on_device(): jnp.concatenate([contract_rows(whole_tokens, gate_grad), contract_rows(wh...]
    unnamed x27 -> x26, local copies, waits for them, and re-layouts: 4.96 us -> 11.2 us
    dot_general x2, matrix products: 13.7 us -> 9.78 us  [contract_rows(): lax.dot_general(left, right, (((0,), (0,)), ((), ())), preferred_element_...]
  transfers between devices with their start and end apart: 6 -> 5, of which waited for: 4 -> 4; matrix products, arithmetic and copies ran while one was open for 20% -> 14% of each run, Pallas kernels for 0% -> 0%
where the time goes in v1:
time: 377 us
  waiting for transfers between devices  291 us (77%)
  matrix products  23.3 us (6%)
  other arithmetic  20.5 us (5%)
  starting transfers between devices  15.1 us (4%)
  between operations  14 us (4%)
  local copies, waits for them, and re-layouts  12.7 us (3%)
    unnamed x4, waiting for transfers between devices  158 us
    all_gather x1, waiting for transfers between devices, in_one_piece(): lax.all_gather(both, axis, axis=dim, tiled=True)  60.2 us
    all_to_all x1, waiting for transfers between devices, summed_on_arrival(): lax.all_to_all(blocks, axis, split_axis=0, concat_axis=0, tiled=True)  47.6 us
    all_gather x1, waiting for transfers between devices, on_device(): whole_tokens = lax.all_gather(tokens, 'tp', axis=0, tiled=True)  25 us
    dot_general x2, matrix products, contract_cols(): lax.dot_general(left, right, (((1,), (1,)), ((), ())), preferred_element_...  13.5 us
    unnamed x26, local copies, waits for them, and re-layouts  11.2 us
    all_to_all x1, starting transfers between devices, copy_for_each(): lax.all_to_all(jnp.broadcast_to(shard[None], (peers, *shard.shape)), axis...  10 us
    dot_general x2, matrix products, contract_rows(): lax.dot_general(left, right, (((0,), (0,)), ((), ())), preferred_element_...  9.78 us
  transfers between devices with their start and end apart: 5, of which 4 were waited for; matrix products, arithmetic and copies ran while one was open for 14% of the time, Pallas kernels for 0%

profile of v1, /device:TPU:8, one launch (start us, length us, event | category | flops | bytes accessed | tf_op | source)
XLA Modules:
  0.0 376.6 jit_solution(886776564580868433)
XLA Ops:
  7.2 0.0 copy-start
  7.2 0.0 all-gather.5.cloned.1.call-start
  7.3 0.7 all-gather.5.cloned.1.call-update
  7.9 0.0 all-gather.3.cloned.1.call-start
  8.0 1.8 pad_maximum_fusion.1
  9.8 0.0 all-gather.3.cloned.1.call-update
  9.8 0.0 reduce-scatter.4.cloned.1.call-start
  9.9 0.0 copy-start.3
  9.9 1.8 convert_element_type.30
  11.8 6.5 %multiply_reduce_fusion.2 = (f32[704]{0:T(1024)S(1)}, f32[704]{0:T(1024)S(1)}, f32[704]{0:T(1024)S(1)}, f32[704]{0:T(1024)S(1)}, f32[1024,704]{0,1:T(8,128)S(1)}, /*index=5*/f32[1024,704]{0,1:T(8,128)}) fusion(f32[1024,704]{0,1:T(8,128)S(1)} %convert_element_type.30, bf16[1024,704]{0,1:T(8,128)(2,1)S(1)} %copy-done, bf16[1024,704]{0,1:T(8,128)(2,1)S(1)} %copy-done.2, ...), kind=kLoop, calls=%fused_computation.31 | loop fusion | flops 25949440 | bytes 12998656 | tf_op jit(solution)/shard_map/reduce_sum | solution.py:87
  18.3 3.0 fusion.8
  21.3 25.0 %all-gather.5.cloned.1.call-done = bf16[1024,2048]{1,0:T(8,128)(2,1)} async-done(((bf16[128,2048]{1,0:T(8,128)(2,1)}), bf16[1024,2048]{1,0:T(8,128)(2,1)}) %all-gather.5.cloned.1.call-update) | async-done | bytes 4194320 | tf_op jit(solution)/shard_map/all_gather | solution.py:94
  46.4 5.9 %fusion.3 = bf16[2048,704]{0,1:T(8,128)(2,1)S(1)} fusion(bf16[1024,704]{0,1:T(8,128)(2,1)} %fusion.8, bf16[1024,2048]{1,0:T(8,128)(2,1)} %all-gather.5.cloned.1.call-done), kind=kOutput, calls=%fused_computation.15 | convolution fusion | flops 2954231808 | bytes 8519680 | tf_op jit(solution)/shard_map/dot_general | solution.py:50
  52.3 3.9 %fusion.4 = bf16[2048,704]{0,1:T(8,128)(2,1)S(1)} fusion(bf16[1024,2048]{1,0:T(8,128)(2,1)S(1)} %copy-done.10, bf16[1024,704]{0,1:T(8,128)(2,1)S(1)} %copy-done.4, f32[1024,704]{0,1:T(8,128)S(1)} %copy-done.1), kind=kOutput, calls=%fused_computation.16 | convolution fusion | flops 2962161664 | bytes 11403264 | tf_op jit(solution)/shard_map/dot_general | solution.py:50
  56.2 3.1 pad_maximum_fusion
  59.4 8.4 %copy.22 = bf16[2048,1408]{1,0:T(8,128)(2,1)} copy(bf16[2048,1408]{0,1:T(8,128)(2,1)} %pad_maximum_fusion) | data formatting | bytes 11534336
  67.8 0.0 reduce-scatter.4.cloned.1.call-update
  67.8 0.8 broadcast_in_dim.2
  68.6 10.0 %all-to-all-start.1 = ((f32[32,4,704]{2,1,0:T(4,128)}), f32[32,4,704]{2,1,0:T(4,128)S(1)}, u32[]{:S(2)}, u32[]{:S(2)}) async-start(f32[32,4,704]{2,1,0:T(4,128)} %broadcast_in_dim.2), calls=%async_computation.1 | async-start | bytes 786432 | tf_op jit(solution)/shard_map/all_to_all | solution.py:13
  78.7 60.2 %all-gather.3.cloned.1.call-done = bf16[2048,1408]{1,0:T(8,128)(2,1)} async-done(((bf16[64,1408]{1,0:T(8,128)(2,1)}), bf16[2048,1408]{1,0:T(8,128)(2,1)}) %all-gather.3.cloned.1.call-update) | async-done | bytes 5767184 | tf_op jit(solution)/shard_map/all_gather | solution.py:28
  138.9 6.0 %fusion.1 = f32[1024,2048]{1,0:T(8,128)S(1)} fusion(bf16[1024,704]{0,1:T(8,128)(2,1)} %fusion.8, bf16[2048,1408]{1,0:T(8,128)(2,1)} %all-gather.3.cloned.1.call-done), kind=kOutput, calls=%fused_computation.13 | convolution fusion | flops 2952790016 | bytes 12976128 | tf_op jit(solution)/shard_map/dot_general | solution.py:56
  144.9 7.6 %add_convert_fusion = bf16[1024,2048]{1,0:T(8,128)(2,1)} fusion(f32[1024,2048]{1,0:T(8,128)S(1)} %fusion.1, bf16[2048,1408]{1,0:T(8,128)(2,1)S(1)} %copy-done.9, bf16[1024,704]{0,1:T(8,128)(2,1)S(1)} %copy-done.5, f32[1024,704]{0,1:T(8,128)S(1)} %copy-done.1), kind=kOutput, calls=%fused_computation | convolution fusion | flops 2964914176 | bytes 20054016 | tf_op jit(solution)/shard_map/dot_general | solution.py:56
  152.5 5.0 %all-to-all-start = ((bf16[8,128,2048]{2,1,0:T(8,128)(2,1)}), bf16[8,128,2048]{2,1,0:T(8,128)(2,1)}, u32[]{:S(2)}, u32[]{:S(2)}) async-start(bf16[8,128,2048]{2,1,0:T(8,128)(2,1)} %bitcast.11), calls=%async_computation | async-start | bytes 8388608 | tf_op jit(solution)/shard_map/all_to_all | solution.py:45
  157.4 0.1 reduce_sum.62
  157.5 0.6 slice_reduce_fusion
  158.1 47.6 %all-to-all-done = bf16[8,128,2048]{2,1,0:T(8,128)(2,1)} async-done(((bf16[8,128,2048]{2,1,0:T(8,128)(2,1)}), bf16[8,128,2048]{2,1,0:T(8,128)(2,1)}, u32[]{:S(2)}, u32[]{:S(2)}) %all-to-all-start) | async-done | bytes 4194336 | tf_op jit(solution)/shard_map/all_to_all | solution.py:45
  205.8 4.0 %reduce_sum.57 = bf16[128,2048]{1,0:T(8,128)(2,1)} reduce(bf16[8,128,2048]{2,1,0:T(8,128)(2,1)} %all-to-all-done, bf16[]{:T(256)} %constant.19.clone.1), dimensions={0}, to_apply=%region_0.1 | reduce | flops 1835008 | bytes 4718594 | tf_op jit(solution)/shard_map/reduce_sum | solution.py:46
  209.7 157.4 %reduce-scatter.4.cloned.1.call-done = bf16[64,1408]{1,0:T(8,128)(2,1)} async-done(((bf16[2048,1408]{1,0:T(8,128)(2,1)}), bf16[64,1408]{1,0:T(8,128)(2,1)}) %reduce-scatter.4.cloned.1.call-update) | async-done | bytes 180240
  367.2 1.1 copy.23
  368.4 0.1 slice_multiply_fusion
  368.4 0.8 copy.21
  369.3 0.8 copy.20
  (29 shorter events, 0.2 us)
Async XLA Ops:
  7.2 4.6 %copy-start = (bf16[1024,704]{0,1:T(8,128)(2,1)S(1)}, bf16[1024,704]{0,1:T(8,128)(2,1)}, u32[]{:S(2)}) copy-start(bf16[1024,704]{0,1:T(8,128)(2,1)} %param.9) | copy-start | bytes 4325380
  7.2 4.5 %copy-start.7 = (f32[3,704]{1,0:T(4,128)S(1)}, f32[3,704]{1,0:T(4,128)}, u32[]{:S(2)}) copy-start(f32[3,704]{1,0:T(4,128)} %param.13) | copy-start | bytes 25348
  7.2 4.6 %copy-start.8 = (f32[704]{0:T(1024)S(1)}, f32[704]{0:T(1024)}, u32[]{:S(2)}) copy-start(f32[704]{0:T(1024)} %param.14) | copy-start | bytes 8452
  7.2 4.6 %copy-start.2 = (bf16[1024,704]{0,1:T(8,128)(2,1)S(1)}, bf16[1024,704]{0,1:T(8,128)(2,1)}, u32[]{:S(2)}) copy-start(bf16[1024,704]{0,1:T(8,128)(2,1)} %param.10) | copy-start | bytes 4325380
  7.2 39.2 %all-gather.5.cloned.1.call-start = ((), (), s32[]{:S(2)}) async-start(), calls=%async_computation.4 | async-start | bytes 4718592 | tf_op jit(solution)/shard_map/all_gather | solution.py:94
  7.9 131.0 %all-gather.3.cloned.1.call-start = ((), (), s32[]{:S(2)}) async-start(), calls=%async_computation.3 | async-start | bytes 5947392 | tf_op jit(solution)/shard_map/all_gather | solution.py:28
  9.8 357.4 %reduce-scatter.4.cloned.1.call-start = ((), (), s32[]{:S(2)}) async-start(), calls=%async_computation.5 | async-start | bytes 5947392
  9.9 1.9 copy-start.3
  21.3 31.0 %copy-start.1 = (f32[1024,704]{0,1:T(8,128)S(1)}, f32[1024,704]{0,1:T(8,128)}, u32[]{:S(2)}) copy-start(f32[1024,704]{0,1:T(8,128)} %get-tuple-element.33) | copy-start | bytes 8650756
  46.4 5.9 %copy-start.4 = (bf16[1024,704]{0,1:T(8,128)(2,1)S(1)}, bf16[1024,704]{0,1:T(8,128)(2,1)}, u32[]{:S(2)}) copy-start(bf16[1024,704]{0,1:T(8,128)(2,1)} %param.15) | copy-start | bytes 4325380
  46.4 5.9 %copy-start.10 = (bf16[1024,2048]{1,0:T(8,128)(2,1)S(1)}, bf16[1024,2048]{1,0:T(8,128)(2,1)}, u32[]{:S(2)}) copy-start(bf16[1024,2048]{1,0:T(8,128)(2,1)} %all-gather.5.cloned.1.call-done) | copy-start | bytes 12582916
  68.6 83.8 %all-to-all-start.1 = ((f32[32,4,704]{2,1,0:T(4,128)}), f32[32,4,704]{2,1,0:T(4,128)S(1)}, u32[]{:S(2)}, u32[]{:S(2)}) async-start(f32[32,4,704]{2,1,0:T(4,128)} %broadcast_in_dim.2), calls=%async_computation.1 | async-start | bytes 786432 | tf_op jit(solution)/shard_map/all_to_all | solution.py:13
  138.9 6.0 %copy-start.5 = (bf16[1024,704]{0,1:T(8,128)(2,1)S(1)}, bf16[1024,704]{0,1:T(8,128)(2,1)}, u32[]{:S(2)}) copy-start(bf16[1024,704]{0,1:T(8,128)(2,1)} %param.15) | copy-start | bytes 4325380
  138.9 6.0 %copy-start.9 = (bf16[2048,1408]{1,0:T(8,128)(2,1)S(1)}, bf16[2048,1408]{1,0:T(8,128)(2,1)}, u32[]{:S(2)}) copy-start(bf16[2048,1408]{1,0:T(8,128)(2,1)} %all-gather.3.cloned.1.call-done) | copy-start | bytes 17301508
  152.5 53.3 %all-to-all-start = ((bf16[8,128,2048]{2,1,0:T(8,128)(2,1)}), bf16[8,128,2048]{2,1,0:T(8,128)(2,1)}, u32[]{:S(2)}, u32[]{:S(2)}) async-start(bf16[8,128,2048]{2,1,0:T(8,128)(2,1)} %bitcast.11), calls=%async_computation | async-start | bytes 8388608 | tf_op jit(solution)/shard_map/all_to_all | solution.py:45
  157.5 210.8 %copy-start.6 = (f32[4,704]{1,0:T(4,128)}, f32[4,704]{1,0:T(4,128)S(1)}, u32[]{:S(2)}) copy-start(f32[4,704]{1,0:T(4,128)S(1)} %broadcast_multiply_fusion) | copy-start | bytes 33796
Sparse Core Ops, SparseCore 0:
  9.9 36.4 all-gather.4
  49.5 89.3 all-gather.2
  142.9 224.2 reduce-scatter.3

commit v2 on v1

v2 whole, which is shorter than its diff:
```python
import jax
import jax.numpy as jnp
from jax import lax
from jax.sharding import Mesh
from jax.sharding import PartitionSpec as P

FS = ("z", "x")
TP = ("y", "c")
FS_TP = ("z", "x", "y", "c")


def shifted(block, axis, by):
    size = lax.axis_size(axis)
    return lax.ppermute(block, axis, [(i, (i + by) % size) for i in range(size)])


def swapped(block, axis, bit):
    size = lax.axis_size(axis)
    return lax.ppermute(block, axis, [(i, i ^ bit) for i in range(size)])


def place_of(axis, by=0):
    size = lax.axis_size(axis)
    return (lax.axis_index(axis).astype(jnp.uint32) + jnp.uint32(by % size)) & jnp.uint32(size - 1)


def put(out, block, axis, by, dim, half=0, start=0):
    at = [jnp.uint32(0)] * out.ndim
    at[half] = jnp.uint32(start)
    at[dim] = place_of(axis, by)
    return lax.dynamic_update_slice(out, block, at)


def take(terms, axis, by, dim):
    at = [jnp.uint32(0)] * terms.ndim
    at[dim] = place_of(axis, by)
    lengths = list(terms.shape)
    lengths[dim] = 1
    return lax.dynamic_slice(terms, at, lengths)


def exchanged(blocks, axis):
    return lax.all_to_all(blocks, axis, 0, 0, tiled=True)


def copies_of_all(block, axis):
    peers = lax.axis_size(axis)
    return exchanged(jnp.broadcast_to(block[None], (peers, *block.shape)), axis)


def halves(block, dim):
    cut = block.shape[dim] // 2
    return (
        lax.slice_in_dim(block, 0, cut, axis=dim),
        lax.slice_in_dim(block, cut, 2 * cut, axis=dim),
    )


def gathered_four(block, axis, dim, half):
    up, down = shifted(block, axis, 1), shifted(block, axis, -1)
    far_low = shifted(halves(up, half)[0], axis, 1)
    far_high = shifted(halves(down, half)[1], axis, -1)
    lengths = list(block.shape)
    lengths[dim] = 4
    out = put(jnp.zeros(lengths, block.dtype), block, axis, 0, dim)
    out = put(out, up, axis, -1, dim)
    out = put(out, down, axis, 1, dim)
    out = put(out, far_low, axis, 2, dim)
    return put(out, far_high, axis, 2, dim, half, block.shape[half] // 2)


def summed_four(terms, axis, dim, half):
    mine, after, far, before = [take(terms, axis, k, dim) for k in range(4)]
    low = shifted(halves(far, half)[0], axis, 1)
    high = shifted(halves(far, half)[1], axis, -1)
    after_low, after_high = halves(after, half)
    before_low, before_high = halves(before, half)

    def joined(one, other):
        return (one.astype(jnp.float32) + other.astype(jnp.float32)).astype(one.dtype)

    up = lax.concatenate([joined(after_low, low), after_high], half)
    down = lax.concatenate([before_low, joined(before_high, high)], half)
    up, down = shifted(up, axis, 1), shifted(down, axis, -1)
    return mine.astype(jnp.float32) + up.astype(jnp.float32) + down.astype(jnp.float32)


def added_up(blocks):
    return blocks.astype(jnp.float32).sum(axis=0)


def contract_rows(left, right):
    return lax.dot_general(
        left, right, (((0,), (0,)), ((), ())), preferred_element_type=jnp.float32
    )


def contract_cols(left, right):
    return lax.dot_general(
        left, right, (((1,), (1,)), ((), ())), preferred_element_type=jnp.float32
    )


def on_device(
    tokens, gate_pre, value_pre, up_gate_w, up_value_w, conv_weight, conv_bias, hidden_grad
):
    length, cols = gate_pre.shape
    rows, width = tokens.shape
    nz, nx = lax.axis_size("z"), lax.axis_size("x")
    ny, nc = lax.axis_size("y"), lax.axis_size("c")
    share = up_gate_w.shape[0]
    scale = float(length * nz * nx) ** (-0.5)
    narrow = jnp.bfloat16

    value_part = copies_of_all(up_value_w, "x").reshape(nx * share, cols)
    gate_part = copies_of_all(up_gate_w, "z")
    full_value = lax.all_gather(value_part, "z", axis=0, tiled=True)
    full_gate = gathered_four(gate_part[:, None], "x", 1, 0).reshape(width, cols)
    token_blocks = gathered_four(tokens[None], "y", 0, 1)[:, None]
    token_blocks, gate_part = lax.optimization_barrier((token_blocks, gate_part))
    whole_tokens = jnp.zeros((ny, nc, rows, width), tokens.dtype)
    whole_tokens = put(whole_tokens, token_blocks, "c", 0, 1)
    whole_tokens = put(whole_tokens, swapped(token_blocks, "c", 1), "c", 1, 1)
    whole_tokens = whole_tokens.reshape(length, width)

    gate_float = gate_pre.astype(jnp.float32)
    padded = jnp.pad(gate_float, ((2, 0), (0, 0)))
    gate_conv = (
        conv_bias
        + conv_weight[0] * padded[:length]
        + conv_weight[1] * padded[1 : length + 1]
        + conv_weight[2] * padded[2:]
    )
    active, gelu_back = jax.vjp(jax.nn.gelu, gate_conv)
    grad_float = hidden_grad.astype(jnp.float32)
    value_grad = (grad_float * active).astype(narrow)
    conv_grad = gelu_back(grad_float * value_pre.astype(jnp.float32))[0]
    late = jnp.pad(conv_grad, ((0, 2), (0, 0)))
    gate_grad = (
        conv_weight[2] * conv_grad
        + conv_weight[1] * late[1 : length + 1]
        + conv_weight[0] * late[2:]
    ).astype(narrow)
    conv_terms = jnp.stack(
        [
            jnp.sum(conv_grad * padded[:length], axis=0),
            jnp.sum(conv_grad * padded[1 : length + 1], axis=0),
            jnp.sum(conv_grad * padded[2:], axis=0),
            jnp.sum(conv_grad, axis=0),
        ]
    )
    conv_total = added_up(copies_of_all(conv_terms, FS)) * scale

    gate_terms = contract_rows(whole_tokens, gate_grad).astype(narrow)
    value_terms = contract_rows(whole_tokens, value_grad).astype(narrow)
    gate_grad, value_grad, gate_terms, value_terms = lax.optimization_barrier(
        (gate_grad, value_grad, gate_terms, value_terms)
    )
    gate_sums = summed_four(gate_terms.reshape(nz, nx, share, cols), "x", 1, 0)
    value_sums = lax.psum_scatter(value_terms, "z", scatter_dimension=0, tiled=True)
    value_sums, gate_sums = lax.optimization_barrier((value_sums, gate_sums))
    value_out = added_up(exchanged(value_sums.reshape(nx, share, cols), "x")) * scale
    gate_out = (
        lax.psum_scatter(
            gate_sums.astype(narrow).reshape(nz * share, cols), "z", scatter_dimension=0, tiled=True
        ).astype(jnp.float32)
        * scale
    )

    part = contract_cols(value_grad, full_value)
    part = (part + contract_cols(gate_grad, full_gate)).astype(narrow)
    part = part.reshape(ny, nc, rows, width)
    pair = take(part, "c", 0, 1).astype(jnp.float32) + swapped(
        take(part, "c", 1, 1), "c", 1
    ).astype(jnp.float32)
    input_grad = summed_four(pair.astype(narrow)[:, 0], "y", 0, 1)[0].astype(narrow)
    return (input_grad, gate_out, value_out, conv_total[:3], conv_total[3])


def solution(mesh):
    finer = Mesh(mesh.devices.reshape(8, 4, 4, 2), FS_TP)
    in_specs = (
        P(FS_TP, None),
        P(FS, TP),
        P(FS, TP),
        P(FS, TP),
        P(FS, TP),
        P(None, TP),
        P(TP),
        P(FS, TP),
    )
    out_specs = (P(FS_TP, None), P(FS, TP), P(FS, TP), P(None, TP), P(TP))
    return jax.shard_map(
        on_device, mesh=finer, in_specs=in_specs, out_specs=out_specs, check_vma=False
    )
```

time: 377 us -> 221 us (0.59)
  waiting for transfers between devices: 291 us -> 79.6 us
  starting transfers between devices: 15.1 us -> 49.7 us
  local copies, waits for them, and re-layouts: 12.7 us -> 32 us
  other arithmetic: 20.5 us -> 25.7 us
  matrix products: 23.3 us -> 18.8 us
    unnamed x4 -> x3, waiting for transfers between devices: 158 us -> 0.7 us
    all_gather x2 -> x1, waiting for transfers between devices: 85.3 us -> 0.02 us  [on_device(): full_value = lax.all_gather(value_part, 'z', axis=0, tiled=True)]
    ppermute x0 -> x18, waiting for transfers between devices: none -> 44.2 us  [the longest x16 44.2 us: shifted(): lax.ppermute(block, axis, [(i, (i + by) % size) for i in range(size)])]
    all_to_all x2 -> x4, waiting for transfers between devices: 47.6 us -> 16.2 us  [exchanged(): return lax.all_to_all(blocks, axis, 0, 0, tiled=True)]
    ppermute x0 -> x18, starting transfers between devices: none -> 27.2 us  [the longest x16 27.1 us: shifted(): lax.ppermute(block, axis, [(i, (i + by) % size) for i in range(size)])]
    reduce_scatter x0 -> x2, waiting for transfers between devices: none -> 18.4 us  [the longest x1 18.4 us: on_device(): lax.psum_scatter(gate_sums.astype(narrow).reshape(nz * share, cols), 'z',...]
    dynamic_update_slice x0 -> x12, local copies, waits for them, and re-layouts: none -> 12.3 us  [put(): return lax.dynamic_update_slice(out, block, at)]
    unnamed x26 -> x28, local copies, waits for them, and re-layouts: 11.2 us -> 2 us
  transfers between devices with their start and end apart: 5 -> 25, of which waited for: 4 -> 12; matrix products, arithmetic and copies ran while one was open for 14% -> 33% of each run, Pallas kernels for 0% -> 0%
where the time goes in v2:
time: 221 us; the launch traced here: 220 us
  waiting for transfers between devices  79.6 us (36%)
  starting transfers between devices  49.7 us (22%)
  local copies, waits for them, and re-layouts  32 us (14%)
  other arithmetic  25.7 us (12%)
  matrix products  18.8 us (9%)
  between operations  14.2 us (6%)
    ppermute x16, waiting for transfers between devices, shifted(): lax.ppermute(block, axis, [(i, (i + by) % size) for i in range(size)])  44.2 us
    ppermute x16, starting transfers between devices, shifted(): lax.ppermute(block, axis, [(i, (i + by) % size) for i in range(size)])  27.1 us
    all_to_all x4, starting transfers between devices, exchanged(): return lax.all_to_all(blocks, axis, 0, 0, tiled=True)  22.5 us
    reduce_scatter x1, waiting for transfers between devices, on_device(): lax.psum_scatter(gate_sums.astype(narrow).reshape(nz * share, cols), 'z',...  18.4 us
    all_to_all x4, waiting for transfers between devices, exchanged(): return lax.all_to_all(blocks, axis, 0, 0, tiled=True)  16.2 us
    dynamic_update_slice x12, local copies, waits for them, and re-layouts, put(): return lax.dynamic_update_slice(out, block, at)  12.3 us
    dot_general x2, matrix products, contract_cols(): lax.dot_general(left, right, (((1,), (1,)), ((), ())), preferred_element_...  9.74 us
    dot_general x2, matrix products, contract_rows(): lax.dot_general(left, right, (((0,), (0,)), ((), ())), preferred_element_...  9.08 us
  transfers between devices with their start and end apart: 25, of which 12 were waited for; matrix products, arithmetic and copies ran while one was open for 33% of the time, Pallas kernels for 0%

profile of v2, /device:TPU:8, one launch (start us, length us, event | category | flops | bytes accessed | tf_op | source)
XLA Modules:
  0.0 220.0 jit_solution(14339127756717590097)
XLA Ops:
  11.2 4.1 %all-to-all-start.1 = ((bf16[4,64,704]{2,1,0:T(8,128)(2,1)}), bf16[4,64,704]{2,1,0:T(8,128)(2,1)S(1)}, u32[]{:S(2)}, u32[]{:S(2)}) async-start(bf16[4,64,704]{2,1,0:T(8,128)(2,1)} %broadcast_in_dim.54), calls=%async_computation.1 | async-start | bytes 786432 | tf_op jit(solution)/shard_map/all_to_all | solution.py:43
  19.5 3.2 %all-to-all-done.1 = bf16[4,64,704]{2,1,0:T(8,128)(2,1)S(1)} async-done(((bf16[4,64,704]{2,1,0:T(8,128)(2,1)}), bf16[4,64,704]{2,1,0:T(8,128)(2,1)S(1)}, u32[]{:S(2)}, u32[]{:S(2)}) %all-to-all-start.1) | async-done | bytes 360480 | tf_op jit(solution)/shard_map/all_to_all | solution.py:43
  23.8 8.6 %all-to-all-start = ((bf16[8,64,704]{2,1,0:T(8,128)(2,1)}), bf16[8,64,704]{2,1,0:T(8,128)(2,1)}, u32[]{:S(2)}, u32[]{:S(2)}) async-start(bf16[8,64,704]{2,1,0:T(8,128)(2,1)} %broadcast_in_dim.53), calls=%async_computation | async-start | bytes 1572864 | tf_op jit(solution)/shard_map/all_to_all | solution.py:43
  37.3 1.9 bitcast_dynamic-update-slice_fusion.1
  43.9 9.7 %all-to-all-done = bf16[8,64,704]{2,1,0:T(8,128)(2,1)} async-done(((bf16[8,64,704]{2,1,0:T(8,128)(2,1)}), bf16[8,64,704]{2,1,0:T(8,128)(2,1)}, u32[]{:S(2)}, u32[]{:S(2)}) %all-to-all-start) | async-done | bytes 720928 | tf_op jit(solution)/shard_map/all_to_all | solution.py:43
  53.6 8.0 %multiply_reduce_fusion.2 = (f32[704]{0:T(1024)S(1)}, f32[704]{0:T(1024)S(1)}, f32[704]{0:T(1024)S(1)}, f32[704]{0:T(1024)S(1)}, f32[1024,704]{0,1:T(8,128)}, /*index=5*/f32[1024,704]{0,1:T(8,128)S(1)}) fusion(f32[1024,704]{0,1:T(8,128)S(1)} %convert_element_type.147, bf16[1024,704]{0,1:T(8,128)(2,1)} %param.9, bf16[1024,704]{0,1:T(8,128)(2,1)} %param.10, ...), kind=kLoop, calls=%fused_computation.26 | loop fusion | flops 25949440 | bytes 12998656 | tf_op jit(solution)/shard_map/reduce_sum | solution.py:146
  62.3 2.2 %fusion.5 = bf16[1024,704]{0,1:T(8,128)(2,1)} fusion(bf16[1024,704]{0,1:T(8,128)(2,1)S(1)} %copy-done.2, f32[1024,704]{0,1:T(8,128)S(1)} %get-tuple-element.27), kind=kLoop, calls=%fused_computation.17 | loop fusion | flops 7929856 | bytes 5767168 | tf_op jit(solution)/shard_map/convert_element_type | solution.py:136
  64.5 2.5 %collective-permute-start.6 = (bf16[8,1,64,704]{3,2,1,0:T(8,128)(2,1)}, bf16[8,1,64,704]{3,2,1,0:T(8,128)(2,1)S(1)}, u32[]{:S(2)}, u32[]{:S(2)}) collective-permute-start(bf16[8,1,64,704]{3,2,1,0:T(8,128)(2,1)} %bitcast.8), channel_id=1, source_target_pairs={{0,24},{8,0},{16,8},{24,16},{1,25},{9,1},{17,9},{25,17},{2,26},{10... | collective-permute-start | bytes 2162696 | tf_op jit(solution)/shard_map/ppermute | solution.py:14
  67.1 2.1 fusion.3
  71.5 11.4 %collective-permute-done.5 = bf16[8,1,64,704]{3,2,1,0:T(8,128)(2,1)} collective-permute-done((bf16[8,1,64,704]{3,2,1,0:T(8,128)(2,1)}, bf16[8,1,64,704]{3,2,1,0:T(8,128)(2,1)}, u32[]{:S(2)}, u32[]{:S(2)}) %collective-permute-start.5) | collective-permute-done | bytes 720928 | tf_op jit(solution)/shard_map/ppermute | solution.py:14
  85.9 3.3 %collective-permute-start.8 = (bf16[4,1,64,704]{3,2,1,0:T(8,128)(2,1)S(1)}, bf16[4,1,64,704]{3,2,1,0:T(8,128)(2,1)S(1)}, u32[]{:S(2)}, u32[]{:S(2)}) collective-permute-start(bf16[4,1,64,704]{3,2,1,0:T(8,128)(2,1)S(1)} %slice.110), channel_id=1, source_target_pairs={{0,24},{8,0},{16,8},{24,16},{1,25},{9,1},{17,9},{25,17},{2,26},{10... | collective-permute-start | bytes 1081352 | tf_op jit(solution)/shard_map/ppermute | solution.py:14
  90.5 5.6 %collective-permute-done.7 = bf16[4,1,64,704]{3,2,1,0:T(8,128)(2,1)S(1)} collective-permute-done((bf16[4,1,64,704]{3,2,1,0:T(8,128)(2,1)S(1)}, bf16[4,1,64,704]{3,2,1,0:T(8,128)(2,1)S(1)}, u32[]{:S(2)}, u32[]{:S(2)}) %collective-permute-start.7) | collective-permute-done | bytes 360480 | tf_op jit(solution)/shard_map/ppermute | solution.py:14
  98.9 4.6 %convolution_convert_fusion.1 = bf16[2048,704]{0,1:T(8,128)(2,1)} fusion(bf16[1024,704]{0,1:T(8,128)(2,1)S(1)} %fusion.3, bf16[1024,2048]{1,0:T(8,128)(2,1)S(1)} %bitcast.45), kind=kOutput, calls=%fused_computation.7 | convolution fusion | flops 2954231808 | bytes 8519680 | tf_op jit(solution)/shard_map/dot_general | solution.py:93
  103.5 4.5 %convolution_convert_fusion = bf16[2048,704]{0,1:T(8,128)(2,1)} fusion(bf16[1024,704]{0,1:T(8,128)(2,1)S(1)} %copy-done.8, bf16[1024,2048]{1,0:T(8,128)(2,1)S(1)} %bitcast.46), kind=kOutput, calls=%fused_computation.6 | convolution fusion | flops 2954231808 | bytes 8519680 | tf_op jit(solution)/shard_map/dot_general | solution.py:93
  108.1 5.9 %fusion.17 = f32[1024,2048]{1,0:T(8,128)S(1)} fusion(bf16[1024,704]{0,1:T(8,128)(2,1)} %fusion.5, bf16[2048,704]{1,0:T(8,128)(2,1)} %all-gather.2.cloned.1.call-done), kind=kOutput, calls=%fused_computation.71 | convolution fusion | flops 2952790016 | bytes 12713984 | tf_op jit(solution)/shard_map/dot_general | solution.py:99
  114.0 3.8 %add_convert_fusion = bf16[1024,2048]{1,0:T(8,128)(2,1)S(1)} fusion(f32[1024,2048]{1,0:T(8,128)S(1)} %fusion.17, bf16[1024,704]{0,1:T(8,128)(2,1)S(1)} %copy-done.7, bf16[2048,704]{1,0:T(8,128)(2,1)S(1)} %bitcast.47), kind=kOutput, calls=%fused_computation | convolution fusion | flops 2956984320 | bytes 16908288 | tf_op jit(solution)/shard_map/dot_general | solution.py:99
  117.9 1.9 copy-done.3
  121.4 3.1 %copy.18 = bf16[2048,704]{1,0:T(8,128)(2,1)S(1)} copy(bf16[2048,704]{0,1:T(8,128)(2,1)} %convolution_convert_fusion.1) | data formatting | bytes 5767168 | tf_op jit(solution)/shard_map/optimization_barrier | solution.py:156
  125.8 3.7 %collective-permute-start.16 = (bf16[4,1,64,704]{3,2,1,0:T(8,128)(2,1)}, bf16[4,1,64,704]{3,2,1,0:T(8,128)(2,1)}, u32[]{:S(2)}, u32[]{:S(2)}) collective-permute-start(bf16[4,1,64,704]{3,2,1,0:T(8,128)(2,1)} %get-tuple-element.32), channel_id=1, source_target_pairs={{0,24},{8,0},{16,8},{24,16},{1,25},{9,1},{17,9},{25,17},{2,26},{10... | collective-permute-start | bytes 1081352 | tf_op jit(solution)/shard_map/ppermute | solution.py:14
  130.3 5.1 %all-to-all-start.3 = ((f32[32,4,704]{2,1,0:T(4,128)}), f32[32,4,704]{2,1,0:T(4,128)S(1)}, u32[]{:S(2)}, u32[]{:S(2)}) async-start(f32[32,4,704]{2,1,0:T(4,128)} %broadcast_in_dim.57), calls=%async_computation.5 | async-start | bytes 786432 | tf_op jit(solution)/shard_map/all_to_all | solution.py:43
  135.5 4.3 %collective-permute-done.14 = bf16[4,1,64,704]{3,2,1,0:T(8,128)(2,1)} collective-permute-done((bf16[4,1,64,704]{3,2,1,0:T(8,128)(2,1)}, bf16[4,1,64,704]{3,2,1,0:T(8,128)(2,1)}, u32[]{:S(2)}, u32[]{:S(2)}) %collective-permute-start.14) | collective-permute-done | bytes 360480 | tf_op jit(solution)/shard_map/ppermute | solution.py:14
  144.4 2.6 %collective-permute-start.17 = (bf16[8,1,64,704]{3,2,1,0:T(8,128)(2,1)S(1)}, bf16[8,1,64,704]{3,2,1,0:T(8,128)(2,1)S(1)}, u32[]{:S(2)}, u32[]{:S(2)}) collective-permute-start(bf16[8,1,64,704]{3,2,1,0:T(8,128)(2,1)S(1)} %pad_maximum_fusion.1), channel_id=1, source_target_pairs={{0,24},{8,0},{16,8},{24,16},{1,25},{9,1},{17,9},{25,17},{2,26},{10... | collective-permute-start | bytes 2162696 | tf_op jit(solution)/shard_map/ppermute | solution.py:14
  147.0 2.4 %add_convert_fusion.1 = bf16[4,1,128,2048]{3,2,1,0:T(8,128)(2,1)S(1)} fusion(bf16[4,1,128,2048]{3,2,1,0:T(8,128)(2,1)} %collective-permute-done.9, bf16[4,2,128,2048]{3,2,1,0:T(8,128)(2,1)S(1)} %bitcast.44, u32[]{:T(128)S(6)} %and.49), kind=kLoop, calls=%fused_computation.1 | loop fusion | flops 4194304 | bytes 6291460 | tf_op jit(solution)/shard_map/convert_element_type | solution.py:176
  151.1 14.1 %collective-permute-done.15 = bf16[8,1,64,704]{3,2,1,0:T(8,128)(2,1)S(1)} collective-permute-done((bf16[8,1,64,704]{3,2,1,0:T(8,128)(2,1)S(1)}, bf16[8,1,64,704]{3,2,1,0:T(8,128)(2,1)S(1)}, u32[]{:S(2)}, u32[]{:S(2)}) %collective-permute-start.15) | collective-permute-done | bytes 720928 | tf_op jit(solution)/shard_map/ppermute | solution.py:14
  166.4 4.2 %collective-permute-start.12 = (bf16[1,64,2048]{2,1,0:T(8,128)(2,1)S(1)}, bf16[1,64,2048]{2,1,0:T(8,128)(2,1)S(1)}, u32[]{:S(2)}, u32[]{:S(2)}) collective-permute-start(bf16[1,64,2048]{2,1,0:T(8,128)(2,1)S(1)} %get-tuple-element.38), channel_id=1, source_target_pairs={{0,6},{2,0},{4,2},{6,4},{1,7},{3,1},{5,3},{7,5},{8,14},{10,8},{12,... | collective-permute-start | bytes 786440 | tf_op jit(solution)/shard_map/ppermute | solution.py:14
  170.8 4.4 %collective-permute-done.12 = bf16[1,64,2048]{2,1,0:T(8,128)(2,1)S(1)} collective-permute-done((bf16[1,64,2048]{2,1,0:T(8,128)(2,1)S(1)}, bf16[1,64,2048]{2,1,0:T(8,128)(2,1)S(1)}, u32[]{:S(2)}, u32[]{:S(2)}) %collective-permute-start.12) | collective-permute-done | bytes 262176 | tf_op jit(solution)/shard_map/ppermute | solution.py:14
  175.4 2.6 %collective-permute-start.13 = (bf16[1,128,2048]{2,1,0:T(8,128)(2,1)S(1)}, bf16[1,128,2048]{2,1,0:T(8,128)(2,1)S(1)}, u32[]{:S(2)}, u32[]{:S(2)}) collective-permute-start(bf16[1,128,2048]{2,1,0:T(8,128)(2,1)S(1)} %pad_maximum_fusion.3), channel_id=1, source_target_pairs={{0,6},{2,0},{4,2},{6,4},{1,7},{3,1},{5,3},{7,5},{8,14},{10,8},{12,... | collective-permute-start | bytes 1572872 | tf_op jit(solution)/shard_map/ppermute | solution.py:14
  180.6 4.7 %all-to-all-start.2 = ((bf16[4,64,704]{2,1,0:T(8,128)(2,1)}), bf16[4,64,704]{2,1,0:T(8,128)(2,1)S(1)}, u32[]{:S(2)}, u32[]{:S(2)}) async-start(bf16[4,64,704]{2,1,0:T(8,128)(2,1)} %bitcast.18), calls=%async_computation.4 | async-start | bytes 786432 | tf_op jit(solution)/shard_map/all_to_all | solution.py:43
  185.4 2.1 collective-permute-done.13
  187.4 2.1 fusion.14
  189.5 3.2 %all-to-all-done.2 = bf16[4,64,704]{2,1,0:T(8,128)(2,1)S(1)} async-done(((bf16[4,64,704]{2,1,0:T(8,128)(2,1)}), bf16[4,64,704]{2,1,0:T(8,128)(2,1)S(1)}, u32[]{:S(2)}, u32[]{:S(2)}) %all-to-all-start.2) | async-done | bytes 360480 | tf_op jit(solution)/shard_map/all_to_all | solution.py:43
  193.5 18.4 %reduce-scatter.5.cloned.1.call-done = bf16[64,704]{1,0:T(8,128)(2,1)} async-done(((bf16[512,704]{1,0:T(8,128)(2,1)}), bf16[64,704]{1,0:T(8,128)(2,1)}) %reduce-scatter.5.cloned.1.call-update) | async-done | bytes 90128 | tf_op jit(solution)/shard_map/reduce_scatter | solution.py:164
  (109 shorter events, 45.5 us)
Async XLA Ops:
  7.2 9.7 %copy-start.9 = (bf16[128,2048]{1,0:T(8,128)(2,1)S(1)}, bf16[128,2048]{1,0:T(8,128)(2,1)}, u32[]{:S(2)}) copy-start(bf16[128,2048]{1,0:T(8,128)(2,1)} %param.8) | copy-start | bytes 1572868
  7.2 26.0 %collective-permute-start = (bf16[1,128,2048]{2,1,0:T(8,128)(2,1)}, bf16[1,128,2048]{2,1,0:T(8,128)(2,1)}, u32[]{:S(2)}, u32[]{:S(2)}) collective-permute-start(bf16[1,128,2048]{2,1,0:T(8,128)(2,1)} %bitcast.50), channel_id=1, source_target_pairs={{0,2},{2,4},{4,6},{6,0},{1,3},{3,5},{5,7},{7,1},{8,10},{10,12},{12... | collective-permute-start | bytes 1572872 | tf_op jit(solution)/shard_map/ppermute | solution.py:14
  8.8 26.9 %collective-permute-start.1 = (bf16[1,128,2048]{2,1,0:T(8,128)(2,1)}, bf16[1,128,2048]{2,1,0:T(8,128)(2,1)}, u32[]{:S(2)}, u32[]{:S(2)}) collective-permute-start(bf16[1,128,2048]{2,1,0:T(8,128)(2,1)} %bitcast.51), channel_id=1, source_target_pairs={{0,6},{2,0},{4,2},{6,4},{1,7},{3,1},{5,3},{7,5},{8,14},{10,8},{12,... | collective-permute-start | bytes 1572872 | tf_op jit(solution)/shard_map/ppermute | solution.py:14
  11.2 11.6 %all-to-all-start.1 = ((bf16[4,64,704]{2,1,0:T(8,128)(2,1)}), bf16[4,64,704]{2,1,0:T(8,128)(2,1)S(1)}, u32[]{:S(2)}, u32[]{:S(2)}) async-start(bf16[4,64,704]{2,1,0:T(8,128)(2,1)} %broadcast_in_dim.54), calls=%async_computation.1 | async-start | bytes 786432 | tf_op jit(solution)/shard_map/all_to_all | solution.py:43
  22.8 9.6 %copy-start.5 = (bf16[4,64,704]{2,1,0:T(8,128)(2,1)}, bf16[4,64,704]{2,1,0:T(8,128)(2,1)S(1)}, u32[]{:S(2)}) copy-start(bf16[4,64,704]{2,1,0:T(8,128)(2,1)S(1)} %all-to-all-done.1) | copy-start | bytes 1081348
  23.7 29.9 %copy-start.13 = (f32[704]{0:T(1024)S(1)}, f32[704]{0:T(1024)}, u32[]{:S(2)}) copy-start(f32[704]{0:T(1024)} %param.14) | copy-start | bytes 8452
  23.8 29.9 %all-to-all-start = ((bf16[8,64,704]{2,1,0:T(8,128)(2,1)}), bf16[8,64,704]{2,1,0:T(8,128)(2,1)}, u32[]{:S(2)}, u32[]{:S(2)}) async-start(bf16[8,64,704]{2,1,0:T(8,128)(2,1)} %broadcast_in_dim.53), calls=%async_computation | async-start | bytes 1572864 | tf_op jit(solution)/shard_map/all_to_all | solution.py:43
  32.3 75.7 %all-gather.2.cloned.1.call-start = ((), (), s32[]{:S(2)}) async-start(), calls=%async_computation.6 | async-start | bytes 3538944 | tf_op jit(solution)/shard_map/all_gather | solution.py:117
  33.1 142.3 %reduce-scatter.3.cloned.1.call-start = ((), (), s32[]{:S(2)}) async-start(), calls=%async_computation.7 | async-start | bytes 3244032 | tf_op jit(solution)/shard_map/reduce_scatter | solution.py:160
  34.1 6.9 %collective-permute-start.2 = (bf16[1,64,2048]{2,1,0:T(8,128)(2,1)S(1)}, bf16[1,64,2048]{2,1,0:T(8,128)(2,1)S(1)}, u32[]{:S(2)}, u32[]{:S(2)}) collective-permute-start(bf16[1,64,2048]{2,1,0:T(8,128)(2,1)S(1)} %slice.107), channel_id=1, source_target_pairs={{0,2},{2,4},{4,6},{6,0},{1,3},{3,5},{5,7},{7,1},{8,10},{10,12},{12... | collective-permute-start | bytes 786440 | tf_op jit(solution)/shard_map/ppermute | solution.py:14
  36.7 6.4 %collective-permute-start.3 = (bf16[1,64,2048]{2,1,0:T(8,128)(2,1)S(1)}, bf16[1,64,2048]{2,1,0:T(8,128)(2,1)S(1)}, u32[]{:S(2)}, u32[]{:S(2)}) collective-permute-start(bf16[1,64,2048]{2,1,0:T(8,128)(2,1)S(1)} %slice.108), channel_id=1, source_target_pairs={{0,6},{2,0},{4,2},{6,4},{1,7},{3,1},{5,3},{7,5},{8,14},{10,8},{12,... | collective-permute-start | bytes 786440 | tf_op jit(solution)/shard_map/ppermute | solution.py:14
  53.6 43.4 %collective-permute-start.4 = (bf16[4,1,128,2048]{3,2,1,0:T(8,128)(2,1)}, bf16[4,1,128,2048]{3,2,1,0:T(8,128)(2,1)}, u32[]{:S(2)}, u32[]{:S(2)}) collective-permute-start(bf16[4,1,128,2048]{3,2,1,0:T(8,128)(2,1)} %bitcast_dynamic-update-slice_fusion.3), channel_id=1, source_target_pairs={{0,1},{1,0},{2,3},{3,2},{4,5},{5,4},{6,7},{7,6},{8,9},{9,8},{10,11... | collective-permute-start | bytes 6291464 | tf_op jit(solution)/shard_map/ppermute | solution.py:19
  61.6 21.4 %collective-permute-start.5 = (bf16[8,1,64,704]{3,2,1,0:T(8,128)(2,1)}, bf16[8,1,64,704]{3,2,1,0:T(8,128)(2,1)}, u32[]{:S(2)}, u32[]{:S(2)}) collective-permute-start(bf16[8,1,64,704]{3,2,1,0:T(8,128)(2,1)} %bitcast.8), channel_id=1, source_target_pairs={{0,8},{8,16},{16,24},{24,0},{1,9},{9,17},{17,25},{25,1},{2,10},{10... | collective-permute-start | bytes 2162696 | tf_op jit(solution)/shard_map/ppermute | solution.py:14
  64.5 21.3 %collective-permute-start.6 = (bf16[8,1,64,704]{3,2,1,0:T(8,128)(2,1)}, bf16[8,1,64,704]{3,2,1,0:T(8,128)(2,1)S(1)}, u32[]{:S(2)}, u32[]{:S(2)}) collective-permute-start(bf16[8,1,64,704]{3,2,1,0:T(8,128)(2,1)} %bitcast.8), channel_id=1, source_target_pairs={{0,24},{8,0},{16,8},{24,16},{1,25},{9,1},{17,9},{25,17},{2,26},{10... | collective-permute-start | bytes 2162696 | tf_op jit(solution)/shard_map/ppermute | solution.py:14
  69.1 29.8 %copy-start.6 = (bf16[1024,704]{0,1:T(8,128)(2,1)}, bf16[1024,704]{0,1:T(8,128)(2,1)S(1)}, u32[]{:S(2)}) copy-start(bf16[1024,704]{0,1:T(8,128)(2,1)S(1)} %fusion.3) | copy-start | bytes 4325380
  84.0 12.1 %collective-permute-start.7 = (bf16[4,1,64,704]{3,2,1,0:T(8,128)(2,1)S(1)}, bf16[4,1,64,704]{3,2,1,0:T(8,128)(2,1)S(1)}, u32[]{:S(2)}, u32[]{:S(2)}) collective-permute-start(bf16[4,1,64,704]{3,2,1,0:T(8,128)(2,1)S(1)} %slice.109), channel_id=1, source_target_pairs={{0,8},{8,16},{16,24},{24,0},{1,9},{9,17},{17,25},{25,1},{2,10},{10... | collective-permute-start | bytes 1081352 | tf_op jit(solution)/shard_map/ppermute | solution.py:14
  85.9 11.1 %collective-permute-start.8 = (bf16[4,1,64,704]{3,2,1,0:T(8,128)(2,1)S(1)}, bf16[4,1,64,704]{3,2,1,0:T(8,128)(2,1)S(1)}, u32[]{:S(2)}, u32[]{:S(2)}) collective-permute-start(bf16[4,1,64,704]{3,2,1,0:T(8,128)(2,1)S(1)} %slice.110), channel_id=1, source_target_pairs={{0,24},{8,0},{16,8},{24,16},{1,25},{9,1},{17,9},{25,17},{2,26},{10... | collective-permute-start | bytes 1081352 | tf_op jit(solution)/shard_map/ppermute | solution.py:14
  121.4 25.6 %collective-permute-start.9 = (bf16[4,1,128,2048]{3,2,1,0:T(8,128)(2,1)}, bf16[4,1,128,2048]{3,2,1,0:T(8,128)(2,1)}, u32[]{:S(2)}, u32[]{:S(2)}) collective-permute-start(bf16[4,1,128,2048]{3,2,1,0:T(8,128)(2,1)} %constant_dynamic-slice_fusion.4), channel_id=1, source_target_pairs={{0,1},{1,0},{2,3},{3,2},{4,5},{5,4},{6,7},{7,6},{8,9},{9,8},{10,11... | collective-permute-start | bytes 6291464 | tf_op jit(solution)/shard_map/ppermute | solution.py:19
  125.8 14.0 %collective-permute-start.14 = (bf16[4,1,64,704]{3,2,1,0:T(8,128)(2,1)}, bf16[4,1,64,704]{3,2,1,0:T(8,128)(2,1)}, u32[]{:S(2)}, u32[]{:S(2)}) collective-permute-start(bf16[4,1,64,704]{3,2,1,0:T(8,128)(2,1)} %get-tuple-element.30), channel_id=1, source_target_pairs={{0,8},{8,16},{16,24},{24,0},{1,9},{9,17},{17,25},{25,1},{2,10},{10... | collective-permute-start | bytes 1081352 | tf_op jit(solution)/shard_map/ppermute | solution.py:14
  125.8 14.0 %collective-permute-start.16 = (bf16[4,1,64,704]{3,2,1,0:T(8,128)(2,1)}, bf16[4,1,64,704]{3,2,1,0:T(8,128)(2,1)}, u32[]{:S(2)}, u32[]{:S(2)}) collective-permute-start(bf16[4,1,64,704]{3,2,1,0:T(8,128)(2,1)} %get-tuple-element.32), channel_id=1, source_target_pairs={{0,24},{8,0},{16,8},{24,16},{1,25},{9,1},{17,9},{25,17},{2,26},{10... | collective-permute-start | bytes 1081352 | tf_op jit(solution)/shard_map/ppermute | solution.py:14
  130.3 47.7 %all-to-all-start.3 = ((f32[32,4,704]{2,1,0:T(4,128)}), f32[32,4,704]{2,1,0:T(4,128)S(1)}, u32[]{:S(2)}, u32[]{:S(2)}) async-start(f32[32,4,704]{2,1,0:T(4,128)} %broadcast_in_dim.57), calls=%async_computation.5 | async-start | bytes 786432 | tf_op jit(solution)/shard_map/all_to_all | solution.py:43
  135.4 76.5 %reduce-scatter.5.cloned.1.call-start = ((), (), s32[]{:S(2)}) async-start(), calls=%async_computation.8 | async-start | bytes 884736 | tf_op jit(solution)/shard_map/reduce_scatter | solution.py:164
  135.5 11.5 %copy-start.4 = (bf16[1024,2048]{1,0:T(8,128)(2,1)S(1)}, bf16[1024,2048]{1,0:T(8,128)(2,1)}, u32[]{:S(2)}) copy-start(bf16[1024,2048]{1,0:T(8,128)(2,1)} %copy-done.3) | copy-start | bytes 12582916
  142.1 23.0 %collective-permute-start.15 = (bf16[8,1,64,704]{3,2,1,0:T(8,128)(2,1)S(1)}, bf16[8,1,64,704]{3,2,1,0:T(8,128)(2,1)S(1)}, u32[]{:S(2)}, u32[]{:S(2)}) collective-permute-start(bf16[8,1,64,704]{3,2,1,0:T(8,128)(2,1)S(1)} %pad_maximum_fusion), channel_id=1, source_target_pairs={{0,8},{8,16},{16,24},{24,0},{1,9},{9,17},{17,25},{25,1},{2,10},{10... | collective-permute-start | bytes 2162696 | tf_op jit(solution)/shard_map/ppermute | solution.py:14
  144.4 20.7 %collective-permute-start.17 = (bf16[8,1,64,704]{3,2,1,0:T(8,128)(2,1)S(1)}, bf16[8,1,64,704]{3,2,1,0:T(8,128)(2,1)S(1)}, u32[]{:S(2)}, u32[]{:S(2)}) collective-permute-start(bf16[8,1,64,704]{3,2,1,0:T(8,128)(2,1)S(1)} %pad_maximum_fusion.1), channel_id=1, source_target_pairs={{0,24},{8,0},{16,8},{24,16},{1,25},{9,1},{17,9},{25,17},{2,26},{10... | collective-permute-start | bytes 2162696 | tf_op jit(solution)/shard_map/ppermute | solution.py:14
  149.4 16.9 %copy-start.1 = (bf16[4,1,128,2048]{3,2,1,0:T(8,128)(2,1)}, bf16[4,1,128,2048]{3,2,1,0:T(8,128)(2,1)S(1)}, u32[]{:S(2)}) copy-start(bf16[4,1,128,2048]{3,2,1,0:T(8,128)(2,1)S(1)} %add_convert_fusion.1) | copy-start | bytes 6291460
  149.6 21.0 %collective-permute-start.10 = (bf16[1,64,2048]{2,1,0:T(8,128)(2,1)S(1)}, bf16[1,64,2048]{2,1,0:T(8,128)(2,1)S(1)}, u32[]{:S(2)}, u32[]{:S(2)}) collective-permute-start(bf16[1,64,2048]{2,1,0:T(8,128)(2,1)S(1)} %get-tuple-element.37), channel_id=1, source_target_pairs={{0,2},{2,4},{4,6},{6,0},{1,3},{3,5},{5,7},{7,1},{8,10},{10,12},{12... | collective-permute-start | bytes 786440 | tf_op jit(solution)/shard_map/ppermute | solution.py:14
  166.4 8.9 %collective-permute-start.12 = (bf16[1,64,2048]{2,1,0:T(8,128)(2,1)S(1)}, bf16[1,64,2048]{2,1,0:T(8,128)(2,1)S(1)}, u32[]{:S(2)}, u32[]{:S(2)}) collective-permute-start(bf16[1,64,2048]{2,1,0:T(8,128)(2,1)S(1)} %get-tuple-element.38), channel_id=1, source_target_pairs={{0,6},{2,0},{4,2},{6,4},{1,7},{3,1},{5,3},{7,5},{8,14},{10,8},{12,... | collective-permute-start | bytes 786440 | tf_op jit(solution)/shard_map/ppermute | solution.py:14
  170.8 14.6 %collective-permute-start.11 = (bf16[1,128,2048]{2,1,0:T(8,128)(2,1)S(1)}, bf16[1,128,2048]{2,1,0:T(8,128)(2,1)S(1)}, u32[]{:S(2)}, u32[]{:S(2)}) collective-permute-start(bf16[1,128,2048]{2,1,0:T(8,128)(2,1)S(1)} %pad_maximum_fusion.2), channel_id=1, source_target_pairs={{0,2},{2,4},{4,6},{6,0},{1,3},{3,5},{5,7},{7,1},{8,10},{10,12},{12... | collective-permute-start | bytes 1572872 | tf_op jit(solution)/shard_map/ppermute | solution.py:14
  175.4 12.0 %collective-permute-start.13 = (bf16[1,128,2048]{2,1,0:T(8,128)(2,1)S(1)}, bf16[1,128,2048]{2,1,0:T(8,128)(2,1)S(1)}, u32[]{:S(2)}, u32[]{:S(2)}) collective-permute-start(bf16[1,128,2048]{2,1,0:T(8,128)(2,1)S(1)} %pad_maximum_fusion.3), channel_id=1, source_target_pairs={{0,6},{2,0},{4,2},{6,4},{1,7},{3,1},{5,3},{7,5},{8,14},{10,8},{12,... | collective-permute-start | bytes 1572872 | tf_op jit(solution)/shard_map/ppermute | solution.py:14
  178.1 35.4 %copy-start.11 = (f32[4,704]{1,0:T(4,128)}, f32[4,704]{1,0:T(4,128)S(1)}, u32[]{:S(2)}) copy-start(f32[4,704]{1,0:T(4,128)S(1)} %broadcast_multiply_fusion.1) | copy-start | bytes 33796
  180.6 12.1 %all-to-all-start.2 = ((bf16[4,64,704]{2,1,0:T(8,128)(2,1)}), bf16[4,64,704]{2,1,0:T(8,128)(2,1)S(1)}, u32[]{:S(2)}, u32[]{:S(2)}) async-start(bf16[4,64,704]{2,1,0:T(8,128)(2,1)} %bitcast.18), calls=%async_computation.4 | async-start | bytes 786432 | tf_op jit(solution)/shard_map/all_to_all | solution.py:43
  (7 other events, 34.4 us)
Sparse Core Ops, SparseCore 0:
  35.5 46.2 all-gather.1
  108.2 51.8 reduce-scatter.2
  175.5 36.3 reduce-scatter.4

commit v3 on v2

--- a/solution.py
+++ b/solution.py
@@ -24,9 +24,8 @@
     return (lax.axis_index(axis).astype(jnp.uint32) + jnp.uint32(by % size)) & jnp.uint32(size - 1)
 
 
-def put(out, block, axis, by, dim, half=0, start=0):
+def put(out, block, axis, by, dim):
     at = [jnp.uint32(0)] * out.ndim
-    at[half] = jnp.uint32(start)
     at[dim] = place_of(axis, by)
     return lax.dynamic_update_slice(out, block, at)
 
@@ -48,41 +47,24 @@
     return exchanged(jnp.broadcast_to(block[None], (peers, *block.shape)), axis)
 
 
-def halves(block, dim):
-    cut = block.shape[dim] // 2
-    return (
-        lax.slice_in_dim(block, 0, cut, axis=dim),
-        lax.slice_in_dim(block, cut, 2 * cut, axis=dim),
-    )
+def gathered_four(block, axis, dim):
+    size = lax.axis_size(axis)
+    arrived = [shifted(block, axis, k) for k in (1, size - 1, 2)]
+    lengths = list(block.shape)
+    lengths[dim] = size
+    out = jnp.broadcast_to(block, lengths)
+    for k, other in zip((1, size - 1, 2), arrived):
+        out = put(out, other, axis, -k, dim)
+    return out
 
 
-def gathered_four(block, axis, dim, half):
-    up, down = shifted(block, axis, 1), shifted(block, axis, -1)
-    far_low = shifted(halves(up, half)[0], axis, 1)
-    far_high = shifted(halves(down, half)[1], axis, -1)
-    lengths = list(block.shape)
-    lengths[dim] = 4
-    out = put(jnp.zeros(lengths, block.dtype), block, axis, 0, dim)
-    out = put(out, up, axis, -1, dim)
-    out = put(out, down, axis, 1, dim)
-    out = put(out, far_low, axis, 2, dim)
-    return put(out, far_high, axis, 2, dim, half, block.shape[half] // 2)
-
-
-def summed_four(terms, axis, dim, half):
-    mine, after, far, before = [take(terms, axis, k, dim) for k in range(4)]
-    low = shifted(halves(far, half)[0], axis, 1)
-    high = shifted(halves(far, half)[1], axis, -1)
-    after_low, after_high = halves(after, half)
-    before_low, before_high = halves(before, half)
-
-    def joined(one, other):
-        return (one.astype(jnp.float32) + other.astype(jnp.float32)).astype(one.dtype)
-
-    up = lax.concatenate([joined(after_low, low), after_high], half)
-    down = lax.concatenate([before_low, joined(before_high, high)], half)
-    up, down = shifted(up, axis, 1), shifted(down, axis, -1)
-    return mine.astype(jnp.float32) + up.astype(jnp.float32) + down.astype(jnp.float32)
+def summed_four(terms, axis, dim):
+    size = lax.axis_size(axis)
+    total = take(terms, axis, 0, dim).astype(jnp.float32)
+    arrived = [shifted(take(terms, axis, k, dim), axis, k) for k in (1, size - 1, 2)]
+    for other in arrived:
+        total = total + other.astype(jnp.float32)
+    return total
 
 
 def added_up(blocks):
@@ -112,14 +94,11 @@
     scale = float(length * nz * nx) ** (-0.5)
     narrow = jnp.bfloat16
 
-    value_part = copies_of_all(up_value_w, "x").reshape(nx * share, cols)
+    token_blocks = gathered_four(tokens[None], "y", 0)[:, None]
     gate_part = copies_of_all(up_gate_w, "z")
-    full_value = lax.all_gather(value_part, "z", axis=0, tiled=True)
-    full_gate = gathered_four(gate_part[:, None], "x", 1, 0).reshape(width, cols)
-    token_blocks = gathered_four(tokens[None], "y", 0, 1)[:, None]
-    token_blocks, gate_part = lax.optimization_barrier((token_blocks, gate_part))
-    whole_tokens = jnp.zeros((ny, nc, rows, width), tokens.dtype)
-    whole_tokens = put(whole_tokens, token_blocks, "c", 0, 1)
+    full_value = lax.all_gather(up_value_w, FS, axis=0, tiled=True)
+    full_gate = gathered_four(gate_part[:, None], "x", 1).reshape(width, cols)
+    whole_tokens = jnp.broadcast_to(token_blocks, (ny, nc, rows, width))
     whole_tokens = put(whole_tokens, swapped(token_blocks, "c", 1), "c", 1, 1)
     whole_tokens = whole_tokens.reshape(length, width)
 
@@ -153,19 +132,13 @@
 
     gate_terms = contract_rows(whole_tokens, gate_grad).astype(narrow)
     value_terms = contract_rows(whole_tokens, value_grad).astype(narrow)
-    gate_grad, value_grad, gate_terms, value_terms = lax.optimization_barrier(
+    gate_grad, value_grad, _, _ = lax.optimization_barrier(
         (gate_grad, value_grad, gate_terms, value_terms)
     )
-    gate_sums = summed_four(gate_terms.reshape(nz, nx, share, cols), "x", 1, 0)
+    gate_sums = summed_four(gate_terms.reshape(nz, nx, share, cols), "x", 1).astype(narrow)
+    gate_out = added_up(exchanged(gate_sums[:, 0], "z")) * scale
     value_sums = lax.psum_scatter(value_terms, "z", scatter_dimension=0, tiled=True)
-    value_sums, gate_sums = lax.optimization_barrier((value_sums, gate_sums))
-    value_out = added_up(exchanged(value_sums.reshape(nx, share, cols), "x")) * scale
-    gate_out = (
-        lax.psum_scatter(
-            gate_sums.astype(narrow).reshape(nz * share, cols), "z", scatter_dimension=0, tiled=True
-        ).astype(jnp.float32)
-        * scale
-    )
+    value_out = summed_four(value_sums.reshape(nx, share, cols), "x", 0)[0] * scale
 
     part = contract_cols(value_grad, full_value)
     part = (part + contract_cols(gate_grad, full_gate)).astype(narrow)
@@ -173,7 +146,7 @@
     pair = take(part, "c", 0, 1).astype(jnp.float32) + swapped(
         take(part, "c", 1, 1), "c", 1
     ).astype(jnp.float32)
-    input_grad = summed_four(pair.astype(narrow)[:, 0], "y", 0, 1)[0].astype(narrow)
+    input_grad = summed_four(pair.astype(narrow)[:, 0], "y", 0)[0].astype(narrow)
     return (input_grad, gate_out, value_out, conv_total[:3], conv_total[3])
 
 

time: 221 us -> 228 us (1.032)
  waiting for transfers between devices: 79.6 us -> 90.9 us
  starting transfers between devices: 49.7 us -> 43.8 us
  local copies, waits for them, and re-layouts: 32 us -> 27.7 us
  matrix products: 18.8 us -> 21.7 us
    ppermute x16 -> x15, waiting for transfers between devices: 44.2 us -> 72.6 us  [shifted(): lax.ppermute(block, axis, [(i, (i + by) % size) for i in range(size)])]
    reduce_scatter x1 -> x0, waiting for transfers between devices: 18.4 us -> none  [on_device(): lax.psum_scatter(gate_sums.astype(narrow).reshape(nz * share, cols), 'z',...]
    ppermute x16 -> x15, starting transfers between devices: 27.1 us -> 21.6 us  [shifted(): lax.ppermute(block, axis, [(i, (i + by) % size) for i in range(size)])]
    dynamic_update_slice x12 -> x7, local copies, waits for them, and re-layouts: 12.3 us -> 6.82 us  [put(): return lax.dynamic_update_slice(out, block, at)]
    optimization_barrier x2 -> x0, local copies, waits for them, and re-layouts: 5.03 us -> none  [the longest x1 3.13 us: on_device(): lax.optimization_barrier((gate_grad, value_grad, gate_terms, value_terms))]
    convert_element_type x1, other arithmetic: 2.07 us -> 6.9 us  [on_device(): gate_grad = (conv_weight[2] * conv_grad + conv_weight[1] * late[1:length...]
    slice x8 -> x0, local copies, waits for them, and re-layouts: 4.29 us -> none  [the longest x5 3.28 us: halves(): lax.slice_in_dim(block, 0, cut, axis=dim)]
    convert_element_type x0 -> x1, local copies, waits for them, and re-layouts: none -> 3.15 us  [on_device(): gate_terms = contract_rows(whole_tokens, gate_grad).astype(narrow)]
  transfers between devices with their start and end apart: 25 -> 22, of which waited for: 12 -> 10; matrix products, arithmetic and copies ran while one was open for 33% -> 32% of each run, Pallas kernels for 0% -> 0%
where the time goes in v3:
time: 228 us; the launch traced here: 226 us
  waiting for transfers between devices  90.9 us (40%)
  starting transfers between devices  43.8 us (19%)
  local copies, waits for them, and re-layouts  27.7 us (12%)
  other arithmetic  26.3 us (12%)
  matrix products  21.7 us (10%)
  between operations  15.8 us (7%)
    ppermute x15, waiting for transfers between devices, shifted(): lax.ppermute(block, axis, [(i, (i + by) % size) for i in range(size)])  72.6 us
    all_to_all x3, starting transfers between devices, exchanged(): return lax.all_to_all(blocks, axis, 0, 0, tiled=True)  22.1 us
    ppermute x15, starting transfers between devices, shifted(): lax.ppermute(block, axis, [(i, (i + by) % size) for i in range(size)])  21.6 us
    all_to_all x3, waiting for transfers between devices, exchanged(): return lax.all_to_all(blocks, axis, 0, 0, tiled=True)  17.6 us
    dot_general x2, matrix products, contract_rows(): lax.dot_general(left, right, (((0,), (0,)), ((), ())), preferred_element_...  11.9 us
    dot_general x2, matrix products, contract_cols(): lax.dot_general(left, right, (((1,), (1,)), ((), ())), preferred_element_...  9.75 us
    convert_element_type x1, other arithmetic, on_device(): gate_grad = (conv_weight[2] * conv_grad + conv_weight[1] * late[1:length...  6.9 us
    dynamic_update_slice x7, local copies, waits for them, and re-layouts, put(): return lax.dynamic_update_slice(out, block, at)  6.82 us
  transfers between devices with their start and end apart: 22, of which 10 were waited for; matrix products, arithmetic and copies ran while one was open for 32% of the time, Pallas kernels for 0%

profile of v3, /device:TPU:8, one launch (start us, length us, event | category | flops | bytes accessed | tf_op | source)
XLA Modules:
  0.0 226.1 jit_solution(12169726146549118795)
XLA Ops:
  11.1 2.1 collective-permute-start.2
  13.1 1.8 broadcast_in_dim.50
  15.0 8.6 %all-to-all-start = ((bf16[8,64,704]{2,1,0:T(8,128)(2,1)}), bf16[8,64,704]{2,1,0:T(8,128)(2,1)}, u32[]{:S(2)}, u32[]{:S(2)}) async-start(bf16[8,64,704]{2,1,0:T(8,128)(2,1)} %broadcast_in_dim.50), calls=%async_computation | async-start | bytes 1572864 | tf_op jit(solution)/shard_map/all_to_all | solution.py:42
  28.2 7.7 %collective-permute-done.2 = bf16[1,128,2048]{2,1,0:T(8,128)(2,1)S(1)} collective-permute-done((bf16[1,128,2048]{2,1,0:T(8,128)(2,1)}, bf16[1,128,2048]{2,1,0:T(8,128)(2,1)S(1)}, u32[]{:S(2)}, u32[]{:S(2)}) %collective-permute-start.2) | collective-permute-done | bytes 524320 | tf_op jit(solution)/shard_map/ppermute | solution.py:14
  36.8 6.5 %multiply_reduce_fusion.2 = (f32[704]{0:T(1024)S(1)}, f32[704]{0:T(1024)S(1)}, f32[704]{0:T(1024)S(1)}, f32[704]{0:T(1024)S(1)}, f32[1024,704]{0,1:T(8,128)}, /*index=5*/f32[1024,704]{0,1:T(8,128)S(1)}) fusion(f32[1024,704]{0,1:T(8,128)S(1)} %convert_element_type.125, bf16[1024,704]{0,1:T(8,128)(2,1)S(1)} %copy-done.1, bf16[1024,704]{0,1:T(8,128)(2,1)S(1)} %copy-done.5, ...), kind=kLoop, calls=%fused_computation.26 | loop fusion | flops 25949440 | bytes 12998656 | tf_op jit(solution)/shard_map/reduce_sum | solution.py:125
  43.3 4.8 %all-to-all-done = bf16[8,64,704]{2,1,0:T(8,128)(2,1)} async-done(((bf16[8,64,704]{2,1,0:T(8,128)(2,1)}), bf16[8,64,704]{2,1,0:T(8,128)(2,1)}, u32[]{:S(2)}, u32[]{:S(2)}) %all-to-all-start) | async-done | bytes 720928 | tf_op jit(solution)/shard_map/all_to_all | solution.py:42
  51.4 6.9 %fusion.3 = bf16[1024,704]{0,1:T(8,128)(2,1)} fusion(f32[1024,704]{0,1:T(8,128)} %get-tuple-element.16, f32[704]{0:T(1024)S(1)} %get-tuple-element.14, f32[704]{0:T(1024)S(1)} %get-tuple-element.15, f32[704]{0:T(1024)S(1)} %get-tuple-element.13), kind=kLoop, calls=%fused_computation.15 | loop fusion | flops 4325376 | bytes 4333824 | tf_op jit(solution)/shard_map/convert_element_type | solution.py:122
  58.3 1.9 collective-permute-start.6
  60.2 2.4 %fusion.5 = bf16[1024,704]{0,1:T(8,128)(2,1)S(1)} fusion(bf16[1024,704]{0,1:T(8,128)(2,1)} %param.15, f32[1024,704]{0,1:T(8,128)S(1)} %get-tuple-element.17), kind=kLoop, calls=%fused_computation.17 | loop fusion | flops 7929856 | bytes 5767168 | tf_op jit(solution)/shard_map/convert_element_type | solution.py:115
  62.6 10.3 %collective-permute-done.4 = bf16[8,1,64,704]{3,2,1,0:T(8,128)(2,1)} collective-permute-done((bf16[8,1,64,704]{3,2,1,0:T(8,128)(2,1)}, bf16[8,1,64,704]{3,2,1,0:T(8,128)(2,1)}, u32[]{:S(2)}, u32[]{:S(2)}) %collective-permute-start.4) | collective-permute-done | bytes 720928 | tf_op jit(solution)/shard_map/ppermute | solution.py:14
  77.4 20.8 %collective-permute-done.6 = bf16[8,1,64,704]{3,2,1,0:T(8,128)(2,1)S(1)} collective-permute-done((bf16[8,1,64,704]{3,2,1,0:T(8,128)(2,1)}, bf16[8,1,64,704]{3,2,1,0:T(8,128)(2,1)S(1)}, u32[]{:S(2)}, u32[]{:S(2)}) %collective-permute-start.6) | collective-permute-done | bytes 720928 | tf_op jit(solution)/shard_map/ppermute | solution.py:14
  98.3 2.1 broadcast_in_dim.49
  100.5 1.9 constant_dynamic-update-slice_fusion.3
  102.4 1.9 copy-done.4
  104.3 4.5 %convolution_convert_fusion = bf16[2048,704]{0,1:T(8,128)(2,1)} fusion(bf16[1024,704]{0,1:T(8,128)(2,1)S(1)} %fusion.5, bf16[1024,2048]{1,0:T(8,128)(2,1)S(1)} %bitcast.42), kind=kOutput, calls=%fused_computation.6 | convolution fusion | flops 2954231808 | bytes 8519680 | tf_op jit(solution)/shard_map/dot_general | solution.py:75
  108.8 7.4 %convolution_convert_fusion.1 = bf16[2048,704]{0,1:T(8,128)(2,1)} fusion(bf16[1024,704]{0,1:T(8,128)(2,1)} %fusion.3, bf16[1024,2048]{1,0:T(8,128)(2,1)} %bitcast.43), kind=kOutput, calls=%fused_computation.7 | convolution fusion | flops 2954231808 | bytes 8519680 | tf_op jit(solution)/shard_map/dot_general | solution.py:75
  116.2 5.9 %fusion.18 = f32[1024,2048]{1,0:T(8,128)S(1)} fusion(bf16[1024,704]{0,1:T(8,128)(2,1)} %copy-done.7, bf16[2048,704]{1,0:T(8,128)(2,1)} %all-gather.2.cloned.1.call-done), kind=kOutput, calls=%fused_computation.61 | convolution fusion | flops 2952790016 | bytes 12713984 | tf_op jit(solution)/shard_map/dot_general | solution.py:81
  122.2 3.8 %add_convert_fusion = bf16[1024,2048]{1,0:T(8,128)(2,1)S(1)} fusion(f32[1024,2048]{1,0:T(8,128)S(1)} %fusion.18, bf16[1024,704]{0,1:T(8,128)(2,1)S(1)} %copy-done.6, bf16[2048,704]{1,0:T(8,128)(2,1)S(1)} %bitcast.44), kind=kOutput, calls=%fused_computation | convolution fusion | flops 2956984320 | bytes 16908288 | tf_op jit(solution)/shard_map/dot_general | solution.py:81
  128.6 3.1 %copy.21 = bf16[2048,704]{1,0:T(8,128)(2,1)S(1)} copy(bf16[2048,704]{0,1:T(8,128)(2,1)} %convolution_convert_fusion.1) | data formatting | bytes 5767168 | tf_op jit(solution)/shard_map/convert_element_type | solution.py:133
  134.4 2.1 collective-permute-start.12
  137.5 8.5 %all-to-all-start.2 = ((f32[32,4,704]{2,1,0:T(4,128)}), f32[32,4,704]{2,1,0:T(4,128)S(1)}, u32[]{:S(2)}, u32[]{:S(2)}) async-start(f32[32,4,704]{2,1,0:T(4,128)} %broadcast_in_dim.53), calls=%async_computation.3 | async-start | bytes 786432 | tf_op jit(solution)/shard_map/all_to_all | solution.py:42
  146.1 10.8 %collective-permute-done.11 = bf16[8,1,64,704]{3,2,1,0:T(8,128)(2,1)} collective-permute-done((bf16[8,1,64,704]{3,2,1,0:T(8,128)(2,1)}, bf16[8,1,64,704]{3,2,1,0:T(8,128)(2,1)}, u32[]{:S(2)}, u32[]{:S(2)}) %collective-permute-start.11) | collective-permute-done | bytes 720928 | tf_op jit(solution)/shard_map/ppermute | solution.py:14
  156.9 18.1 %collective-permute-done.12 = bf16[8,1,64,704]{3,2,1,0:T(8,128)(2,1)} collective-permute-done((bf16[8,1,64,704]{3,2,1,0:T(8,128)(2,1)}, bf16[8,1,64,704]{3,2,1,0:T(8,128)(2,1)}, u32[]{:S(2)}, u32[]{:S(2)}) %collective-permute-start.12) | collective-permute-done | bytes 720928 | tf_op jit(solution)/shard_map/ppermute | solution.py:14
  175.9 2.9 %fusion.15 = bf16[8,64,704]{2,1,0:T(8,128)(2,1)} fusion(bf16[8,1,64,704]{3,2,1,0:T(8,128)(2,1)} %collective-permute-done.13, bf16[8,1,64,704]{3,2,1,0:T(8,128)(2,1)} %collective-permute-done.12, bf16[8,1,64,704]{3,2,1,0:T(8,128)(2,1)} %collective-permute-done.11, bf16[8,4,64,704]{3,2,1,0:T(8,128)(2,1)S(1)} %bitcast.39, u32[]{:T(128)S(6)} %and.53), kind=kLoop, calls=%fused_computation.34 | loop fusion | flops 2883584 | bytes 3604484 | tf_op jit(solution)/shard_map/squeeze | solution.py:139
  178.8 5.0 %all-to-all-start.1 = ((bf16[8,64,704]{2,1,0:T(8,128)(2,1)}), bf16[8,64,704]{2,1,0:T(8,128)(2,1)S(1)}, u32[]{:S(2)}, u32[]{:S(2)}) async-start(bf16[8,64,704]{2,1,0:T(8,128)(2,1)} %fusion.15), calls=%async_computation.1 | async-start | bytes 1572864 | tf_op jit(solution)/shard_map/all_to_all | solution.py:42
  183.9 3.0 %add_convert_fusion.1 = bf16[4,1,128,2048]{3,2,1,0:T(8,128)(2,1)S(1)} fusion(bf16[4,1,128,2048]{3,2,1,0:T(8,128)(2,1)} %collective-permute-done.7, bf16[4,2,128,2048]{3,2,1,0:T(8,128)(2,1)} %bitcast.41, u32[]{:T(128)S(6)} %and.51), kind=kLoop, calls=%fused_computation.1 | loop fusion | flops 4194304 | bytes 6291460 | tf_op jit(solution)/shard_map/convert_element_type | solution.py:149
  188.0 2.5 %collective-permute-start.10 = (bf16[1,128,2048]{2,1,0:T(8,128)(2,1)}, bf16[1,128,2048]{2,1,0:T(8,128)(2,1)}, u32[]{:S(2)}, u32[]{:S(2)}) collective-permute-start(bf16[1,128,2048]{2,1,0:T(8,128)(2,1)} %get-tuple-element.22), channel_id=1, source_target_pairs={{0,4},{2,6},{4,0},{6,2},{1,5},{3,7},{5,1},{7,3},{8,12},{10,14},{12... | collective-permute-start | bytes 1572872 | tf_op jit(solution)/shard_map/ppermute | solution.py:14
  190.9 2.1 collective-permute-start.9
  193.6 12.9 %all-to-all-done.1 = bf16[8,64,704]{2,1,0:T(8,128)(2,1)S(1)} async-done(((bf16[8,64,704]{2,1,0:T(8,128)(2,1)}), bf16[8,64,704]{2,1,0:T(8,128)(2,1)S(1)}, u32[]{:S(2)}, u32[]{:S(2)}) %all-to-all-start.1) | async-done | bytes 720928 | tf_op jit(solution)/shard_map/all_to_all | solution.py:42
  209.4 2.4 %collective-permute-start.15 = (bf16[1,64,704]{2,1,0:T(8,128)(2,1)S(1)}, bf16[1,64,704]{2,1,0:T(8,128)(2,1)S(1)}, u32[]{:S(2)}, u32[]{:S(2)}) collective-permute-start(bf16[1,64,704]{2,1,0:T(8,128)(2,1)S(1)} %get-tuple-element.26), channel_id=1, source_target_pairs={{0,24},{8,0},{16,8},{24,16},{1,25},{9,1},{17,9},{25,17},{2,26},{10... | collective-permute-start | bytes 270344 | tf_op jit(solution)/shard_map/ppermute | solution.py:14
  212.1 3.3 %collective-permute-done.8 = bf16[1,128,2048]{2,1,0:T(8,128)(2,1)} collective-permute-done((bf16[1,128,2048]{2,1,0:T(8,128)(2,1)}, bf16[1,128,2048]{2,1,0:T(8,128)(2,1)}, u32[]{:S(2)}, u32[]{:S(2)}) %collective-permute-start.8) | collective-permute-done | bytes 524320 | tf_op jit(solution)/shard_map/ppermute | solution.py:14
  215.4 2.5 %fusion.16 = bf16[128,2048]{1,0:T(8,128)(2,1)} fusion(bf16[1,128,2048]{2,1,0:T(8,128)(2,1)} %collective-permute-done.10, bf16[1,128,2048]{2,1,0:T(8,128)(2,1)} %collective-permute-done.9, bf16[1,128,2048]{2,1,0:T(8,128)(2,1)} %collective-permute-done.8, bf16[4,1,128,2048]{3,2,1,0:T(8,128)(2,1)S(1)} %add_convert_fusion.1, u32[]{:T(128)S(6)} %and.52), kind=kLoop, calls=%fused_computation.35 | loop fusion | flops 2097152 | bytes 2621444 | tf_op jit(solution)/shard_map/convert_element_type | solution.py:149
  (77 shorter events, 29.6 us)
Async XLA Ops:
  8.0 16.5 %copy-start = (bf16[1024,704]{0,1:T(8,128)(2,1)S(1)}, bf16[1024,704]{0,1:T(8,128)(2,1)}, u32[]{:S(2)}) copy-start(bf16[1024,704]{0,1:T(8,128)(2,1)} %param.9) | copy-start | bytes 4325380
  8.0 108.2 %all-gather.2.cloned.1.call-start = ((), (), s32[]{:S(2)}) async-start(), calls=%async_computation.4 | async-start | bytes 3244032 | tf_op jit(solution)/shard_map/all_gather | solution.py:99
  8.7 16.2 %collective-permute-start = (bf16[1,128,2048]{2,1,0:T(8,128)(2,1)}, bf16[1,128,2048]{2,1,0:T(8,128)(2,1)S(1)}, u32[]{:S(2)}, u32[]{:S(2)}) collective-permute-start(bf16[1,128,2048]{2,1,0:T(8,128)(2,1)} %bitcast.47), channel_id=1, source_target_pairs={{0,2},{2,4},{4,6},{6,0},{1,3},{3,5},{5,7},{7,1},{8,10},{10,12},{12... | collective-permute-start | bytes 1572872 | tf_op jit(solution)/shard_map/ppermute | solution.py:14
  10.4 17.0 %collective-permute-start.1 = (bf16[1,128,2048]{2,1,0:T(8,128)(2,1)}, bf16[1,128,2048]{2,1,0:T(8,128)(2,1)S(1)}, u32[]{:S(2)}, u32[]{:S(2)}) collective-permute-start(bf16[1,128,2048]{2,1,0:T(8,128)(2,1)} %bitcast.48), channel_id=1, source_target_pairs={{0,6},{2,0},{4,2},{6,4},{1,7},{3,1},{5,3},{7,5},{8,14},{10,8},{12,... | collective-permute-start | bytes 1572872 | tf_op jit(solution)/shard_map/ppermute | solution.py:14
  11.1 24.9 %collective-permute-start.2 = (bf16[1,128,2048]{2,1,0:T(8,128)(2,1)}, bf16[1,128,2048]{2,1,0:T(8,128)(2,1)S(1)}, u32[]{:S(2)}, u32[]{:S(2)}) collective-permute-start(bf16[1,128,2048]{2,1,0:T(8,128)(2,1)} %bitcast.49), channel_id=1, source_target_pairs={{0,4},{2,6},{4,0},{6,2},{1,5},{3,7},{5,1},{7,3},{8,12},{10,14},{12... | collective-permute-start | bytes 1572872 | tf_op jit(solution)/shard_map/ppermute | solution.py:14
  15.0 10.0 %copy-start.8 = (bf16[128,2048]{1,0:T(8,128)(2,1)S(1)}, bf16[128,2048]{1,0:T(8,128)(2,1)}, u32[]{:S(2)}) copy-start(bf16[128,2048]{1,0:T(8,128)(2,1)} %param.8) | copy-start | bytes 1572868
  15.0 33.1 %all-to-all-start = ((bf16[8,64,704]{2,1,0:T(8,128)(2,1)}), bf16[8,64,704]{2,1,0:T(8,128)(2,1)}, u32[]{:S(2)}, u32[]{:S(2)}) async-start(bf16[8,64,704]{2,1,0:T(8,128)(2,1)} %broadcast_in_dim.50), calls=%async_computation | async-start | bytes 1572864 | tf_op jit(solution)/shard_map/all_to_all | solution.py:42
  23.6 183.7 %reduce-scatter.2.cloned.1.call-start = ((), (), s32[]{:S(2)}) async-start(), calls=%async_computation.5 | async-start | bytes 3244032 | tf_op jit(solution)/shard_map/reduce_scatter | solution.py:140
  24.9 11.9 %copy-start.1 = (bf16[1024,704]{0,1:T(8,128)(2,1)S(1)}, bf16[1024,704]{0,1:T(8,128)(2,1)}, u32[]{:S(2)}) copy-start(bf16[1024,704]{0,1:T(8,128)(2,1)} %param.9) | copy-start | bytes 4325380
  24.9 11.9 %copy-start.2 = (bf16[1024,704]{0,1:T(8,128)(2,1)S(1)}, bf16[1024,704]{0,1:T(8,128)(2,1)}, u32[]{:S(2)}) copy-start(bf16[1024,704]{0,1:T(8,128)(2,1)} %param.15) | copy-start | bytes 4325380
  24.9 11.9 %copy-start.5 = (bf16[1024,704]{0,1:T(8,128)(2,1)S(1)}, bf16[1024,704]{0,1:T(8,128)(2,1)}, u32[]{:S(2)}) copy-start(bf16[1024,704]{0,1:T(8,128)(2,1)} %param.10) | copy-start | bytes 4325380
  24.9 11.9 %copy-start.10 = (f32[704]{0:T(1024)S(1)}, f32[704]{0:T(1024)}, u32[]{:S(2)}) copy-start(f32[704]{0:T(1024)} %param.14) | copy-start | bytes 8452
  36.8 61.5 %collective-permute-start.3 = (bf16[4,1,128,2048]{3,2,1,0:T(8,128)(2,1)}, bf16[4,1,128,2048]{3,2,1,0:T(8,128)(2,1)}, u32[]{:S(2)}, u32[]{:S(2)}) collective-permute-start(bf16[4,1,128,2048]{3,2,1,0:T(8,128)(2,1)} %bitcast_dynamic-update-slice_fusion), channel_id=1, source_target_pairs={{0,1},{1,0},{2,3},{3,2},{4,5},{5,4},{6,7},{7,6},{8,9},{9,8},{10,11... | collective-permute-start | bytes 6291464 | tf_op jit(solution)/shard_map/ppermute | solution.py:19
  48.1 24.8 %collective-permute-start.4 = (bf16[8,1,64,704]{3,2,1,0:T(8,128)(2,1)}, bf16[8,1,64,704]{3,2,1,0:T(8,128)(2,1)}, u32[]{:S(2)}, u32[]{:S(2)}) collective-permute-start(bf16[8,1,64,704]{3,2,1,0:T(8,128)(2,1)} %bitcast.6), channel_id=1, source_target_pairs={{0,8},{8,16},{16,24},{24,0},{1,9},{9,17},{17,25},{25,1},{2,10},{10... | collective-permute-start | bytes 2162696 | tf_op jit(solution)/shard_map/ppermute | solution.py:14
  49.7 26.5 %collective-permute-start.5 = (bf16[8,1,64,704]{3,2,1,0:T(8,128)(2,1)}, bf16[8,1,64,704]{3,2,1,0:T(8,128)(2,1)}, u32[]{:S(2)}, u32[]{:S(2)}) collective-permute-start(bf16[8,1,64,704]{3,2,1,0:T(8,128)(2,1)} %bitcast.6), channel_id=1, source_target_pairs={{0,24},{8,0},{16,8},{24,16},{1,25},{9,1},{17,9},{25,17},{2,26},{10... | collective-permute-start | bytes 2162696 | tf_op jit(solution)/shard_map/ppermute | solution.py:14
  58.3 40.0 %collective-permute-start.6 = (bf16[8,1,64,704]{3,2,1,0:T(8,128)(2,1)}, bf16[8,1,64,704]{3,2,1,0:T(8,128)(2,1)S(1)}, u32[]{:S(2)}, u32[]{:S(2)}) collective-permute-start(bf16[8,1,64,704]{3,2,1,0:T(8,128)(2,1)} %bitcast.6), channel_id=1, source_target_pairs={{0,16},{8,24},{16,0},{24,8},{1,17},{9,25},{17,1},{25,9},{2,18},{10... | collective-permute-start | bytes 2162696 | tf_op jit(solution)/shard_map/ppermute | solution.py:14
  62.6 39.7 %copy-start.7 = (bf16[1024,704]{0,1:T(8,128)(2,1)}, bf16[1024,704]{0,1:T(8,128)(2,1)S(1)}, u32[]{:S(2)}) copy-start(bf16[1024,704]{0,1:T(8,128)(2,1)S(1)} %fusion.5) | copy-start | bytes 4325380
  116.2 6.0 %copy-start.6 = (bf16[1024,704]{0,1:T(8,128)(2,1)S(1)}, bf16[1024,704]{0,1:T(8,128)(2,1)}, u32[]{:S(2)}) copy-start(bf16[1024,704]{0,1:T(8,128)(2,1)} %fusion.3) | copy-start | bytes 4325380
  126.0 2.6 %copy-start.3 = (bf16[1024,2048]{1,0:T(8,128)(2,1)}, bf16[1024,2048]{1,0:T(8,128)(2,1)S(1)}, u32[]{:S(2)}) copy-start(bf16[1024,2048]{1,0:T(8,128)(2,1)S(1)} %add_convert_fusion) | copy-start | bytes 12582916
  128.6 55.3 %collective-permute-start.7 = (bf16[4,1,128,2048]{3,2,1,0:T(8,128)(2,1)}, bf16[4,1,128,2048]{3,2,1,0:T(8,128)(2,1)}, u32[]{:S(2)}, u32[]{:S(2)}) collective-permute-start(bf16[4,1,128,2048]{3,2,1,0:T(8,128)(2,1)} %constant_dynamic-slice_fusion.6), channel_id=1, source_target_pairs={{0,1},{1,0},{2,3},{3,2},{4,5},{5,4},{6,7},{7,6},{8,9},{9,8},{10,11... | collective-permute-start | bytes 6291464 | tf_op jit(solution)/shard_map/ppermute | solution.py:19
  133.2 23.6 %collective-permute-start.11 = (bf16[8,1,64,704]{3,2,1,0:T(8,128)(2,1)}, bf16[8,1,64,704]{3,2,1,0:T(8,128)(2,1)}, u32[]{:S(2)}, u32[]{:S(2)}) collective-permute-start(bf16[8,1,64,704]{3,2,1,0:T(8,128)(2,1)} %get-tuple-element.18), channel_id=1, source_target_pairs={{0,8},{8,16},{16,24},{24,0},{1,9},{9,17},{17,25},{25,1},{2,10},{10... | collective-permute-start | bytes 2162696 | tf_op jit(solution)/shard_map/ppermute | solution.py:14
  134.4 40.6 %collective-permute-start.12 = (bf16[8,1,64,704]{3,2,1,0:T(8,128)(2,1)}, bf16[8,1,64,704]{3,2,1,0:T(8,128)(2,1)}, u32[]{:S(2)}, u32[]{:S(2)}) collective-permute-start(bf16[8,1,64,704]{3,2,1,0:T(8,128)(2,1)} %get-tuple-element.20), channel_id=1, source_target_pairs={{0,24},{8,0},{16,8},{24,16},{1,25},{9,1},{17,9},{25,17},{2,26},{10... | collective-permute-start | bytes 2162696 | tf_op jit(solution)/shard_map/ppermute | solution.py:14
  136.5 39.4 %collective-permute-start.13 = (bf16[8,1,64,704]{3,2,1,0:T(8,128)(2,1)}, bf16[8,1,64,704]{3,2,1,0:T(8,128)(2,1)}, u32[]{:S(2)}, u32[]{:S(2)}) collective-permute-start(bf16[8,1,64,704]{3,2,1,0:T(8,128)(2,1)} %get-tuple-element.19), channel_id=1, source_target_pairs={{0,16},{8,24},{16,0},{24,8},{1,17},{9,25},{17,1},{25,9},{2,18},{10... | collective-permute-start | bytes 2162696 | tf_op jit(solution)/shard_map/ppermute | solution.py:14
  137.5 41.2 %all-to-all-start.2 = ((f32[32,4,704]{2,1,0:T(4,128)}), f32[32,4,704]{2,1,0:T(4,128)S(1)}, u32[]{:S(2)}, u32[]{:S(2)}) async-start(f32[32,4,704]{2,1,0:T(4,128)} %broadcast_in_dim.53), calls=%async_computation.3 | async-start | bytes 786432 | tf_op jit(solution)/shard_map/all_to_all | solution.py:42
  178.8 27.6 %all-to-all-start.1 = ((bf16[8,64,704]{2,1,0:T(8,128)(2,1)}), bf16[8,64,704]{2,1,0:T(8,128)(2,1)S(1)}, u32[]{:S(2)}, u32[]{:S(2)}) async-start(bf16[8,64,704]{2,1,0:T(8,128)(2,1)} %fusion.15), calls=%async_computation.1 | async-start | bytes 1572864 | tf_op jit(solution)/shard_map/all_to_all | solution.py:42
  183.9 9.1 %copy-start.9 = (f32[4,704]{1,0:T(4,128)}, f32[4,704]{1,0:T(4,128)S(1)}, u32[]{:S(2)}) copy-start(f32[4,704]{1,0:T(4,128)S(1)} %broadcast_multiply_fusion.1) | copy-start | bytes 33796
  188.0 23.7 %collective-permute-start.10 = (bf16[1,128,2048]{2,1,0:T(8,128)(2,1)}, bf16[1,128,2048]{2,1,0:T(8,128)(2,1)}, u32[]{:S(2)}, u32[]{:S(2)}) collective-permute-start(bf16[1,128,2048]{2,1,0:T(8,128)(2,1)} %get-tuple-element.22), channel_id=1, source_target_pairs={{0,4},{2,6},{4,0},{6,2},{1,5},{3,7},{5,1},{7,3},{8,12},{10,14},{12... | collective-permute-start | bytes 1572872 | tf_op jit(solution)/shard_map/ppermute | solution.py:14
  190.5 24.9 %collective-permute-start.8 = (bf16[1,128,2048]{2,1,0:T(8,128)(2,1)}, bf16[1,128,2048]{2,1,0:T(8,128)(2,1)}, u32[]{:S(2)}, u32[]{:S(2)}) collective-permute-start(bf16[1,128,2048]{2,1,0:T(8,128)(2,1)} %get-tuple-element.21), channel_id=1, source_target_pairs={{0,2},{2,4},{4,6},{6,0},{1,3},{3,5},{5,7},{7,1},{8,10},{10,12},{12... | collective-permute-start | bytes 1572872 | tf_op jit(solution)/shard_map/ppermute | solution.py:14
  190.9 24.5 %collective-permute-start.9 = (bf16[1,128,2048]{2,1,0:T(8,128)(2,1)S(1)}, bf16[1,128,2048]{2,1,0:T(8,128)(2,1)}, u32[]{:S(2)}, u32[]{:S(2)}) collective-permute-start(bf16[1,128,2048]{2,1,0:T(8,128)(2,1)S(1)} %get-tuple-element.23), channel_id=1, source_target_pairs={{0,6},{2,0},{4,2},{6,4},{1,7},{3,1},{5,3},{7,5},{8,14},{10,8},{12,... | collective-permute-start | bytes 1572872 | tf_op jit(solution)/shard_map/ppermute | solution.py:14
  208.4 9.4 %collective-permute-start.14 = (bf16[1,64,704]{2,1,0:T(8,128)(2,1)S(1)}, bf16[1,64,704]{2,1,0:T(8,128)(2,1)S(1)}, u32[]{:S(2)}, u32[]{:S(2)}) collective-permute-start(bf16[1,64,704]{2,1,0:T(8,128)(2,1)S(1)} %get-tuple-element.24), channel_id=1, source_target_pairs={{0,8},{8,16},{16,24},{24,0},{1,9},{9,17},{17,25},{25,1},{2,10},{10... | collective-permute-start | bytes 270344 | tf_op jit(solution)/shard_map/ppermute | solution.py:14
  209.4 8.5 %collective-permute-start.15 = (bf16[1,64,704]{2,1,0:T(8,128)(2,1)S(1)}, bf16[1,64,704]{2,1,0:T(8,128)(2,1)S(1)}, u32[]{:S(2)}, u32[]{:S(2)}) collective-permute-start(bf16[1,64,704]{2,1,0:T(8,128)(2,1)S(1)} %get-tuple-element.26), channel_id=1, source_target_pairs={{0,24},{8,0},{16,8},{24,16},{1,25},{9,1},{17,9},{25,17},{2,26},{10... | collective-permute-start | bytes 270344 | tf_op jit(solution)/shard_map/ppermute | solution.py:14
  211.8 6.1 %collective-permute-start.16 = (bf16[1,64,704]{2,1,0:T(8,128)(2,1)S(1)}, bf16[1,64,704]{2,1,0:T(8,128)(2,1)S(1)}, u32[]{:S(2)}, u32[]{:S(2)}) collective-permute-start(bf16[1,64,704]{2,1,0:T(8,128)(2,1)S(1)} %get-tuple-element.25), channel_id=1, source_target_pairs={{0,16},{8,24},{16,0},{24,8},{1,17},{9,25},{17,1},{25,9},{2,18},{10... | collective-permute-start | bytes 270344 | tf_op jit(solution)/shard_map/ppermute | solution.py:14
  (1 other events, 2.0 us)
Sparse Core Ops, SparseCore 0:
  11.4 91.2 all-gather.1
Sparse Core Ops, SparseCore 1:
  108.9 50.6 reduce-scatter.1

commit v4 on v3

--- a/solution.py
+++ b/solution.py
@@ -96,12 +96,14 @@
 
     token_blocks = gathered_four(tokens[None], "y", 0)[:, None]
     gate_part = copies_of_all(up_gate_w, "z")
-    full_value = lax.all_gather(up_value_w, FS, axis=0, tiled=True)
+    value_part = gathered_four(up_value_w[None], "x", 0).reshape(nx * share, cols)
+    full_value = lax.all_gather(value_part, "z", axis=0, tiled=True)
     full_gate = gathered_four(gate_part[:, None], "x", 1).reshape(width, cols)
     whole_tokens = jnp.broadcast_to(token_blocks, (ny, nc, rows, width))
     whole_tokens = put(whole_tokens, swapped(token_blocks, "c", 1), "c", 1, 1)
     whole_tokens = whole_tokens.reshape(length, width)
 
+    gate_pre, value_part = lax.optimization_barrier((gate_pre, value_part))
     gate_float = gate_pre.astype(jnp.float32)
     padded = jnp.pad(gate_float, ((2, 0), (0, 0)))
     gate_conv = (
@@ -128,7 +130,8 @@
             jnp.sum(conv_grad, axis=0),
         ]
     )
-    conv_total = added_up(copies_of_all(conv_terms, FS)) * scale
+    conv_copies = copies_of_all(conv_terms, FS)
+    conv_total = added_up(conv_copies) * scale
 
     gate_terms = contract_rows(whole_tokens, gate_grad).astype(narrow)
     value_terms = contract_rows(whole_tokens, value_grad).astype(narrow)
@@ -138,7 +141,7 @@
     gate_sums = summed_four(gate_terms.reshape(nz, nx, share, cols), "x", 1).astype(narrow)
     gate_out = added_up(exchanged(gate_sums[:, 0], "z")) * scale
     value_sums = lax.psum_scatter(value_terms, "z", scatter_dimension=0, tiled=True)
-    value_out = summed_four(value_sums.reshape(nx, share, cols), "x", 0)[0] * scale
+    value_out = added_up(exchanged(value_sums.reshape(nx, share, cols), "x")) * scale
 
     part = contract_cols(value_grad, full_value)
     part = (part + contract_cols(gate_grad, full_gate)).astype(narrow)

time: 228 us -> 237 us (1.039)
  waiting for transfers between devices: 90.9 us -> 99.9 us
  matrix products: 21.7 us -> 26.2 us
    all_to_all x3 -> x4, waiting for transfers between devices: 17.6 us -> 29.5 us  [exchanged(): return lax.all_to_all(blocks, axis, 0, 0, tiled=True)]
    dot_general x2, matrix products: 9.75 us -> 14.2 us  [contract_cols(): lax.dot_general(left, right, (((1,), (1,)), ((), ())), preferred_element_...]
    dynamic_update_slice x7 -> x10, local copies, waits for them, and re-layouts: 6.82 us -> 4.61 us  [put(): return lax.dynamic_update_slice(out, block, at)]
    all_to_all x3 -> x4, starting transfers between devices: 22.1 us -> 20.4 us  [exchanged(): return lax.all_to_all(blocks, axis, 0, 0, tiled=True)]
  transfers between devices with their start and end apart: 22 -> 23, of which waited for: 10 -> 9; matrix products, arithmetic and copies ran while one was open for 32% -> 32% of each run, Pallas kernels for 0% -> 0%
where the time goes in v4:
time: 237 us; the launch traced here: 236 us
  waiting for transfers between devices  99.9 us (42%)
  starting transfers between devices  42.4 us (18%)
  local copies, waits for them, and re-layouts  27.8 us (12%)
  matrix products  26.2 us (11%)
  other arithmetic  25 us (11%)
  between operations  14.4 us (6%)
    ppermute x15, waiting for transfers between devices, shifted(): lax.ppermute(block, axis, [(i, (i + by) % size) for i in range(size)])  70.4 us
    all_to_all x4, waiting for transfers between devices, exchanged(): return lax.all_to_all(blocks, axis, 0, 0, tiled=True)  29.5 us
    ppermute x15, starting transfers between devices, shifted(): lax.ppermute(block, axis, [(i, (i + by) % size) for i in range(size)])  21.9 us
    all_to_all x4, starting transfers between devices, exchanged(): return lax.all_to_all(blocks, axis, 0, 0, tiled=True)  20.4 us
    dot_general x2, matrix products, contract_cols(): lax.dot_general(left, right, (((1,), (1,)), ((), ())), preferred_element_...  14.2 us
    dot_general x2, matrix products, contract_rows(): lax.dot_general(left, right, (((0,), (0,)), ((), ())), preferred_element_...  12 us
    convert_element_type x1, other arithmetic, on_device(): gate_grad = (conv_weight[2] * conv_grad + conv_weight[1] * late[1:length...  6.9 us
    reduce_sum x1, other arithmetic, on_device(): jnp.sum(conv_grad * padded[:length], axis=0)  6.53 us
  transfers between devices with their start and end apart: 23, of which 9 were waited for; matrix products, arithmetic and copies ran while one was open for 32% of the time, Pallas kernels for 0%

profile of v4, /device:TPU:8, one launch (start us, length us, event | category | flops | bytes accessed | tf_op | source)
XLA Modules:
  0.0 235.9 jit_solution(1777199961281688596)
XLA Ops:
  8.8 2.7 %collective-permute-start.2 = (bf16[1,64,704]{2,1,0:T(8,128)(2,1)}, bf16[1,64,704]{2,1,0:T(8,128)(2,1)S(1)}, u32[]{:S(2)}, u32[]{:S(2)}) collective-permute-start(bf16[1,64,704]{2,1,0:T(8,128)(2,1)} %bitcast.50), channel_id=1, source_target_pairs={{0,16},{8,24},{16,0},{24,8},{1,17},{9,25},{17,1},{25,9},{2,18},{10... | collective-permute-start | bytes 270344 | tf_op jit(solution)/shard_map/ppermute | solution.py:14
  17.2 2.4 %collective-permute-start.5 = (bf16[1,128,2048]{2,1,0:T(8,128)(2,1)}, bf16[1,128,2048]{2,1,0:T(8,128)(2,1)S(1)}, u32[]{:S(2)}, u32[]{:S(2)}) collective-permute-start(bf16[1,128,2048]{2,1,0:T(8,128)(2,1)} %bitcast.47), channel_id=1, source_target_pairs={{0,4},{2,6},{4,0},{6,2},{1,5},{3,7},{5,1},{7,3},{8,12},{10,14},{12... | collective-permute-start | bytes 1572872 | tf_op jit(solution)/shard_map/ppermute | solution.py:14
  20.9 1.8 broadcast_in_dim.60
  22.7 8.6 %all-to-all-start = ((bf16[8,64,704]{2,1,0:T(8,128)(2,1)}), bf16[8,64,704]{2,1,0:T(8,128)(2,1)}, u32[]{:S(2)}, u32[]{:S(2)}) async-start(bf16[8,64,704]{2,1,0:T(8,128)(2,1)} %broadcast_in_dim.60), calls=%async_computation | async-start | bytes 1572864 | tf_op jit(solution)/shard_map/all_to_all | solution.py:42
  35.2 7.6 %collective-permute-done.4 = bf16[1,128,2048]{2,1,0:T(8,128)(2,1)S(1)} collective-permute-done((bf16[1,128,2048]{2,1,0:T(8,128)(2,1)}, bf16[1,128,2048]{2,1,0:T(8,128)(2,1)S(1)}, u32[]{:S(2)}, u32[]{:S(2)}) %collective-permute-start.4) | collective-permute-done | bytes 524320 | tf_op jit(solution)/shard_map/ppermute | solution.py:14
  44.6 6.5 %multiply_reduce_fusion.2 = (f32[704]{0:T(1024)S(1)}, f32[704]{0:T(1024)S(1)}, f32[704]{0:T(1024)S(1)}, f32[704]{0:T(1024)S(1)}, f32[1024,704]{0,1:T(8,128)}, /*index=5*/f32[1024,704]{0,1:T(8,128)S(1)}) fusion(f32[1024,704]{0,1:T(8,128)S(1)} %convert_element_type.116, bf16[1024,704]{0,1:T(8,128)(2,1)S(1)} %copy-done.1, bf16[1024,704]{0,1:T(8,128)(2,1)S(1)} %copy-done.7, ...), kind=kLoop, calls=%fused_computation.26 | loop fusion | flops 25949440 | bytes 12998656 | tf_op jit(solution)/shard_map/reduce_sum | solution.py:127
  51.1 10.7 %all-to-all-done = bf16[8,64,704]{2,1,0:T(8,128)(2,1)} async-done(((bf16[8,64,704]{2,1,0:T(8,128)(2,1)}), bf16[8,64,704]{2,1,0:T(8,128)(2,1)}, u32[]{:S(2)}, u32[]{:S(2)}) %all-to-all-start) | async-done | bytes 720928 | tf_op jit(solution)/shard_map/all_to_all | solution.py:42
  61.8 2.7 %collective-permute-start.8 = (bf16[8,1,64,704]{3,2,1,0:T(8,128)(2,1)}, bf16[8,1,64,704]{3,2,1,0:T(8,128)(2,1)S(1)}, u32[]{:S(2)}, u32[]{:S(2)}) collective-permute-start(bf16[8,1,64,704]{3,2,1,0:T(8,128)(2,1)} %bitcast.8), channel_id=1, source_target_pairs={{0,24},{8,0},{16,8},{24,16},{1,25},{9,1},{17,9},{25,17},{2,26},{10... | collective-permute-start | bytes 2162696 | tf_op jit(solution)/shard_map/ppermute | solution.py:14
  64.5 6.9 %fusion.3 = bf16[1024,704]{0,1:T(8,128)(2,1)} fusion(f32[1024,704]{0,1:T(8,128)} %get-tuple-element.18, f32[704]{0:T(1024)S(1)} %get-tuple-element.16, f32[704]{0:T(1024)S(1)} %get-tuple-element.17, f32[704]{0:T(1024)S(1)} %get-tuple-element.15), kind=kLoop, calls=%fused_computation.15 | loop fusion | flops 4325376 | bytes 4333824 | tf_op jit(solution)/shard_map/convert_element_type | solution.py:124
  71.4 1.9 collective-permute-start.9
  74.5 25.6 %collective-permute-done.7 = bf16[8,1,64,704]{3,2,1,0:T(8,128)(2,1)S(1)} collective-permute-done((bf16[8,1,64,704]{3,2,1,0:T(8,128)(2,1)}, bf16[8,1,64,704]{3,2,1,0:T(8,128)(2,1)S(1)}, u32[]{:S(2)}, u32[]{:S(2)}) %collective-permute-start.7) | collective-permute-done | bytes 720928 | tf_op jit(solution)/shard_map/ppermute | solution.py:14
  101.8 2.1 broadcast_in_dim.59
  103.9 1.9 constant_dynamic-update-slice_fusion.3
  105.8 1.9 copy-done.5
  107.7 4.6 %convolution_convert_fusion = bf16[2048,704]{0,1:T(8,128)(2,1)} fusion(bf16[1024,704]{0,1:T(8,128)(2,1)S(1)} %fusion.5, bf16[1024,2048]{1,0:T(8,128)(2,1)S(1)} %bitcast.42), kind=kOutput, calls=%fused_computation.6 | convolution fusion | flops 2954231808 | bytes 8519680 | tf_op jit(solution)/shard_map/dot_general | solution.py:75
  112.3 7.4 %convolution_convert_fusion.1 = bf16[2048,704]{0,1:T(8,128)(2,1)} fusion(bf16[1024,704]{0,1:T(8,128)(2,1)} %fusion.3, bf16[1024,2048]{1,0:T(8,128)(2,1)} %bitcast.43), kind=kOutput, calls=%fused_computation.7 | convolution fusion | flops 2954231808 | bytes 8519680 | tf_op jit(solution)/shard_map/dot_general | solution.py:75
  119.8 5.8 %fusion.18 = f32[1024,2048]{1,0:T(8,128)} fusion(bf16[1024,704]{0,1:T(8,128)(2,1)S(1)} %copy-done.8, bf16[2048,704]{1,0:T(8,128)(2,1)S(1)} %bitcast.44), kind=kOutput, calls=%fused_computation.62 | convolution fusion | flops 2952790016 | bytes 12713984 | tf_op jit(solution)/shard_map/dot_general | solution.py:81
  125.6 8.4 %add_convert_fusion = bf16[1024,2048]{1,0:T(8,128)(2,1)S(1)} fusion(f32[1024,2048]{1,0:T(8,128)} %fusion.18, bf16[1024,704]{0,1:T(8,128)(2,1)} %copy-done.9, bf16[2048,704]{1,0:T(8,128)(2,1)} %all-gather.2.cloned.1.call-done), kind=kOutput, calls=%fused_computation | convolution fusion | flops 2956984320 | bytes 16908288 | tf_op jit(solution)/shard_map/dot_general | solution.py:81
  136.6 3.1 %copy.17 = bf16[2048,704]{1,0:T(8,128)(2,1)S(1)} copy(bf16[2048,704]{0,1:T(8,128)(2,1)} %convolution_convert_fusion.1) | data formatting | bytes 5767168 | tf_op jit(solution)/shard_map/convert_element_type | solution.py:136
  142.4 2.1 collective-permute-start.15
  145.4 4.6 %all-to-all-start.3 = ((f32[32,4,704]{2,1,0:T(4,128)}), f32[32,4,704]{2,1,0:T(4,128)S(1)}, u32[]{:S(2)}, u32[]{:S(2)}) async-start(f32[32,4,704]{2,1,0:T(4,128)} %broadcast_in_dim.63), calls=%async_computation.4 | async-start | bytes 786432 | tf_op jit(solution)/shard_map/all_to_all | solution.py:42
  150.0 33.7 %collective-permute-done.14 = bf16[8,1,64,704]{3,2,1,0:T(8,128)(2,1)} collective-permute-done((bf16[8,1,64,704]{3,2,1,0:T(8,128)(2,1)}, bf16[8,1,64,704]{3,2,1,0:T(8,128)(2,1)}, u32[]{:S(2)}, u32[]{:S(2)}) %collective-permute-start.14) | collective-permute-done | bytes 720928 | tf_op jit(solution)/shard_map/ppermute | solution.py:14
  184.5 3.0 %fusion.15 = bf16[8,64,704]{2,1,0:T(8,128)(2,1)} fusion(bf16[8,1,64,704]{3,2,1,0:T(8,128)(2,1)} %collective-permute-done.16, bf16[8,1,64,704]{3,2,1,0:T(8,128)(2,1)} %collective-permute-done.15, bf16[8,1,64,704]{3,2,1,0:T(8,128)(2,1)} %collective-permute-done.14, bf16[8,4,64,704]{3,2,1,0:T(8,128)(2,1)S(1)} %bitcast.39, u32[]{:T(128)S(6)} %and.52), kind=kLoop, calls=%fused_computation.34 | loop fusion | flops 2883584 | bytes 3604484 | tf_op jit(solution)/shard_map/squeeze | solution.py:142
  187.4 3.5 %all-to-all-start.1 = ((bf16[8,64,704]{2,1,0:T(8,128)(2,1)}), bf16[8,64,704]{2,1,0:T(8,128)(2,1)S(1)}, u32[]{:S(2)}, u32[]{:S(2)}) async-start(bf16[8,64,704]{2,1,0:T(8,128)(2,1)} %fusion.15), calls=%async_computation.1 | async-start | bytes 1572864 | tf_op jit(solution)/shard_map/all_to_all | solution.py:42
  191.1 3.0 %add_convert_fusion.1 = bf16[4,1,128,2048]{3,2,1,0:T(8,128)(2,1)S(1)} fusion(bf16[4,1,128,2048]{3,2,1,0:T(8,128)(2,1)} %collective-permute-done.10, bf16[4,2,128,2048]{3,2,1,0:T(8,128)(2,1)} %bitcast.41, u32[]{:T(128)S(6)} %and.50), kind=kLoop, calls=%fused_computation.1 | loop fusion | flops 4194304 | bytes 6291460 | tf_op jit(solution)/shard_map/convert_element_type | solution.py:152
  196.0 2.1 collective-permute-start.13
  198.8 14.8 %all-to-all-done.1 = bf16[8,64,704]{2,1,0:T(8,128)(2,1)S(1)} async-done(((bf16[8,64,704]{2,1,0:T(8,128)(2,1)}), bf16[8,64,704]{2,1,0:T(8,128)(2,1)S(1)}, u32[]{:S(2)}, u32[]{:S(2)}) %all-to-all-start.1) | async-done | bytes 720928 | tf_op jit(solution)/shard_map/all_to_all | solution.py:42
  214.4 1.9 copy.18
  216.3 3.7 %all-to-all-start.2 = ((bf16[4,64,704]{2,1,0:T(8,128)(2,1)}), bf16[4,64,704]{2,1,0:T(8,128)(2,1)S(1)}, u32[]{:S(2)}, u32[]{:S(2)}) async-start(bf16[4,64,704]{2,1,0:T(8,128)(2,1)} %bitcast.18), calls=%async_computation.3 | async-start | bytes 786432 | tf_op jit(solution)/shard_map/all_to_all | solution.py:42
  219.9 1.8 collective-permute-done.12
  221.7 2.5 %fusion.16 = bf16[128,2048]{1,0:T(8,128)(2,1)} fusion(bf16[1,128,2048]{2,1,0:T(8,128)(2,1)} %collective-permute-done.13, bf16[1,128,2048]{2,1,0:T(8,128)(2,1)} %collective-permute-done.12, bf16[1,128,2048]{2,1,0:T(8,128)(2,1)} %collective-permute-done.11, bf16[4,1,128,2048]{3,2,1,0:T(8,128)(2,1)S(1)} %add_convert_fusion.1, u32[]{:T(128)S(6)} %and.51), kind=kLoop, calls=%fused_computation.36 | loop fusion | flops 2097152 | bytes 2621444 | tf_op jit(solution)/shard_map/convert_element_type | solution.py:152
  224.2 4.0 %all-to-all-done.2 = bf16[4,64,704]{2,1,0:T(8,128)(2,1)S(1)} async-done(((bf16[4,64,704]{2,1,0:T(8,128)(2,1)}), bf16[4,64,704]{2,1,0:T(8,128)(2,1)S(1)}, u32[]{:S(2)}, u32[]{:S(2)}) %all-to-all-start.2) | async-done | bytes 360480 | tf_op jit(solution)/shard_map/all_to_all | solution.py:42
  (87 shorter events, 28.0 us)
Async XLA Ops:
  7.2 25.1 %copy-start = (bf16[1024,704]{0,1:T(8,128)(2,1)S(1)}, bf16[1024,704]{0,1:T(8,128)(2,1)}, u32[]{:S(2)}) copy-start(bf16[1024,704]{0,1:T(8,128)(2,1)} %param.9) | copy-start | bytes 4325380
  7.2 118.4 %all-gather.2.cloned.1.call-start = ((), (), s32[]{:S(2)}) async-start(), calls=%async_computation.5 | async-start | bytes 3538944 | tf_op jit(solution)/shard_map/all_gather | solution.py:100
  7.2 7.3 %collective-permute-start = (bf16[1,64,704]{2,1,0:T(8,128)(2,1)}, bf16[1,64,704]{2,1,0:T(8,128)(2,1)S(1)}, u32[]{:S(2)}, u32[]{:S(2)}) collective-permute-start(bf16[1,64,704]{2,1,0:T(8,128)(2,1)} %bitcast.49), channel_id=1, source_target_pairs={{0,8},{8,16},{16,24},{24,0},{1,9},{9,17},{17,25},{25,1},{2,10},{10... | collective-permute-start | bytes 270344 | tf_op jit(solution)/shard_map/ppermute | solution.py:14
  8.8 7.6 %collective-permute-start.2 = (bf16[1,64,704]{2,1,0:T(8,128)(2,1)}, bf16[1,64,704]{2,1,0:T(8,128)(2,1)S(1)}, u32[]{:S(2)}, u32[]{:S(2)}) collective-permute-start(bf16[1,64,704]{2,1,0:T(8,128)(2,1)} %bitcast.50), channel_id=1, source_target_pairs={{0,16},{8,24},{16,0},{24,8},{1,17},{9,25},{17,1},{25,9},{2,18},{10... | collective-permute-start | bytes 270344 | tf_op jit(solution)/shard_map/ppermute | solution.py:14
  11.5 4.8 %collective-permute-start.1 = (bf16[1,64,704]{2,1,0:T(8,128)(2,1)}, bf16[1,64,704]{2,1,0:T(8,128)(2,1)S(1)}, u32[]{:S(2)}, u32[]{:S(2)}) collective-permute-start(bf16[1,64,704]{2,1,0:T(8,128)(2,1)} %bitcast.51), channel_id=1, source_target_pairs={{0,24},{8,0},{16,8},{24,16},{1,25},{9,1},{17,9},{25,17},{2,26},{10... | collective-permute-start | bytes 270344 | tf_op jit(solution)/shard_map/ppermute | solution.py:14
  13.0 19.7 %collective-permute-start.3 = (bf16[1,128,2048]{2,1,0:T(8,128)(2,1)}, bf16[1,128,2048]{2,1,0:T(8,128)(2,1)S(1)}, u32[]{:S(2)}, u32[]{:S(2)}) collective-permute-start(bf16[1,128,2048]{2,1,0:T(8,128)(2,1)} %bitcast.46), channel_id=1, source_target_pairs={{0,2},{2,4},{4,6},{6,0},{1,3},{3,5},{5,7},{7,1},{8,10},{10,12},{12... | collective-permute-start | bytes 1572872 | tf_op jit(solution)/shard_map/ppermute | solution.py:14
  17.2 26.4 %collective-permute-start.5 = (bf16[1,128,2048]{2,1,0:T(8,128)(2,1)}, bf16[1,128,2048]{2,1,0:T(8,128)(2,1)S(1)}, u32[]{:S(2)}, u32[]{:S(2)}) collective-permute-start(bf16[1,128,2048]{2,1,0:T(8,128)(2,1)} %bitcast.47), channel_id=1, source_target_pairs={{0,4},{2,6},{4,0},{6,2},{1,5},{3,7},{5,1},{7,3},{8,12},{10,14},{12... | collective-permute-start | bytes 1572872 | tf_op jit(solution)/shard_map/ppermute | solution.py:14
  19.5 23.2 %collective-permute-start.4 = (bf16[1,128,2048]{2,1,0:T(8,128)(2,1)}, bf16[1,128,2048]{2,1,0:T(8,128)(2,1)S(1)}, u32[]{:S(2)}, u32[]{:S(2)}) collective-permute-start(bf16[1,128,2048]{2,1,0:T(8,128)(2,1)} %bitcast.48), channel_id=1, source_target_pairs={{0,6},{2,0},{4,2},{6,4},{1,7},{3,1},{5,3},{7,5},{8,14},{10,8},{12,... | collective-permute-start | bytes 1572872 | tf_op jit(solution)/shard_map/ppermute | solution.py:14
  22.7 10.0 %copy-start.10 = (bf16[128,2048]{1,0:T(8,128)(2,1)S(1)}, bf16[128,2048]{1,0:T(8,128)(2,1)}, u32[]{:S(2)}) copy-start(bf16[128,2048]{1,0:T(8,128)(2,1)} %param.8) | copy-start | bytes 1572868
  22.7 39.1 %all-to-all-start = ((bf16[8,64,704]{2,1,0:T(8,128)(2,1)}), bf16[8,64,704]{2,1,0:T(8,128)(2,1)}, u32[]{:S(2)}, u32[]{:S(2)}) async-start(bf16[8,64,704]{2,1,0:T(8,128)(2,1)} %broadcast_in_dim.60), calls=%async_computation | async-start | bytes 1572864 | tf_op jit(solution)/shard_map/all_to_all | solution.py:42
  31.3 183.1 %reduce-scatter.2.cloned.1.call-start = ((), (), s32[]{:S(2)}) async-start(), calls=%async_computation.6 | async-start | bytes 3244032 | tf_op jit(solution)/shard_map/reduce_scatter | solution.py:143
  32.6 12.0 %copy-start.1 = (bf16[1024,704]{0,1:T(8,128)(2,1)S(1)}, bf16[1024,704]{0,1:T(8,128)(2,1)}, u32[]{:S(2)}) copy-start(bf16[1024,704]{0,1:T(8,128)(2,1)} %param.9) | copy-start | bytes 4325380
  32.6 12.0 %copy-start.2 = (bf16[1024,704]{0,1:T(8,128)(2,1)S(1)}, bf16[1024,704]{0,1:T(8,128)(2,1)}, u32[]{:S(2)}) copy-start(bf16[1024,704]{0,1:T(8,128)(2,1)} %param.15) | copy-start | bytes 4325380
  32.6 11.9 %copy-start.7 = (bf16[1024,704]{0,1:T(8,128)(2,1)S(1)}, bf16[1024,704]{0,1:T(8,128)(2,1)}, u32[]{:S(2)}) copy-start(bf16[1024,704]{0,1:T(8,128)(2,1)} %param.10) | copy-start | bytes 4325380
  32.7 11.9 %copy-start.12 = (f32[704]{0:T(1024)S(1)}, f32[704]{0:T(1024)}, u32[]{:S(2)}) copy-start(f32[704]{0:T(1024)} %param.14) | copy-start | bytes 8452
  44.5 57.3 %collective-permute-start.6 = (bf16[4,1,128,2048]{3,2,1,0:T(8,128)(2,1)}, bf16[4,1,128,2048]{3,2,1,0:T(8,128)(2,1)}, u32[]{:S(2)}, u32[]{:S(2)}) collective-permute-start(bf16[4,1,128,2048]{3,2,1,0:T(8,128)(2,1)} %bitcast_dynamic-update-slice_fusion), channel_id=1, source_target_pairs={{0,1},{1,0},{2,3},{3,2},{4,5},{5,4},{6,7},{7,6},{8,9},{9,8},{10,11... | collective-permute-start | bytes 6291464 | tf_op jit(solution)/shard_map/ppermute | solution.py:19
  61.8 11.5 %copy-start.3 = (bf16[1024,704]{0,1:T(8,128)(2,1)S(1)}, bf16[1024,704]{0,1:T(8,128)(2,1)}, u32[]{:S(2)}) copy-start(bf16[1024,704]{0,1:T(8,128)(2,1)} %param.15) | copy-start | bytes 4325380
  61.8 39.8 %collective-permute-start.8 = (bf16[8,1,64,704]{3,2,1,0:T(8,128)(2,1)}, bf16[8,1,64,704]{3,2,1,0:T(8,128)(2,1)S(1)}, u32[]{:S(2)}, u32[]{:S(2)}) collective-permute-start(bf16[8,1,64,704]{3,2,1,0:T(8,128)(2,1)} %bitcast.8), channel_id=1, source_target_pairs={{0,24},{8,0},{16,8},{24,16},{1,25},{9,1},{17,9},{25,17},{2,26},{10... | collective-permute-start | bytes 2162696 | tf_op jit(solution)/shard_map/ppermute | solution.py:14
  64.5 35.6 %collective-permute-start.7 = (bf16[8,1,64,704]{3,2,1,0:T(8,128)(2,1)}, bf16[8,1,64,704]{3,2,1,0:T(8,128)(2,1)S(1)}, u32[]{:S(2)}, u32[]{:S(2)}) collective-permute-start(bf16[8,1,64,704]{3,2,1,0:T(8,128)(2,1)} %bitcast.8), channel_id=1, source_target_pairs={{0,8},{8,16},{16,24},{24,0},{1,9},{9,17},{17,25},{25,1},{2,10},{10... | collective-permute-start | bytes 2162696 | tf_op jit(solution)/shard_map/ppermute | solution.py:14
  71.4 30.3 %collective-permute-start.9 = (bf16[8,1,64,704]{3,2,1,0:T(8,128)(2,1)}, bf16[8,1,64,704]{3,2,1,0:T(8,128)(2,1)S(1)}, u32[]{:S(2)}, u32[]{:S(2)}) collective-permute-start(bf16[8,1,64,704]{3,2,1,0:T(8,128)(2,1)} %bitcast.8), channel_id=1, source_target_pairs={{0,16},{8,24},{16,0},{24,8},{1,17},{9,25},{17,1},{25,9},{2,18},{10... | collective-permute-start | bytes 2162696 | tf_op jit(solution)/shard_map/ppermute | solution.py:14
  74.5 31.3 %copy-start.9 = (bf16[1024,704]{0,1:T(8,128)(2,1)}, bf16[1024,704]{0,1:T(8,128)(2,1)S(1)}, u32[]{:S(2)}) copy-start(bf16[1024,704]{0,1:T(8,128)(2,1)S(1)} %fusion.5) | copy-start | bytes 4325380
  136.6 54.4 %collective-permute-start.10 = (bf16[4,1,128,2048]{3,2,1,0:T(8,128)(2,1)}, bf16[4,1,128,2048]{3,2,1,0:T(8,128)(2,1)}, u32[]{:S(2)}, u32[]{:S(2)}) collective-permute-start(bf16[4,1,128,2048]{3,2,1,0:T(8,128)(2,1)} %constant_dynamic-slice_fusion.3), channel_id=1, source_target_pairs={{0,1},{1,0},{2,3},{3,2},{4,5},{5,4},{6,7},{7,6},{8,9},{9,8},{10,11... | collective-permute-start | bytes 6291464 | tf_op jit(solution)/shard_map/ppermute | solution.py:19
  141.3 42.4 %collective-permute-start.14 = (bf16[8,1,64,704]{3,2,1,0:T(8,128)(2,1)}, bf16[8,1,64,704]{3,2,1,0:T(8,128)(2,1)}, u32[]{:S(2)}, u32[]{:S(2)}) collective-permute-start(bf16[8,1,64,704]{3,2,1,0:T(8,128)(2,1)} %get-tuple-element.20), channel_id=1, source_target_pairs={{0,8},{8,16},{16,24},{24,0},{1,9},{9,17},{17,25},{25,1},{2,10},{10... | collective-permute-start | bytes 2162696 | tf_op jit(solution)/shard_map/ppermute | solution.py:14
  141.3 42.4 %collective-permute-start.16 = (bf16[8,1,64,704]{3,2,1,0:T(8,128)(2,1)}, bf16[8,1,64,704]{3,2,1,0:T(8,128)(2,1)}, u32[]{:S(2)}, u32[]{:S(2)}) collective-permute-start(bf16[8,1,64,704]{3,2,1,0:T(8,128)(2,1)} %get-tuple-element.21), channel_id=1, source_target_pairs={{0,16},{8,24},{16,0},{24,8},{1,17},{9,25},{17,1},{25,9},{2,18},{10... | collective-permute-start | bytes 2162696 | tf_op jit(solution)/shard_map/ppermute | solution.py:14
  142.4 42.1 %collective-permute-start.15 = (bf16[8,1,64,704]{3,2,1,0:T(8,128)(2,1)}, bf16[8,1,64,704]{3,2,1,0:T(8,128)(2,1)}, u32[]{:S(2)}, u32[]{:S(2)}) collective-permute-start(bf16[8,1,64,704]{3,2,1,0:T(8,128)(2,1)} %get-tuple-element.22), channel_id=1, source_target_pairs={{0,24},{8,0},{16,8},{24,16},{1,25},{9,1},{17,9},{25,17},{2,26},{10... | collective-permute-start | bytes 2162696 | tf_op jit(solution)/shard_map/ppermute | solution.py:14
  145.4 42.1 %all-to-all-start.3 = ((f32[32,4,704]{2,1,0:T(4,128)}), f32[32,4,704]{2,1,0:T(4,128)S(1)}, u32[]{:S(2)}, u32[]{:S(2)}) async-start(f32[32,4,704]{2,1,0:T(4,128)} %broadcast_in_dim.63), calls=%async_computation.4 | async-start | bytes 786432 | tf_op jit(solution)/shard_map/all_to_all | solution.py:42
  187.4 26.1 %all-to-all-start.1 = ((bf16[8,64,704]{2,1,0:T(8,128)(2,1)}), bf16[8,64,704]{2,1,0:T(8,128)(2,1)S(1)}, u32[]{:S(2)}, u32[]{:S(2)}) async-start(bf16[8,64,704]{2,1,0:T(8,128)(2,1)} %fusion.15), calls=%async_computation.1 | async-start | bytes 1572864 | tf_op jit(solution)/shard_map/all_to_all | solution.py:42
  195.2 24.8 %collective-permute-start.11 = (bf16[1,128,2048]{2,1,0:T(8,128)(2,1)}, bf16[1,128,2048]{2,1,0:T(8,128)(2,1)}, u32[]{:S(2)}, u32[]{:S(2)}) collective-permute-start(bf16[1,128,2048]{2,1,0:T(8,128)(2,1)} %get-tuple-element.23), channel_id=1, source_target_pairs={{0,2},{2,4},{4,6},{6,0},{1,3},{3,5},{5,7},{7,1},{8,10},{10,12},{12... | collective-permute-start | bytes 1572872 | tf_op jit(solution)/shard_map/ppermute | solution.py:14
  196.0 23.9 %collective-permute-start.13 = (bf16[1,128,2048]{2,1,0:T(8,128)(2,1)}, bf16[1,128,2048]{2,1,0:T(8,128)(2,1)}, u32[]{:S(2)}, u32[]{:S(2)}) collective-permute-start(bf16[1,128,2048]{2,1,0:T(8,128)(2,1)} %get-tuple-element.24), channel_id=1, source_target_pairs={{0,4},{2,6},{4,0},{6,2},{1,5},{3,7},{5,1},{7,3},{8,12},{10,14},{12... | collective-permute-start | bytes 1572872 | tf_op jit(solution)/shard_map/ppermute | solution.py:14
  198.1 23.6 %collective-permute-start.12 = (bf16[1,128,2048]{2,1,0:T(8,128)(2,1)S(1)}, bf16[1,128,2048]{2,1,0:T(8,128)(2,1)}, u32[]{:S(2)}, u32[]{:S(2)}) collective-permute-start(bf16[1,128,2048]{2,1,0:T(8,128)(2,1)S(1)} %get-tuple-element.25), channel_id=1, source_target_pairs={{0,6},{2,0},{4,2},{6,4},{1,7},{3,1},{5,3},{7,5},{8,14},{10,8},{12,... | collective-permute-start | bytes 1572872 | tf_op jit(solution)/shard_map/ppermute | solution.py:14
  198.1 30.2 %copy-start.11 = (f32[4,704]{1,0:T(4,128)}, f32[4,704]{1,0:T(4,128)S(1)}, u32[]{:S(2)}) copy-start(f32[4,704]{1,0:T(4,128)S(1)} %broadcast_multiply_fusion.2) | copy-start | bytes 33796
  216.3 12.0 %all-to-all-start.2 = ((bf16[4,64,704]{2,1,0:T(8,128)(2,1)}), bf16[4,64,704]{2,1,0:T(8,128)(2,1)S(1)}, u32[]{:S(2)}, u32[]{:S(2)}) async-start(bf16[4,64,704]{2,1,0:T(8,128)(2,1)} %bitcast.18), calls=%async_computation.3 | async-start | bytes 786432 | tf_op jit(solution)/shard_map/all_to_all | solution.py:42
  (4 other events, 12.7 us)
Sparse Core Ops, SparseCore 0:
  17.3 62.8 all-gather.1
  112.5 38.4 reduce-scatter.1

commit v5 on v4

--- a/solution.py
+++ b/solution.py
@@ -58,11 +58,16 @@
     return out
 
 
-def summed_four(terms, axis, dim):
+def sent_four(terms, axis, dim):
     size = lax.axis_size(axis)
-    total = take(terms, axis, 0, dim).astype(jnp.float32)
-    arrived = [shifted(take(terms, axis, k, dim), axis, k) for k in (1, size - 1, 2)]
-    for other in arrived:
+    return [take(terms, axis, 0, dim)] + [
+        shifted(take(terms, axis, k, dim), axis, k) for k in (1, size - 1, 2)
+    ]
+
+
+def total_of(terms):
+    total = terms[0].astype(jnp.float32)
+    for other in terms[1:]:
         total = total + other.astype(jnp.float32)
     return total
 
@@ -100,7 +105,8 @@
     full_value = lax.all_gather(value_part, "z", axis=0, tiled=True)
     full_gate = gathered_four(gate_part[:, None], "x", 1).reshape(width, cols)
     whole_tokens = jnp.broadcast_to(token_blocks, (ny, nc, rows, width))
-    whole_tokens = put(whole_tokens, swapped(token_blocks, "c", 1), "c", 1, 1)
+    other_blocks = swapped(token_blocks, "c", 1)
+    whole_tokens = put(whole_tokens, other_blocks, "c", 1, 1)
     whole_tokens = whole_tokens.reshape(length, width)
 
     gate_pre, value_part = lax.optimization_barrier((gate_pre, value_part))
@@ -138,18 +144,22 @@
     gate_grad, value_grad, _, _ = lax.optimization_barrier(
         (gate_grad, value_grad, gate_terms, value_terms)
     )
-    gate_sums = summed_four(gate_terms.reshape(nz, nx, share, cols), "x", 1).astype(narrow)
-    gate_out = added_up(exchanged(gate_sums[:, 0], "z")) * scale
+    gate_blocks = sent_four(gate_terms.reshape(nz, nx, share, cols), "x", 1)
     value_sums = lax.psum_scatter(value_terms, "z", scatter_dimension=0, tiled=True)
-    value_out = added_up(exchanged(value_sums.reshape(nx, share, cols), "x")) * scale
 
     part = contract_cols(value_grad, full_value)
     part = (part + contract_cols(gate_grad, full_gate)).astype(narrow)
     part = part.reshape(ny, nc, rows, width)
-    pair = take(part, "c", 0, 1).astype(jnp.float32) + swapped(
-        take(part, "c", 1, 1), "c", 1
-    ).astype(jnp.float32)
-    input_grad = summed_four(pair.astype(narrow)[:, 0], "y", 0)[0].astype(narrow)
+    partner = swapped(take(part, "c", 1, 1), "c", 1)
+    pair = total_of([take(part, "c", 0, 1), partner]).astype(narrow)
+    input_blocks = sent_four(pair[:, 0], "y", 0)
+    input_grad = total_of(input_blocks)[0].astype(narrow)
+
+    gate_blocks, _ = lax.optimization_barrier((gate_blocks, pair))
+    gate_sums = total_of(gate_blocks).astype(narrow)
+    gate_sums = exchanged(gate_sums[:, 0], "z")
+    gate_out = added_up(gate_sums) * scale
+    value_out = added_up(exchanged(value_sums.reshape(nx, share, cols), "x")) * scale
     return (input_grad, gate_out, value_out, conv_total[:3], conv_total[3])
 
 

time: 237 us -> 234 us (0.987)
  waiting for transfers between devices: 99.9 us -> 86.7 us
  starting transfers between devices: 42.4 us -> 52.9 us
  local copies, waits for them, and re-layouts: 27.8 us -> 30.6 us
    all_to_all x4, waiting for transfers between devices: 29.5 us -> 7.69 us  [exchanged(): return lax.all_to_all(blocks, axis, 0, 0, tiled=True)]
    all_to_all x4, starting transfers between devices: 20.4 us -> 32.2 us  [exchanged(): return lax.all_to_all(blocks, axis, 0, 0, tiled=True)]
    ppermute x15, waiting for transfers between devices: 70.4 us -> 79 us  [shifted(): lax.ppermute(block, axis, [(i, (i + by) % size) for i in range(size)])]
    dot_general x2, matrix products: 12 us -> 9 us  [contract_rows(): lax.dot_general(left, right, (((0,), (0,)), ((), ())), preferred_element_...]
    dynamic_update_slice x10, local copies, waits for them, and re-layouts: 4.61 us -> 7.44 us  [put(): return lax.dynamic_update_slice(out, block, at)]
where the time goes in v5:
time: 234 us; the launch traced here: 233 us
  waiting for transfers between devices  86.7 us (37%)
  starting transfers between devices  52.9 us (23%)
  local copies, waits for them, and re-layouts  30.6 us (13%)
  matrix products  24.6 us (11%)
  other arithmetic  24.1 us (10%)
  between operations  14.4 us (6%)
    ppermute x15, waiting for transfers between devices, shifted(): lax.ppermute(block, axis, [(i, (i + by) % size) for i in range(size)])  79 us
    all_to_all x4, starting transfers between devices, exchanged(): return lax.all_to_all(blocks, axis, 0, 0, tiled=True)  32.2 us
    ppermute x15, starting transfers between devices, shifted(): lax.ppermute(block, axis, [(i, (i + by) % size) for i in range(size)])  20.7 us
    dot_general x2, matrix products, contract_cols(): lax.dot_general(left, right, (((1,), (1,)), ((), ())), preferred_element_...  15.6 us
    dot_general x2, matrix products, contract_rows(): lax.dot_general(left, right, (((0,), (0,)), ((), ())), preferred_element_...  9 us
    all_to_all x4, waiting for transfers between devices, exchanged(): return lax.all_to_all(blocks, axis, 0, 0, tiled=True)  7.69 us
    dynamic_update_slice x10, local copies, waits for them, and re-layouts, put(): return lax.dynamic_update_slice(out, block, at)  7.44 us
    reduce_sum x1, other arithmetic, on_device(): jnp.sum(conv_grad * padded[:length], axis=0)  6.54 us
  transfers between devices with their start and end apart: 23, of which 9 were waited for; matrix products, arithmetic and copies ran while one was open for 32% of the time, Pallas kernels for 0%

profile of v5, /device:TPU:8, one launch (start us, length us, event | category | flops | bytes accessed | tf_op | source)
XLA Modules:
  0.0 233.4 jit_solution(10049465804627682175)
XLA Ops:
  8.8 3.0 %collective-permute-start.2 = (bf16[1,64,704]{2,1,0:T(8,128)(2,1)}, bf16[1,64,704]{2,1,0:T(8,128)(2,1)S(1)}, u32[]{:S(2)}, u32[]{:S(2)}) collective-permute-start(bf16[1,64,704]{2,1,0:T(8,128)(2,1)} %bitcast.48), channel_id=1, source_target_pairs={{0,16},{8,24},{16,0},{24,8},{1,17},{9,25},{17,1},{25,9},{2,18},{10... | collective-permute-start | bytes 270344 | tf_op jit(solution)/shard_map/ppermute | solution.py:14
  16.7 8.5 %all-to-all-start = ((bf16[8,64,704]{2,1,0:T(8,128)(2,1)}), bf16[8,64,704]{2,1,0:T(8,128)(2,1)}, u32[]{:S(2)}, u32[]{:S(2)}) async-start(bf16[8,64,704]{2,1,0:T(8,128)(2,1)} %broadcast_in_dim.60), calls=%async_computation | async-start | bytes 1572864 | tf_op jit(solution)/shard_map/all_to_all | solution.py:42
  26.7 2.4 %collective-permute-start.4 = (bf16[1,128,2048]{2,1,0:T(8,128)(2,1)}, bf16[1,128,2048]{2,1,0:T(8,128)(2,1)}, u32[]{:S(2)}, u32[]{:S(2)}) collective-permute-start(bf16[1,128,2048]{2,1,0:T(8,128)(2,1)} %bitcast.47), channel_id=1, source_target_pairs={{0,6},{2,0},{4,2},{6,4},{1,7},{3,1},{5,3},{7,5},{8,14},{10,8},{12,... | collective-permute-start | bytes 1572872 | tf_op jit(solution)/shard_map/ppermute | solution.py:14
  35.6 3.8 %collective-permute-done.4 = bf16[1,128,2048]{2,1,0:T(8,128)(2,1)} collective-permute-done((bf16[1,128,2048]{2,1,0:T(8,128)(2,1)}, bf16[1,128,2048]{2,1,0:T(8,128)(2,1)}, u32[]{:S(2)}, u32[]{:S(2)}) %collective-permute-start.4) | collective-permute-done | bytes 524320 | tf_op jit(solution)/shard_map/ppermute | solution.py:14
  39.5 1.9 bitcast_dynamic-update-slice_fusion.1
  42.3 6.5 %multiply_reduce_fusion.2 = (f32[704]{0:T(1024)S(1)}, f32[704]{0:T(1024)S(1)}, f32[704]{0:T(1024)S(1)}, f32[704]{0:T(1024)S(1)}, f32[1024,704]{0,1:T(8,128)}, /*index=5*/f32[1024,704]{0,1:T(8,128)S(1)}) fusion(f32[1024,704]{0,1:T(8,128)S(1)} %convert_element_type.116, bf16[1024,704]{0,1:T(8,128)(2,1)S(1)} %copy-done.1, bf16[1024,704]{0,1:T(8,128)(2,1)S(1)} %copy-done.7, ...), kind=kLoop, calls=%fused_computation.26 | loop fusion | flops 25949440 | bytes 12998656 | tf_op jit(solution)/shard_map/reduce_sum | solution.py:133
  48.8 2.4 %collective-permute-start.8 = (bf16[8,1,64,704]{3,2,1,0:T(8,128)(2,1)}, bf16[8,1,64,704]{3,2,1,0:T(8,128)(2,1)S(1)}, u32[]{:S(2)}, u32[]{:S(2)}) collective-permute-start(bf16[8,1,64,704]{3,2,1,0:T(8,128)(2,1)} %bitcast.8), channel_id=1, source_target_pairs={{0,24},{8,0},{16,8},{24,16},{1,25},{9,1},{17,9},{25,17},{2,26},{10... | collective-permute-start | bytes 2162696 | tf_op jit(solution)/shard_map/ppermute | solution.py:14
  51.2 6.2 %fusion.3 = bf16[1024,704]{0,1:T(8,128)(2,1)S(1)} fusion(f32[1024,704]{0,1:T(8,128)} %get-tuple-element.26, f32[704]{0:T(1024)S(1)} %get-tuple-element.24, f32[704]{0:T(1024)S(1)} %get-tuple-element.25, f32[704]{0:T(1024)S(1)} %get-tuple-element.23), kind=kLoop, calls=%fused_computation.15 | loop fusion | flops 4325376 | bytes 4333824 | tf_op jit(solution)/shard_map/convert_element_type | solution.py:130
  60.3 28.8 %collective-permute-done.7 = bf16[8,1,64,704]{3,2,1,0:T(8,128)(2,1)S(1)} collective-permute-done((bf16[8,1,64,704]{3,2,1,0:T(8,128)(2,1)}, bf16[8,1,64,704]{3,2,1,0:T(8,128)(2,1)S(1)}, u32[]{:S(2)}, u32[]{:S(2)}) %collective-permute-start.7) | collective-permute-done | bytes 720928 | tf_op jit(solution)/shard_map/ppermute | solution.py:14
  90.8 2.1 broadcast_in_dim.59
  94.8 4.5 %convolution_convert_fusion.1 = bf16[2048,704]{0,1:T(8,128)(2,1)} fusion(bf16[1024,704]{0,1:T(8,128)(2,1)S(1)} %fusion.3, bf16[1024,2048]{1,0:T(8,128)(2,1)S(1)} %bitcast.41), kind=kOutput, calls=%fused_computation.7 | convolution fusion | flops 2954231808 | bytes 8519680 | tf_op jit(solution)/shard_map/dot_general | solution.py:80
  99.3 4.5 %convolution_convert_fusion = bf16[2048,704]{0,1:T(8,128)(2,1)} fusion(bf16[1024,704]{0,1:T(8,128)(2,1)S(1)} %fusion.5, bf16[1024,2048]{1,0:T(8,128)(2,1)S(1)} %bitcast.42), kind=kOutput, calls=%fused_computation.6 | convolution fusion | flops 2954231808 | bytes 8519680 | tf_op jit(solution)/shard_map/dot_general | solution.py:80
  103.8 7.1 %fusion.18 = f32[1024,2048]{1,0:T(8,128)} fusion(bf16[1024,704]{0,1:T(8,128)(2,1)} %copy-done.8, bf16[2048,704]{1,0:T(8,128)(2,1)S(1)} %bitcast.43), kind=kOutput, calls=%fused_computation.63 | convolution fusion | flops 2952790016 | bytes 12713984 | tf_op jit(solution)/shard_map/dot_general | solution.py:86
  110.9 8.5 %add_convert_fusion = bf16[1024,2048]{1,0:T(8,128)(2,1)S(1)} fusion(f32[1024,2048]{1,0:T(8,128)} %fusion.18, bf16[1024,704]{0,1:T(8,128)(2,1)} %copy-done.9, bf16[2048,704]{1,0:T(8,128)(2,1)} %all-gather.2.cloned.1.call-done), kind=kOutput, calls=%fused_computation | convolution fusion | flops 2956984320 | bytes 16908288 | tf_op jit(solution)/shard_map/dot_general | solution.py:86
  119.5 1.9 copy-done.4
  123.0 3.1 %copy.17 = bf16[2048,704]{1,0:T(8,128)(2,1)S(1)} copy(bf16[2048,704]{0,1:T(8,128)(2,1)} %convolution_convert_fusion.1) | data formatting | bytes 5767168 | tf_op jit(solution)/shard_map/convert_element_type | solution.py:142
  127.9 2.0 collective-permute-start.14
  130.8 11.9 %all-to-all-start.3 = ((f32[32,4,704]{2,1,0:T(4,128)}), f32[32,4,704]{2,1,0:T(4,128)S(1)}, u32[]{:S(2)}, u32[]{:S(2)}) async-start(f32[32,4,704]{2,1,0:T(4,128)} %broadcast_in_dim.63), calls=%async_computation.4 | async-start | bytes 786432 | tf_op jit(solution)/shard_map/all_to_all | solution.py:42
  142.7 3.1 %add_convert_fusion.1 = bf16[4,1,128,2048]{3,2,1,0:T(8,128)(2,1)S(1)} fusion(bf16[4,1,128,2048]{3,2,1,0:T(8,128)(2,1)} %collective-permute-done.10, bf16[4,2,128,2048]{3,2,1,0:T(8,128)(2,1)} %bitcast.40, u32[]{:T(128)S(6)} %and.50), kind=kLoop, calls=%fused_computation.1 | loop fusion | flops 4194304 | bytes 6291460 | tf_op jit(solution)/shard_map/convert_element_type | solution.py:154
  145.8 5.2 %collective-permute-done.16 = bf16[8,1,64,704]{3,2,1,0:T(8,128)(2,1)S(1)} collective-permute-done((bf16[8,1,64,704]{3,2,1,0:T(8,128)(2,1)}, bf16[8,1,64,704]{3,2,1,0:T(8,128)(2,1)S(1)}, u32[]{:S(2)}, u32[]{:S(2)}) %collective-permute-start.16) | collective-permute-done | bytes 720928 | tf_op jit(solution)/shard_map/ppermute | solution.py:14
  151.0 16.3 %collective-permute-done.15 = bf16[8,1,64,704]{3,2,1,0:T(8,128)(2,1)} collective-permute-done((bf16[8,1,64,704]{3,2,1,0:T(8,128)(2,1)}, bf16[8,1,64,704]{3,2,1,0:T(8,128)(2,1)}, u32[]{:S(2)}, u32[]{:S(2)}) %collective-permute-start.15) | collective-permute-done | bytes 720928 | tf_op jit(solution)/shard_map/ppermute | solution.py:14
  167.2 3.2 %collective-permute-done.14 = bf16[8,1,64,704]{3,2,1,0:T(8,128)(2,1)} collective-permute-done((bf16[8,1,64,704]{3,2,1,0:T(8,128)(2,1)}, bf16[8,1,64,704]{3,2,1,0:T(8,128)(2,1)}, u32[]{:S(2)}, u32[]{:S(2)}) %collective-permute-start.14) | collective-permute-done | bytes 720928 | tf_op jit(solution)/shard_map/ppermute | solution.py:14
  170.4 2.7 %fusion.15 = bf16[8,64,704]{2,1,0:T(8,128)(2,1)} fusion(bf16[8,1,64,704]{3,2,1,0:T(8,128)(2,1)S(1)} %collective-permute-done.16, bf16[8,1,64,704]{3,2,1,0:T(8,128)(2,1)} %collective-permute-done.15, bf16[8,1,64,704]{3,2,1,0:T(8,128)(2,1)} %collective-permute-done.14, bf16[8,1,64,704]{3,2,1,0:T(8,128)(2,1)S(1)} %copy-done.5), kind=kLoop, calls=%fused_computation.34 | loop fusion | flops 2883584 | bytes 3604480 | tf_op jit(solution)/shard_map/squeeze | solution.py:160
  173.1 8.4 %all-to-all-start.1 = ((bf16[8,64,704]{2,1,0:T(8,128)(2,1)}), bf16[8,64,704]{2,1,0:T(8,128)(2,1)S(1)}, u32[]{:S(2)}, u32[]{:S(2)}) async-start(bf16[8,64,704]{2,1,0:T(8,128)(2,1)} %fusion.15), calls=%async_computation.1 | async-start | bytes 1572864 | tf_op jit(solution)/shard_map/all_to_all | solution.py:42
  185.0 2.0 collective-permute-start.12
  187.8 10.0 %collective-permute-done.11 = bf16[1,128,2048]{2,1,0:T(8,128)(2,1)} collective-permute-done((bf16[1,128,2048]{2,1,0:T(8,128)(2,1)}, bf16[1,128,2048]{2,1,0:T(8,128)(2,1)}, u32[]{:S(2)}, u32[]{:S(2)}) %collective-permute-start.11) | collective-permute-done | bytes 524320 | tf_op jit(solution)/shard_map/ppermute | solution.py:14
  197.7 2.2 collective-permute-done.13
  199.9 9.6 %collective-permute-done.12 = bf16[1,128,2048]{2,1,0:T(8,128)(2,1)} collective-permute-done((bf16[1,128,2048]{2,1,0:T(8,128)(2,1)}, bf16[1,128,2048]{2,1,0:T(8,128)(2,1)}, u32[]{:S(2)}, u32[]{:S(2)}) %collective-permute-start.12) | collective-permute-done | bytes 524320 | tf_op jit(solution)/shard_map/ppermute | solution.py:14
  209.5 2.5 %fusion.16 = bf16[128,2048]{1,0:T(8,128)(2,1)} fusion(bf16[1,128,2048]{2,1,0:T(8,128)(2,1)} %collective-permute-done.13, bf16[1,128,2048]{2,1,0:T(8,128)(2,1)} %collective-permute-done.12, bf16[1,128,2048]{2,1,0:T(8,128)(2,1)} %collective-permute-done.11, bf16[4,1,128,2048]{3,2,1,0:T(8,128)(2,1)S(1)} %add_convert_fusion.1, u32[]{:T(128)S(6)} %and.51), kind=kLoop, calls=%fused_computation.36 | loop fusion | flops 2097152 | bytes 2621444 | tf_op jit(solution)/shard_map/convert_element_type | solution.py:156
  212.0 1.9 copy.18
  213.9 3.5 %all-to-all-start.2 = ((bf16[4,64,704]{2,1,0:T(8,128)(2,1)}), bf16[4,64,704]{2,1,0:T(8,128)(2,1)S(1)}, u32[]{:S(2)}, u32[]{:S(2)}) async-start(bf16[4,64,704]{2,1,0:T(8,128)(2,1)} %bitcast.18), calls=%async_computation.3 | async-start | bytes 786432 | tf_op jit(solution)/shard_map/all_to_all | solution.py:42
  218.2 7.7 %all-to-all-done.2 = bf16[4,64,704]{2,1,0:T(8,128)(2,1)S(1)} async-done(((bf16[4,64,704]{2,1,0:T(8,128)(2,1)}), bf16[4,64,704]{2,1,0:T(8,128)(2,1)S(1)}, u32[]{:S(2)}, u32[]{:S(2)}) %all-to-all-start.2) | async-done | bytes 360480 | tf_op jit(solution)/shard_map/all_to_all | solution.py:42
  (89 shorter events, 31.8 us)
Async XLA Ops:
  7.2 25.6 %copy-start = (bf16[1024,704]{0,1:T(8,128)(2,1)S(1)}, bf16[1024,704]{0,1:T(8,128)(2,1)}, u32[]{:S(2)}) copy-start(bf16[1024,704]{0,1:T(8,128)(2,1)} %param.9) | copy-start | bytes 4325380
  7.2 26.0 %collective-permute-start.3 = (bf16[1,128,2048]{2,1,0:T(8,128)(2,1)}, bf16[1,128,2048]{2,1,0:T(8,128)(2,1)S(1)}, u32[]{:S(2)}, u32[]{:S(2)}) collective-permute-start(bf16[1,128,2048]{2,1,0:T(8,128)(2,1)} %bitcast.45), channel_id=1, source_target_pairs={{0,2},{2,4},{4,6},{6,0},{1,3},{3,5},{5,7},{7,1},{8,10},{10,12},{12... | collective-permute-start | bytes 1572872 | tf_op jit(solution)/shard_map/ppermute | solution.py:14
  8.8 23.0 %collective-permute-start.2 = (bf16[1,64,704]{2,1,0:T(8,128)(2,1)}, bf16[1,64,704]{2,1,0:T(8,128)(2,1)S(1)}, u32[]{:S(2)}, u32[]{:S(2)}) collective-permute-start(bf16[1,64,704]{2,1,0:T(8,128)(2,1)} %bitcast.48), channel_id=1, source_target_pairs={{0,16},{8,24},{16,0},{24,8},{1,17},{9,25},{17,1},{25,9},{2,18},{10... | collective-permute-start | bytes 270344 | tf_op jit(solution)/shard_map/ppermute | solution.py:14
  11.9 19.1 %collective-permute-start.1 = (bf16[1,64,704]{2,1,0:T(8,128)(2,1)}, bf16[1,64,704]{2,1,0:T(8,128)(2,1)}, u32[]{:S(2)}, u32[]{:S(2)}) collective-permute-start(bf16[1,64,704]{2,1,0:T(8,128)(2,1)} %bitcast.49), channel_id=1, source_target_pairs={{0,24},{8,0},{16,8},{24,16},{1,25},{9,1},{17,9},{25,17},{2,26},{10... | collective-permute-start | bytes 270344 | tf_op jit(solution)/shard_map/ppermute | solution.py:14
  13.0 13.1 %collective-permute-start = (bf16[1,64,704]{2,1,0:T(8,128)(2,1)}, bf16[1,64,704]{2,1,0:T(8,128)(2,1)S(1)}, u32[]{:S(2)}, u32[]{:S(2)}) collective-permute-start(bf16[1,64,704]{2,1,0:T(8,128)(2,1)} %bitcast.50), channel_id=1, source_target_pairs={{0,8},{8,16},{16,24},{24,0},{1,9},{9,17},{17,25},{25,1},{2,10},{10... | collective-permute-start | bytes 270344 | tf_op jit(solution)/shard_map/ppermute | solution.py:14
  13.9 27.5 %collective-permute-start.5 = (bf16[1,128,2048]{2,1,0:T(8,128)(2,1)}, bf16[1,128,2048]{2,1,0:T(8,128)(2,1)S(1)}, u32[]{:S(2)}, u32[]{:S(2)}) collective-permute-start(bf16[1,128,2048]{2,1,0:T(8,128)(2,1)} %bitcast.46), channel_id=1, source_target_pairs={{0,4},{2,6},{4,0},{6,2},{1,5},{3,7},{5,1},{7,3},{8,12},{10,14},{12... | collective-permute-start | bytes 1572872 | tf_op jit(solution)/shard_map/ppermute | solution.py:14
  16.7 32.1 %all-to-all-start = ((bf16[8,64,704]{2,1,0:T(8,128)(2,1)}), bf16[8,64,704]{2,1,0:T(8,128)(2,1)}, u32[]{:S(2)}, u32[]{:S(2)}) async-start(bf16[8,64,704]{2,1,0:T(8,128)(2,1)} %broadcast_in_dim.60), calls=%async_computation | async-start | bytes 1572864 | tf_op jit(solution)/shard_map/all_to_all | solution.py:42
  25.1 85.8 %all-gather.2.cloned.1.call-start = ((), (), s32[]{:S(2)}) async-start(), calls=%async_computation.5 | async-start | bytes 3538944 | tf_op jit(solution)/shard_map/all_gather | solution.py:105
  26.7 12.8 %collective-permute-start.4 = (bf16[1,128,2048]{2,1,0:T(8,128)(2,1)}, bf16[1,128,2048]{2,1,0:T(8,128)(2,1)}, u32[]{:S(2)}, u32[]{:S(2)}) collective-permute-start(bf16[1,128,2048]{2,1,0:T(8,128)(2,1)} %bitcast.47), channel_id=1, source_target_pairs={{0,6},{2,0},{4,2},{6,4},{1,7},{3,1},{5,3},{7,5},{8,14},{10,8},{12,... | collective-permute-start | bytes 1572872 | tf_op jit(solution)/shard_map/ppermute | solution.py:14
  32.7 179.3 %reduce-scatter.2.cloned.1.call-start = ((), (), s32[]{:S(2)}) async-start(), calls=%async_computation.6 | async-start | bytes 3244032 | tf_op jit(solution)/shard_map/reduce_scatter | solution.py:148
  33.1 9.1 %copy-start.1 = (bf16[1024,704]{0,1:T(8,128)(2,1)S(1)}, bf16[1024,704]{0,1:T(8,128)(2,1)}, u32[]{:S(2)}) copy-start(bf16[1024,704]{0,1:T(8,128)(2,1)} %param.9) | copy-start | bytes 4325380
  33.1 9.1 %copy-start.2 = (bf16[1024,704]{0,1:T(8,128)(2,1)S(1)}, bf16[1024,704]{0,1:T(8,128)(2,1)}, u32[]{:S(2)}) copy-start(bf16[1024,704]{0,1:T(8,128)(2,1)} %param.15) | copy-start | bytes 4325380
  33.1 9.1 %copy-start.7 = (bf16[1024,704]{0,1:T(8,128)(2,1)S(1)}, bf16[1024,704]{0,1:T(8,128)(2,1)}, u32[]{:S(2)}) copy-start(bf16[1024,704]{0,1:T(8,128)(2,1)} %param.10) | copy-start | bytes 4325380
  42.2 48.6 %collective-permute-start.6 = (bf16[4,1,128,2048]{3,2,1,0:T(8,128)(2,1)}, bf16[4,1,128,2048]{3,2,1,0:T(8,128)(2,1)}, u32[]{:S(2)}, u32[]{:S(2)}) collective-permute-start(bf16[4,1,128,2048]{3,2,1,0:T(8,128)(2,1)} %bitcast_dynamic-update-slice_fusion), channel_id=1, source_target_pairs={{0,1},{1,0},{2,3},{3,2},{4,5},{5,4},{6,7},{7,6},{8,9},{9,8},{10,11... | collective-permute-start | bytes 6291464 | tf_op jit(solution)/shard_map/ppermute | solution.py:19
  48.8 10.3 %copy-start.3 = (bf16[1024,704]{0,1:T(8,128)(2,1)S(1)}, bf16[1024,704]{0,1:T(8,128)(2,1)}, u32[]{:S(2)}) copy-start(bf16[1024,704]{0,1:T(8,128)(2,1)} %param.15) | copy-start | bytes 4325380
  48.8 41.9 %collective-permute-start.8 = (bf16[8,1,64,704]{3,2,1,0:T(8,128)(2,1)}, bf16[8,1,64,704]{3,2,1,0:T(8,128)(2,1)S(1)}, u32[]{:S(2)}, u32[]{:S(2)}) collective-permute-start(bf16[8,1,64,704]{3,2,1,0:T(8,128)(2,1)} %bitcast.8), channel_id=1, source_target_pairs={{0,24},{8,0},{16,8},{24,16},{1,25},{9,1},{17,9},{25,17},{2,26},{10... | collective-permute-start | bytes 2162696 | tf_op jit(solution)/shard_map/ppermute | solution.py:14
  51.2 37.9 %collective-permute-start.7 = (bf16[8,1,64,704]{3,2,1,0:T(8,128)(2,1)}, bf16[8,1,64,704]{3,2,1,0:T(8,128)(2,1)S(1)}, u32[]{:S(2)}, u32[]{:S(2)}) collective-permute-start(bf16[8,1,64,704]{3,2,1,0:T(8,128)(2,1)} %bitcast.8), channel_id=1, source_target_pairs={{0,8},{8,16},{16,24},{24,0},{1,9},{9,17},{17,25},{25,1},{2,10},{10... | collective-permute-start | bytes 2162696 | tf_op jit(solution)/shard_map/ppermute | solution.py:14
  57.3 37.5 %copy-start.8 = (bf16[1024,704]{0,1:T(8,128)(2,1)}, bf16[1024,704]{0,1:T(8,128)(2,1)S(1)}, u32[]{:S(2)}) copy-start(bf16[1024,704]{0,1:T(8,128)(2,1)S(1)} %fusion.3) | copy-start | bytes 4325380
  57.3 33.4 %collective-permute-start.9 = (bf16[8,1,64,704]{3,2,1,0:T(8,128)(2,1)}, bf16[8,1,64,704]{3,2,1,0:T(8,128)(2,1)S(1)}, u32[]{:S(2)}, u32[]{:S(2)}) collective-permute-start(bf16[8,1,64,704]{3,2,1,0:T(8,128)(2,1)} %bitcast.8), channel_id=1, source_target_pairs={{0,16},{8,24},{16,0},{24,8},{1,17},{9,25},{17,1},{25,9},{2,18},{10... | collective-permute-start | bytes 2162696 | tf_op jit(solution)/shard_map/ppermute | solution.py:14
  60.3 39.0 %copy-start.9 = (bf16[1024,704]{0,1:T(8,128)(2,1)}, bf16[1024,704]{0,1:T(8,128)(2,1)S(1)}, u32[]{:S(2)}) copy-start(bf16[1024,704]{0,1:T(8,128)(2,1)S(1)} %fusion.5) | copy-start | bytes 4325380
  123.0 19.7 %collective-permute-start.10 = (bf16[4,1,128,2048]{3,2,1,0:T(8,128)(2,1)}, bf16[4,1,128,2048]{3,2,1,0:T(8,128)(2,1)}, u32[]{:S(2)}, u32[]{:S(2)}) collective-permute-start(bf16[4,1,128,2048]{3,2,1,0:T(8,128)(2,1)} %constant_dynamic-slice_fusion.4), channel_id=1, source_target_pairs={{0,1},{1,0},{2,3},{3,2},{4,5},{5,4},{6,7},{7,6},{8,9},{9,8},{10,11... | collective-permute-start | bytes 6291464 | tf_op jit(solution)/shard_map/ppermute | solution.py:19
  127.9 23.1 %collective-permute-start.16 = (bf16[8,1,64,704]{3,2,1,0:T(8,128)(2,1)}, bf16[8,1,64,704]{3,2,1,0:T(8,128)(2,1)S(1)}, u32[]{:S(2)}, u32[]{:S(2)}) collective-permute-start(bf16[8,1,64,704]{3,2,1,0:T(8,128)(2,1)} %get-tuple-element.28), channel_id=1, source_target_pairs={{0,16},{8,24},{16,0},{24,8},{1,17},{9,25},{17,1},{25,9},{2,18},{10... | collective-permute-start | bytes 2162696 | tf_op jit(solution)/shard_map/ppermute | solution.py:14
  127.9 39.4 %collective-permute-start.15 = (bf16[8,1,64,704]{3,2,1,0:T(8,128)(2,1)}, bf16[8,1,64,704]{3,2,1,0:T(8,128)(2,1)}, u32[]{:S(2)}, u32[]{:S(2)}) collective-permute-start(bf16[8,1,64,704]{3,2,1,0:T(8,128)(2,1)} %get-tuple-element.29), channel_id=1, source_target_pairs={{0,24},{8,0},{16,8},{24,16},{1,25},{9,1},{17,9},{25,17},{2,26},{10... | collective-permute-start | bytes 2162696 | tf_op jit(solution)/shard_map/ppermute | solution.py:14
  127.9 42.5 %collective-permute-start.14 = (bf16[8,1,64,704]{3,2,1,0:T(8,128)(2,1)}, bf16[8,1,64,704]{3,2,1,0:T(8,128)(2,1)}, u32[]{:S(2)}, u32[]{:S(2)}) collective-permute-start(bf16[8,1,64,704]{3,2,1,0:T(8,128)(2,1)} %get-tuple-element.30), channel_id=1, source_target_pairs={{0,8},{8,16},{16,24},{24,0},{1,9},{9,17},{17,25},{25,1},{2,10},{10... | collective-permute-start | bytes 2162696 | tf_op jit(solution)/shard_map/ppermute | solution.py:14
  130.8 42.3 %all-to-all-start.3 = ((f32[32,4,704]{2,1,0:T(4,128)}), f32[32,4,704]{2,1,0:T(4,128)S(1)}, u32[]{:S(2)}, u32[]{:S(2)}) async-start(f32[32,4,704]{2,1,0:T(4,128)} %broadcast_in_dim.63), calls=%async_computation.4 | async-start | bytes 786432 | tf_op jit(solution)/shard_map/all_to_all | solution.py:42
  142.6 27.8 %copy-start.5 = (bf16[8,1,64,704]{3,2,1,0:T(8,128)(2,1)S(1)}, bf16[8,1,64,704]{3,2,1,0:T(8,128)(2,1)}, u32[]{:S(2)}) copy-start(bf16[8,1,64,704]{3,2,1,0:T(8,128)(2,1)} %get-tuple-element.15) | copy-start | bytes 2162692
  173.1 40.8 %all-to-all-start.1 = ((bf16[8,64,704]{2,1,0:T(8,128)(2,1)}), bf16[8,64,704]{2,1,0:T(8,128)(2,1)S(1)}, u32[]{:S(2)}, u32[]{:S(2)}) async-start(bf16[8,64,704]{2,1,0:T(8,128)(2,1)} %fusion.15), calls=%async_computation.1 | async-start | bytes 1572864 | tf_op jit(solution)/shard_map/all_to_all | solution.py:42
  182.6 15.1 %collective-permute-start.11 = (bf16[1,128,2048]{2,1,0:T(8,128)(2,1)}, bf16[1,128,2048]{2,1,0:T(8,128)(2,1)}, u32[]{:S(2)}, u32[]{:S(2)}) collective-permute-start(bf16[1,128,2048]{2,1,0:T(8,128)(2,1)} %get-tuple-element.32), channel_id=1, source_target_pairs={{0,2},{2,4},{4,6},{6,0},{1,3},{3,5},{5,7},{7,1},{8,10},{10,12},{12... | collective-permute-start | bytes 1572872 | tf_op jit(solution)/shard_map/ppermute | solution.py:14
  183.3 16.7 %collective-permute-start.13 = (bf16[1,128,2048]{2,1,0:T(8,128)(2,1)}, bf16[1,128,2048]{2,1,0:T(8,128)(2,1)}, u32[]{:S(2)}, u32[]{:S(2)}) collective-permute-start(bf16[1,128,2048]{2,1,0:T(8,128)(2,1)} %get-tuple-element.33), channel_id=1, source_target_pairs={{0,4},{2,6},{4,0},{6,2},{1,5},{3,7},{5,1},{7,3},{8,12},{10,14},{12... | collective-permute-start | bytes 1572872 | tf_op jit(solution)/shard_map/ppermute | solution.py:14
  185.0 24.4 %collective-permute-start.12 = (bf16[1,128,2048]{2,1,0:T(8,128)(2,1)}, bf16[1,128,2048]{2,1,0:T(8,128)(2,1)}, u32[]{:S(2)}, u32[]{:S(2)}) collective-permute-start(bf16[1,128,2048]{2,1,0:T(8,128)(2,1)} %get-tuple-element.34), channel_id=1, source_target_pairs={{0,6},{2,0},{4,2},{6,4},{1,7},{3,1},{5,3},{7,5},{8,14},{10,8},{12,... | collective-permute-start | bytes 1572872 | tf_op jit(solution)/shard_map/ppermute | solution.py:14
  187.1 38.8 %copy-start.12 = (f32[4,704]{1,0:T(4,128)}, f32[4,704]{1,0:T(4,128)S(1)}, u32[]{:S(2)}) copy-start(f32[4,704]{1,0:T(4,128)S(1)} %broadcast_multiply_fusion.2) | copy-start | bytes 33796
  213.9 12.0 %all-to-all-start.2 = ((bf16[4,64,704]{2,1,0:T(8,128)(2,1)}), bf16[4,64,704]{2,1,0:T(8,128)(2,1)S(1)}, u32[]{:S(2)}, u32[]{:S(2)}) async-start(bf16[4,64,704]{2,1,0:T(8,128)(2,1)} %bitcast.18), calls=%async_computation.3 | async-start | bytes 786432 | tf_op jit(solution)/shard_map/all_to_all | solution.py:42
  (5 other events, 19.6 us)
Sparse Core Ops, SparseCore 0:
  32.8 44.2 all-gather.1
  104.0 48.9 reduce-scatter.1

commit v6 on v5

--- a/solution.py
+++ b/solution.py
@@ -1,6 +1,9 @@
 import jax
 import jax.numpy as jnp
 from jax import lax
+from jax.experimental import pallas as pl
+from jax.experimental.layout import Layout, with_layout_constraint
+from jax.experimental.pallas import tpu as pltpu
 from jax.sharding import Mesh
 from jax.sharding import PartitionSpec as P
 
@@ -82,10 +85,49 @@
     )
 
 
-def contract_cols(left, right):
-    return lax.dot_general(
-        left, right, (((1,), (1,)), ((), ())), preferred_element_type=jnp.float32
-    )
+def back_kernel(place, gate_t, value_t, value_w, own, *rest):
+    others, out, gate_w = rest[:-2], rest[-2], rest[-1]
+    groups, share, _ = own.shape
+    size = len(others) + 1
+    for k, piece in enumerate((own, *others)):
+        for group in range(groups):
+            start = pl.multiple_of(group * size * share + place[k] * share, share)
+            gate_w[pl.ds(start, share), :] = piece[group]
+    total = jnp.dot(gate_w[...], gate_t[...], preferred_element_type=jnp.float32)
+    total += jnp.dot(value_w[...], value_t[...], preferred_element_type=jnp.float32)
+    peers, _, lanes = out.shape
+    for peer in range(peers):
+        out[peer] = total[:, peer * lanes : (peer + 1) * lanes].astype(out.dtype)
+
+
+def back_parts(place, gate_t, value_t, value_w, pieces, peers, steps):
+    cols, length = gate_t.shape
+    width = value_w.shape[0]
+    groups, share, _ = pieces[0].shape
+    tall = width // steps
+    whole = pl.BlockSpec((cols, length), lambda i: (0, 0))
+    return pl.pallas_call(
+        back_kernel,
+        grid=(steps,),
+        in_specs=[
+            pl.BlockSpec(memory_space=pltpu.SMEM),
+            whole,
+            whole,
+            pl.BlockSpec((tall, cols), lambda i: (i, 0)),
+        ]
+        + [pl.BlockSpec((groups // steps, share, cols), lambda i: (i, 0, 0))] * len(pieces),
+        out_specs=pl.BlockSpec((peers, tall, length // peers), lambda i: (0, i, 0)),
+        out_shape=jax.ShapeDtypeStruct((peers, width, length // peers), value_w.dtype),
+        scratch_shapes=[pltpu.VMEM((tall, cols), value_w.dtype)],
+        compiler_params=pltpu.CompilerParams(
+            dimension_semantics=("arbitrary",), vmem_limit_bytes=40 * 2**20
+        ),
+        cost_estimate=pl.CostEstimate(
+            flops=4 * width * cols * length,
+            bytes_accessed=4 * (cols * length + width * cols) + 2 * width * length,
+            transcendentals=0,
+        ),
+    )(place, gate_t, value_t, value_w, *pieces)
 
 
 def on_device(
@@ -103,7 +145,11 @@
     gate_part = copies_of_all(up_gate_w, "z")
     value_part = gathered_four(up_value_w[None], "x", 0).reshape(nx * share, cols)
     full_value = lax.all_gather(value_part, "z", axis=0, tiled=True)
-    full_gate = gathered_four(gate_part[:, None], "x", 1).reshape(width, cols)
+    steps = (1, nx - 1, 2)
+    gate_pieces = [gate_part] + [shifted(gate_part, "x", k) for k in steps]
+    gate_places = jnp.stack(
+        [(lax.axis_index("x") + nx - k) & (nx - 1) for k in (0, *steps)]
+    ).astype(jnp.int32)
     whole_tokens = jnp.broadcast_to(token_blocks, (ny, nc, rows, width))
     other_blocks = swapped(token_blocks, "c", 1)
     whole_tokens = put(whole_tokens, other_blocks, "c", 1, 1)
@@ -147,19 +193,22 @@
     gate_blocks = sent_four(gate_terms.reshape(nz, nx, share, cols), "x", 1)
     value_sums = lax.psum_scatter(value_terms, "z", scatter_dimension=0, tiled=True)
 
-    part = contract_cols(value_grad, full_value)
-    part = (part + contract_cols(gate_grad, full_gate)).astype(narrow)
-    part = part.reshape(ny, nc, rows, width)
+    part = back_parts(
+        gate_places, gate_grad.T, value_grad.T, full_value, gate_pieces, ny * nc, 4
+    )
+    part = part.reshape(ny, nc, width, rows)
     partner = swapped(take(part, "c", 1, 1), "c", 1)
     pair = total_of([take(part, "c", 0, 1), partner]).astype(narrow)
     input_blocks = sent_four(pair[:, 0], "y", 0)
     input_grad = total_of(input_blocks)[0].astype(narrow)
+    input_grad = with_layout_constraint(input_grad, Layout((0, 1))).T
 
     gate_blocks, _ = lax.optimization_barrier((gate_blocks, pair))
     gate_sums = total_of(gate_blocks).astype(narrow)
     gate_sums = exchanged(gate_sums[:, 0], "z")
     gate_out = added_up(gate_sums) * scale
-    value_out = added_up(exchanged(value_sums.reshape(nx, share, cols), "x")) * scale
+    value_blocks = sent_four(value_sums.reshape(nx, share, cols), "x", 0)
+    value_out = total_of(value_blocks)[0] * scale
     return (input_grad, gate_out, value_out, conv_total[:3], conv_total[3])
 
 

time: 234 us -> 231 us (0.987)
  matrix products: 24.6 us -> 11.3 us
  Pallas kernels: 0 us -> 8.43 us
  starting transfers between devices: 52.9 us -> 45.1 us
  local copies, waits for them, and re-layouts: 30.6 us -> 35.8 us
  waiting for transfers between devices: 86.7 us -> 90.3 us
    dot_general x2 -> x0, matrix products: 15.6 us -> none  [contract_cols(): lax.dot_general(left, right, (((1,), (1,)), ((), ())), preferred_element_...]
    all_to_all x4 -> x3, starting transfers between devices: 32.2 us -> 18 us  [exchanged(): return lax.all_to_all(blocks, axis, 0, 0, tiled=True)]
    unnamed x28 -> x43, local copies, waits for them, and re-layouts: 3.37 us -> 15 us
    pallas_call x0 -> x1, Pallas kernels: none -> 8.43 us  [back_parts(): pl.pallas_call(back_kernel, grid=(steps,), in_specs=[pl.BlockSpec(memory_...]
    ppermute x15 -> x18, starting transfers between devices: 20.7 us -> 26.9 us  [shifted(): lax.ppermute(block, axis, [(i, (i + by) % size) for i in range(size)])]
    ppermute x15 -> x18, waiting for transfers between devices: 79 us -> 83.9 us  [shifted(): lax.ppermute(block, axis, [(i, (i + by) % size) for i in range(size)])]
    convert_element_type x1 -> x0, other arithmetic: 2.48 us -> none  [on_device(): input_grad = total_of(input_blocks)[0].astype(narrow)]
    dynamic_update_slice x10 -> x7, local copies, waits for them, and re-layouts: 7.44 us -> 5.23 us  [put(): return lax.dynamic_update_slice(out, block, at)]
  transfers between devices with their start and end apart: 23 -> 25, of which waited for: 9 -> 14; matrix products, arithmetic and copies ran while one was open for 32% -> 25% of each run, Pallas kernels for 0% -> 4%
where the time goes in v6:
time: 231 us; the launch traced here: 230 us
  waiting for transfers between devices  90.3 us (39%)
  starting transfers between devices  45.1 us (20%)
  local copies, waits for them, and re-layouts  35.8 us (15%)
  other arithmetic  25.1 us (11%)
  between operations  14.4 us (6%)
  matrix products  11.3 us (5%)
  Pallas kernels  8.43 us (4%)
    ppermute x18, waiting for transfers between devices, shifted(): lax.ppermute(block, axis, [(i, (i + by) % size) for i in range(size)])  83.9 us
    ppermute x18, starting transfers between devices, shifted(): lax.ppermute(block, axis, [(i, (i + by) % size) for i in range(size)])  26.9 us
    all_to_all x3, starting transfers between devices, exchanged(): return lax.all_to_all(blocks, axis, 0, 0, tiled=True)  18 us
    unnamed x43, local copies, waits for them, and re-layouts  15 us
    dot_general x2, matrix products, contract_rows(): lax.dot_general(left, right, (((0,), (0,)), ((), ())), preferred_element_...  11.3 us
    pallas_call x1, Pallas kernels, back_parts(): pl.pallas_call(back_kernel, grid=(steps,), in_specs=[pl.BlockSpec(memory_...  8.43 us
    reduce_sum x1, other arithmetic, on_device(): jnp.sum(conv_grad * padded[:length], axis=0)  7.79 us
    all_to_all x3, waiting for transfers between devices, exchanged(): return lax.all_to_all(blocks, axis, 0, 0, tiled=True)  6.36 us
  transfers between devices with their start and end apart: 25, of which 14 were waited for; matrix products, arithmetic and copies ran while one was open for 25% of the time, Pallas kernels for 4%

profile of v6, /device:TPU:8, one launch (start us, length us, event | category | flops | bytes accessed | tf_op | source)
XLA Modules:
  0.0 230.4 jit_solution(17620533599731861333)
XLA Ops:
  10.5 1.8 collective-permute-start.2
  17.7 2.2 collective-permute-start.4
  20.8 6.6 %collective-permute-done.3 = bf16[1,128,2048]{2,1,0:T(8,128)(2,1)S(1)} collective-permute-done((bf16[1,128,2048]{2,1,0:T(8,128)(2,1)}, bf16[1,128,2048]{2,1,0:T(8,128)(2,1)S(1)}, u32[]{:S(2)}, u32[]{:S(2)}) %collective-permute-start.3) | collective-permute-done | bytes 524320 | tf_op jit(solution)/shard_map/ppermute | solution.py:17
  30.7 1.9 collective-permute-done.4
  33.6 8.8 %collective-permute-done.5 = bf16[1,128,2048]{2,1,0:T(8,128)(2,1)} collective-permute-done((bf16[1,128,2048]{2,1,0:T(8,128)(2,1)}, bf16[1,128,2048]{2,1,0:T(8,128)(2,1)}, u32[]{:S(2)}, u32[]{:S(2)}) %collective-permute-start.5) | collective-permute-done | bytes 524320 | tf_op jit(solution)/shard_map/ppermute | solution.py:17
  44.6 8.5 %all-to-all-start = ((bf16[8,64,704]{2,1,0:T(8,128)(2,1)}), bf16[8,64,704]{2,1,0:T(8,128)(2,1)}, u32[]{:S(2)}, u32[]{:S(2)}) async-start(bf16[8,64,704]{2,1,0:T(8,128)(2,1)} %broadcast_in_dim.52), calls=%async_computation | async-start | bytes 1572864 | tf_op jit(solution)/shard_map/all_to_all | solution.py:45
  55.0 7.8 %multiply_reduce_fusion.2 = (f32[704]{0:T(1024)}, f32[704]{0:T(1024)}, f32[704]{0:T(1024)}, f32[704]{0:T(1024)S(1)}, f32[1024,704]{0,1:T(8,128)}, /*index=5*/f32[1024,704]{0,1:T(8,128)S(1)}) fusion(f32[1024,704]{0,1:T(8,128)S(1)} %convert_element_type.123, bf16[1024,704]{0,1:T(8,128)(2,1)S(1)} %copy-done.8, bf16[1024,704]{0,1:T(8,128)(2,1)S(1)} %copy-done.14, ...), kind=kLoop, calls=%fused_computation.25 | loop fusion | flops 25949440 | bytes 12998656 | tf_op jit(solution)/shard_map/reduce_sum | solution.py:179
  64.4 1.9 constant_dynamic-update-slice_fusion
  66.3 1.9 copy-done.10
  68.2 4.6 %convolution_convert_fusion = bf16[2048,704]{0,1:T(8,128)(2,1)} fusion(bf16[1024,704]{0,1:T(8,128)(2,1)S(1)} %fusion.5, bf16[1024,2048]{1,0:T(8,128)(2,1)S(1)} %bitcast.48), kind=kOutput, calls=%fused_computation.5 | convolution fusion | flops 2954231808 | bytes 8519680 | tf_op jit(solution)/shard_map/dot_general | solution.py:83
  72.9 6.1 %fusion.3 = bf16[1024,704]{0,1:T(8,128)(2,1)S(1)} fusion(f32[1024,704]{0,1:T(8,128)} %get-tuple-element.46, f32[704]{0:T(1024)S(1)} %get-tuple-element.44, f32[704]{0:T(1024)S(1)} %get-tuple-element.45, f32[704]{0:T(1024)S(1)} %get-tuple-element.43), kind=kLoop, calls=%fused_computation.14 | loop fusion | flops 4325376 | bytes 4333824 | tf_op jit(solution)/shard_map/convert_element_type | solution.py:176
  79.0 4.2 %all-to-all-done.own = bf16[8,64,704]{2,1,0:T(8,128)(2,1)} async-done(((bf16[8,64,704]{2,1,0:T(8,128)(2,1)}), bf16[8,64,704]{2,1,0:T(8,128)(2,1)}, u32[]{:S(2)}, u32[]{:S(2)}) %all-to-all-start) | async-done | bytes 720928 | tf_op jit(solution)/shard_map/all_to_all | solution.py:45
  84.7 1.8 collective-permute-start.8
  88.2 6.7 %convolution_convert_fusion.1 = bf16[2048,704]{0,1:T(8,128)(2,1)} fusion(bf16[1024,704]{0,1:T(8,128)(2,1)S(1)} %fusion.3, bf16[1024,2048]{1,0:T(8,128)(2,1)} %bitcast.49), kind=kOutput, calls=%fused_computation.6 | convolution fusion | flops 2954231808 | bytes 8519680 | tf_op jit(solution)/shard_map/dot_general | solution.py:83
  94.9 9.2 %collective-permute-done.7.rest_0_ = bf16[8,64,704]{2,1,0:T(8,128)(2,1)S(1)} collective-permute-done((bf16[8,64,704]{2,1,0:T(8,128)(2,1)}, bf16[8,64,704]{2,1,0:T(8,128)(2,1)S(1)}, u32[]{:S(2)}, u32[]{:S(2)}) %collective-permute-start.7) | collective-permute-done | bytes 720928 | tf_op jit(solution)/shard_map/ppermute | solution.py:17
  105.1 15.3 %collective-permute-done.8.rest_1_ = bf16[8,64,704]{2,1,0:T(8,128)(2,1)S(1)} collective-permute-done((bf16[8,64,704]{2,1,0:T(8,128)(2,1)}, bf16[8,64,704]{2,1,0:T(8,128)(2,1)S(1)}, u32[]{:S(2)}, u32[]{:S(2)}) %collective-permute-start.8) | collective-permute-done | bytes 720928 | tf_op jit(solution)/shard_map/ppermute | solution.py:17
  122.7 1.9 copy-done.1
  128.0 8.4 %shard_map.119 = bf16[8,2048,128]{2,1,0:T(8,128)(2,1)S(1)} custom-call(s32[4]{0:T(128)S(1)} %pad_add_fusion.place, bf16[704,1024]{1,0:T(8,128)(2,1)S(1)} %bitcast.44, bf16[704,1024]{1,0:T(8,128)(2,1)S(1)} %bitcast.45, bf16[2048,704]{1,0:T(8,128)(2,1)S(1)} %copy-done.1, bf16[8,64,704]{2,1,0:T(8,128)(2,1)} %all-to-all-done.own, ...), custom_call_target="tpu_custom_call" | custom-call | flops 5905580032 | bytes 12845056 | tf_op jit(solution)/shard_map/pallas_call | solution.py:109
  136.5 1.9 copy-done
  139.9 3.1 %copy.24 = bf16[2048,704]{1,0:T(8,128)(2,1)S(1)} copy(bf16[2048,704]{0,1:T(8,128)(2,1)} %convolution_convert_fusion.1) | data formatting | bytes 5767168 | tf_op jit(solution)/shard_map/convert_element_type | solution.py:188
  146.0 2.1 collective-permute-start.15
  150.2 5.0 %all-to-all-start.2 = ((f32[32,4,704]{2,1,0:T(4,128)}), f32[32,4,704]{2,1,0:T(4,128)S(1)}, u32[]{:S(2)}, u32[]{:S(2)}) async-start(f32[32,4,704]{2,1,0:T(4,128)} %broadcast_in_dim.53), calls=%async_computation.3 | async-start | bytes 786432 | tf_op jit(solution)/shard_map/all_to_all | solution.py:45
  155.3 2.8 %add_convert_fusion = bf16[4,1,2048,128]{3,2,1,0:T(8,128)(2,1)S(1)} fusion(bf16[4,1,2048,128]{3,2,1,0:T(8,128)(2,1)} %collective-permute-done.10, bf16[4,2,2048,128]{3,2,1,0:T(8,128)(2,1)} %bitcast.43, u32[]{:T(128)S(6)} %and.67), kind=kLoop, calls=%fused_computation | loop fusion | flops 4194304 | bytes 6291460 | tf_op jit(solution)/shard_map/convert_element_type | solution.py:201
  158.0 11.9 %collective-permute-done.14 = bf16[8,1,64,704]{3,2,1,0:T(8,128)(2,1)S(1)} collective-permute-done((bf16[8,1,64,704]{3,2,1,0:T(8,128)(2,1)}, bf16[8,1,64,704]{3,2,1,0:T(8,128)(2,1)S(1)}, u32[]{:S(2)}, u32[]{:S(2)}) %collective-permute-start.14) | collective-permute-done | bytes 720928 | tf_op jit(solution)/shard_map/ppermute | solution.py:17
  169.9 16.7 %collective-permute-done.15 = bf16[8,1,64,704]{3,2,1,0:T(8,128)(2,1)} collective-permute-done((bf16[8,1,64,704]{3,2,1,0:T(8,128)(2,1)}, bf16[8,1,64,704]{3,2,1,0:T(8,128)(2,1)}, u32[]{:S(2)}, u32[]{:S(2)}) %collective-permute-start.15) | collective-permute-done | bytes 720928 | tf_op jit(solution)/shard_map/ppermute | solution.py:17
  191.5 2.2 collective-permute-start.13
  193.7 2.7 %fusion.15 = bf16[8,64,704]{2,1,0:T(8,128)(2,1)} fusion(bf16[8,1,64,704]{3,2,1,0:T(8,128)(2,1)} %collective-permute-done.16, bf16[8,1,64,704]{3,2,1,0:T(8,128)(2,1)} %collective-permute-done.15, bf16[8,1,64,704]{3,2,1,0:T(8,128)(2,1)S(1)} %collective-permute-done.14, bf16[8,1,64,704]{3,2,1,0:T(8,128)(2,1)S(1)} %copy-done.11), kind=kLoop, calls=%fused_computation.33 | loop fusion | flops 2883584 | bytes 3604480 | tf_op jit(solution)/shard_map/squeeze | solution.py:208
  196.4 4.5 %all-to-all-start.1 = ((bf16[8,64,704]{2,1,0:T(8,128)(2,1)}), bf16[8,64,704]{2,1,0:T(8,128)(2,1)S(1)}, u32[]{:S(2)}, u32[]{:S(2)}) async-start(bf16[8,64,704]{2,1,0:T(8,128)(2,1)} %fusion.15), calls=%async_computation.1 | async-start | bytes 1572864 | tf_op jit(solution)/shard_map/all_to_all | solution.py:45
  204.7 2.1 collective-permute-start.18
  206.9 9.2 %collective-permute-done.13 = bf16[1,2048,128]{2,1,0:T(8,128)(2,1)} collective-permute-done((bf16[1,2048,128]{2,1,0:T(8,128)(2,1)}, bf16[1,2048,128]{2,1,0:T(8,128)(2,1)}, u32[]{:S(2)}, u32[]{:S(2)}) %collective-permute-start.13) | collective-permute-done | bytes 524320 | tf_op jit(solution)/shard_map/ppermute | solution.py:17
  218.8 1.8 multiply_bitcast_fusion
  220.6 2.1 all-to-all-done.1
  (104 shorter events, 48.4 us)
Async XLA Ops:
  7.2 115.6 %all-gather.2.cloned.1.call-start = ((), (), s32[]{:S(2)}) async-start(), calls=%async_computation.4 | async-start | bytes 3538944 | tf_op jit(solution)/shard_map/all_gather | solution.py:147
  7.2 6.7 %collective-permute-start = (bf16[1,64,704]{2,1,0:T(8,128)(2,1)}, bf16[1,64,704]{2,1,0:T(8,128)(2,1)S(1)}, u32[]{:S(2)}, u32[]{:S(2)}) collective-permute-start(bf16[1,64,704]{2,1,0:T(8,128)(2,1)} %bitcast.56), channel_id=1, source_target_pairs={{0,8},{8,16},{16,24},{24,0},{1,9},{9,17},{17,25},{25,1},{2,10},{10... | collective-permute-start | bytes 270344 | tf_op jit(solution)/shard_map/ppermute | solution.py:17
  8.8 6.3 %collective-permute-start.1 = (bf16[1,64,704]{2,1,0:T(8,128)(2,1)}, bf16[1,64,704]{2,1,0:T(8,128)(2,1)S(1)}, u32[]{:S(2)}, u32[]{:S(2)}) collective-permute-start(bf16[1,64,704]{2,1,0:T(8,128)(2,1)} %bitcast.57), channel_id=1, source_target_pairs={{0,24},{8,0},{16,8},{24,16},{1,25},{9,1},{17,9},{25,17},{2,26},{10... | collective-permute-start | bytes 270344 | tf_op jit(solution)/shard_map/ppermute | solution.py:17
  10.5 6.3 %collective-permute-start.2 = (bf16[1,64,704]{2,1,0:T(8,128)(2,1)}, bf16[1,64,704]{2,1,0:T(8,128)(2,1)S(1)}, u32[]{:S(2)}, u32[]{:S(2)}) collective-permute-start(bf16[1,64,704]{2,1,0:T(8,128)(2,1)} %bitcast.58), channel_id=1, source_target_pairs={{0,16},{8,24},{16,0},{24,8},{1,17},{9,25},{17,1},{25,9},{2,18},{10... | collective-permute-start | bytes 270344 | tf_op jit(solution)/shard_map/ppermute | solution.py:17
  12.3 15.0 %collective-permute-start.3 = (bf16[1,128,2048]{2,1,0:T(8,128)(2,1)}, bf16[1,128,2048]{2,1,0:T(8,128)(2,1)S(1)}, u32[]{:S(2)}, u32[]{:S(2)}) collective-permute-start(bf16[1,128,2048]{2,1,0:T(8,128)(2,1)} %bitcast.53), channel_id=1, source_target_pairs={{0,2},{2,4},{4,6},{6,0},{1,3},{3,5},{5,7},{7,1},{8,10},{10,12},{12... | collective-permute-start | bytes 1572872 | tf_op jit(solution)/shard_map/ppermute | solution.py:17
  17.7 14.9 %collective-permute-start.4 = (bf16[1,128,2048]{2,1,0:T(8,128)(2,1)}, bf16[1,128,2048]{2,1,0:T(8,128)(2,1)}, u32[]{:S(2)}, u32[]{:S(2)}) collective-permute-start(bf16[1,128,2048]{2,1,0:T(8,128)(2,1)} %bitcast.54), channel_id=1, source_target_pairs={{0,6},{2,0},{4,2},{6,4},{1,7},{3,1},{5,3},{7,5},{8,14},{10,8},{12,... | collective-permute-start | bytes 1572872 | tf_op jit(solution)/shard_map/ppermute | solution.py:17
  19.9 22.6 %collective-permute-start.5 = (bf16[1,128,2048]{2,1,0:T(8,128)(2,1)}, bf16[1,128,2048]{2,1,0:T(8,128)(2,1)}, u32[]{:S(2)}, u32[]{:S(2)}) collective-permute-start(bf16[1,128,2048]{2,1,0:T(8,128)(2,1)} %bitcast.55), channel_id=1, source_target_pairs={{0,4},{2,6},{4,0},{6,2},{1,5},{3,7},{5,1},{7,3},{8,12},{10,14},{12... | collective-permute-start | bytes 1572872 | tf_op jit(solution)/shard_map/ppermute | solution.py:17
  20.8 22.9 %copy-start.16 = (bf16[64,704]{1,0:T(8,128)(2,1)S(1)}, bf16[64,704]{1,0:T(8,128)(2,1)}, u32[]{:S(2)}) copy-start(bf16[64,704]{1,0:T(8,128)(2,1)} %param.11) | copy-start | bytes 270340
  29.5 24.6 %copy-start.8 = (bf16[1024,704]{0,1:T(8,128)(2,1)S(1)}, bf16[1024,704]{0,1:T(8,128)(2,1)}, u32[]{:S(2)}) copy-start(bf16[1024,704]{0,1:T(8,128)(2,1)} %param.9) | copy-start | bytes 4325380
  43.5 20.4 %collective-permute-start.6 = (bf16[4,1,128,2048]{3,2,1,0:T(8,128)(2,1)S(1)}, bf16[4,1,128,2048]{3,2,1,0:T(8,128)(2,1)}, u32[]{:S(2)}, u32[]{:S(2)}) collective-permute-start(bf16[4,1,128,2048]{3,2,1,0:T(8,128)(2,1)S(1)} %bitcast_dynamic-update-slice_fusion), channel_id=1, source_target_pairs={{0,1},{1,0},{2,3},{3,2},{4,5},{5,4},{6,7},{7,6},{8,9},{9,8},{10,11... | collective-permute-start | bytes 6291464 | tf_op jit(solution)/shard_map/ppermute | solution.py:22
  44.6 38.6 %all-to-all-start = ((bf16[8,64,704]{2,1,0:T(8,128)(2,1)}), bf16[8,64,704]{2,1,0:T(8,128)(2,1)}, u32[]{:S(2)}, u32[]{:S(2)}) async-start(bf16[8,64,704]{2,1,0:T(8,128)(2,1)} %broadcast_in_dim.52), calls=%async_computation | async-start | bytes 1572864 | tf_op jit(solution)/shard_map/all_to_all | solution.py:45
  53.1 148.5 %reduce-scatter.2.cloned.1.call-start = ((), (), s32[]{:S(2)}) async-start(), calls=%async_computation.5 | async-start | bytes 3244032 | tf_op jit(solution)/shard_map/reduce_scatter | solution.py:194
  83.2 21.0 %collective-permute-start.7 = (bf16[8,64,704]{2,1,0:T(8,128)(2,1)}, bf16[8,64,704]{2,1,0:T(8,128)(2,1)S(1)}, u32[]{:S(2)}, u32[]{:S(2)}) collective-permute-start(bf16[8,64,704]{2,1,0:T(8,128)(2,1)} %all-to-all-done.own), channel_id=1, source_target_pairs={{0,8},{8,16},{16,24},{24,0},{1,9},{9,17},{17,25},{25,1},{2,10},{10... | collective-permute-start | bytes 2162696 | tf_op jit(solution)/shard_map/ppermute | solution.py:17
  84.7 35.7 %collective-permute-start.8 = (bf16[8,64,704]{2,1,0:T(8,128)(2,1)}, bf16[8,64,704]{2,1,0:T(8,128)(2,1)S(1)}, u32[]{:S(2)}, u32[]{:S(2)}) collective-permute-start(bf16[8,64,704]{2,1,0:T(8,128)(2,1)} %all-to-all-done.own), channel_id=1, source_target_pairs={{0,24},{8,0},{16,8},{24,16},{1,25},{9,1},{17,9},{25,17},{2,26},{10... | collective-permute-start | bytes 2162696 | tf_op jit(solution)/shard_map/ppermute | solution.py:17
  86.5 35.4 %collective-permute-start.9 = (bf16[8,64,704]{2,1,0:T(8,128)(2,1)}, bf16[8,64,704]{2,1,0:T(8,128)(2,1)S(1)}, u32[]{:S(2)}, u32[]{:S(2)}) collective-permute-start(bf16[8,64,704]{2,1,0:T(8,128)(2,1)} %all-to-all-done.own), channel_id=1, source_target_pairs={{0,16},{8,24},{16,0},{24,8},{1,17},{9,25},{17,1},{25,9},{2,18},{10... | collective-permute-start | bytes 2162696 | tf_op jit(solution)/shard_map/ppermute | solution.py:17
  139.9 15.4 %collective-permute-start.10 = (bf16[4,1,2048,128]{3,2,1,0:T(8,128)(2,1)}, bf16[4,1,2048,128]{3,2,1,0:T(8,128)(2,1)}, u32[]{:S(2)}, u32[]{:S(2)}) collective-permute-start(bf16[4,1,2048,128]{3,2,1,0:T(8,128)(2,1)} %constant_dynamic-slice_fusion.7), channel_id=1, source_target_pairs={{0,1},{1,0},{2,3},{3,2},{4,5},{5,4},{6,7},{7,6},{8,9},{9,8},{10,11... | collective-permute-start | bytes 6291464 | tf_op jit(solution)/shard_map/ppermute | solution.py:22
  143.0 6.3 %copy-start.20 = (f32[704]{0:T(1024)S(1)}, f32[704]{0:T(1024)}, u32[]{:S(2)}) copy-start(f32[704]{0:T(1024)} %get-tuple-element.39) | copy-start | bytes 8452
  143.0 6.3 %copy-start.19 = (f32[704]{0:T(1024)S(1)}, f32[704]{0:T(1024)}, u32[]{:S(2)}) copy-start(f32[704]{0:T(1024)} %get-tuple-element.40) | copy-start | bytes 8452
  143.0 6.3 %copy-start.18 = (f32[704]{0:T(1024)S(1)}, f32[704]{0:T(1024)}, u32[]{:S(2)}) copy-start(f32[704]{0:T(1024)} %get-tuple-element.41) | copy-start | bytes 8452
  144.8 25.1 %collective-permute-start.14 = (bf16[8,1,64,704]{3,2,1,0:T(8,128)(2,1)}, bf16[8,1,64,704]{3,2,1,0:T(8,128)(2,1)S(1)}, u32[]{:S(2)}, u32[]{:S(2)}) collective-permute-start(bf16[8,1,64,704]{3,2,1,0:T(8,128)(2,1)} %get-tuple-element.50), channel_id=1, source_target_pairs={{0,8},{8,16},{16,24},{24,0},{1,9},{9,17},{17,25},{25,1},{2,10},{10... | collective-permute-start | bytes 2162696 | tf_op jit(solution)/shard_map/ppermute | solution.py:17
  146.0 40.6 %collective-permute-start.15 = (bf16[8,1,64,704]{3,2,1,0:T(8,128)(2,1)}, bf16[8,1,64,704]{3,2,1,0:T(8,128)(2,1)}, u32[]{:S(2)}, u32[]{:S(2)}) collective-permute-start(bf16[8,1,64,704]{3,2,1,0:T(8,128)(2,1)} %get-tuple-element.49), channel_id=1, source_target_pairs={{0,24},{8,0},{16,8},{24,16},{1,25},{9,1},{17,9},{25,17},{2,26},{10... | collective-permute-start | bytes 2162696 | tf_op jit(solution)/shard_map/ppermute | solution.py:17
  148.0 40.3 %collective-permute-start.16 = (bf16[8,1,64,704]{3,2,1,0:T(8,128)(2,1)}, bf16[8,1,64,704]{3,2,1,0:T(8,128)(2,1)}, u32[]{:S(2)}, u32[]{:S(2)}) collective-permute-start(bf16[8,1,64,704]{3,2,1,0:T(8,128)(2,1)} %get-tuple-element.48), channel_id=1, source_target_pairs={{0,16},{8,24},{16,0},{24,8},{1,17},{9,25},{17,1},{25,9},{2,18},{10... | collective-permute-start | bytes 2162696 | tf_op jit(solution)/shard_map/ppermute | solution.py:17
  150.2 46.2 %all-to-all-start.2 = ((f32[32,4,704]{2,1,0:T(4,128)}), f32[32,4,704]{2,1,0:T(4,128)S(1)}, u32[]{:S(2)}, u32[]{:S(2)}) async-start(f32[32,4,704]{2,1,0:T(4,128)} %broadcast_in_dim.53), calls=%async_computation.3 | async-start | bytes 786432 | tf_op jit(solution)/shard_map/all_to_all | solution.py:45
  158.0 35.7 %copy-start.11 = (bf16[8,1,64,704]{3,2,1,0:T(8,128)(2,1)S(1)}, bf16[8,1,64,704]{3,2,1,0:T(8,128)(2,1)}, u32[]{:S(2)}) copy-start(bf16[8,1,64,704]{3,2,1,0:T(8,128)(2,1)} %get-tuple-element.15) | copy-start | bytes 2162692
  189.5 17.3 %collective-permute-start.11 = (bf16[1,2048,128]{2,1,0:T(8,128)(2,1)}, bf16[1,2048,128]{2,1,0:T(8,128)(2,1)}, u32[]{:S(2)}, u32[]{:S(2)}) collective-permute-start(bf16[1,2048,128]{2,1,0:T(8,128)(2,1)} %get-tuple-element.52), channel_id=1, source_target_pairs={{0,2},{2,4},{4,6},{6,0},{1,3},{3,5},{5,7},{7,1},{8,10},{10,12},{12... | collective-permute-start | bytes 1572872 | tf_op jit(solution)/shard_map/ppermute | solution.py:17
  191.0 16.0 %collective-permute-start.12 = (bf16[1,2048,128]{2,1,0:T(8,128)(2,1)}, bf16[1,2048,128]{2,1,0:T(8,128)(2,1)}, u32[]{:S(2)}, u32[]{:S(2)}) collective-permute-start(bf16[1,2048,128]{2,1,0:T(8,128)(2,1)} %get-tuple-element.54), channel_id=1, source_target_pairs={{0,6},{2,0},{4,2},{6,4},{1,7},{3,1},{5,3},{7,5},{8,14},{10,8},{12,... | collective-permute-start | bytes 1572872 | tf_op jit(solution)/shard_map/ppermute | solution.py:17
  191.5 24.6 %collective-permute-start.13 = (bf16[1,2048,128]{2,1,0:T(8,128)(2,1)}, bf16[1,2048,128]{2,1,0:T(8,128)(2,1)}, u32[]{:S(2)}, u32[]{:S(2)}) collective-permute-start(bf16[1,2048,128]{2,1,0:T(8,128)(2,1)} %get-tuple-element.53), channel_id=1, source_target_pairs={{0,4},{2,6},{4,0},{6,2},{1,5},{3,7},{5,1},{7,3},{8,12},{10,14},{12... | collective-permute-start | bytes 1572872 | tf_op jit(solution)/shard_map/ppermute | solution.py:17
  196.4 26.3 %all-to-all-start.1 = ((bf16[8,64,704]{2,1,0:T(8,128)(2,1)}), bf16[8,64,704]{2,1,0:T(8,128)(2,1)S(1)}, u32[]{:S(2)}, u32[]{:S(2)}) async-start(bf16[8,64,704]{2,1,0:T(8,128)(2,1)} %fusion.15), calls=%async_computation.1 | async-start | bytes 1572864 | tf_op jit(solution)/shard_map/all_to_all | solution.py:45
  201.0 21.8 %copy-start.17 = (f32[4,704]{1,0:T(4,128)}, f32[4,704]{1,0:T(4,128)S(1)}, u32[]{:S(2)}) copy-start(f32[4,704]{1,0:T(4,128)S(1)} %broadcast_multiply_fusion.1) | copy-start | bytes 33796
  203.6 15.3 %collective-permute-start.17 = (bf16[1,64,704]{2,1,0:T(8,128)(2,1)}, bf16[1,64,704]{2,1,0:T(8,128)(2,1)}, u32[]{:S(2)}, u32[]{:S(2)}) collective-permute-start(bf16[1,64,704]{2,1,0:T(8,128)(2,1)} %get-tuple-element.55), channel_id=1, source_target_pairs={{0,8},{8,16},{16,24},{24,0},{1,9},{9,17},{17,25},{25,1},{2,10},{10... | collective-permute-start | bytes 270344 | tf_op jit(solution)/shard_map/ppermute | solution.py:17
  204.7 14.1 %collective-permute-start.18 = (bf16[1,64,704]{2,1,0:T(8,128)(2,1)}, bf16[1,64,704]{2,1,0:T(8,128)(2,1)}, u32[]{:S(2)}, u32[]{:S(2)}) collective-permute-start(bf16[1,64,704]{2,1,0:T(8,128)(2,1)} %get-tuple-element.57), channel_id=1, source_target_pairs={{0,24},{8,0},{16,8},{24,16},{1,25},{9,1},{17,9},{25,17},{2,26},{10... | collective-permute-start | bytes 270344 | tf_op jit(solution)/shard_map/ppermute | solution.py:17
  206.8 12.0 %collective-permute-start.19 = (bf16[1,64,704]{2,1,0:T(8,128)(2,1)S(1)}, bf16[1,64,704]{2,1,0:T(8,128)(2,1)}, u32[]{:S(2)}, u32[]{:S(2)}) collective-permute-start(bf16[1,64,704]{2,1,0:T(8,128)(2,1)S(1)} %get-tuple-element.56), channel_id=1, source_target_pairs={{0,16},{8,24},{16,0},{24,8},{1,17},{9,25},{17,1},{25,9},{2,18},{10... | collective-permute-start | bytes 270344 | tf_op jit(solution)/shard_map/ppermute | solution.py:17
  (14 other events, 20.9 us)
Sparse Core Ops, SparseCore 0:
  17.8 59.5 all-gather.1
  80.0 47.9 reduce-scatter.1

commit v7 on v6

--- a/solution.py
+++ b/solution.py
@@ -182,8 +182,13 @@
             jnp.sum(conv_grad, axis=0),
         ]
     )
-    conv_copies = copies_of_all(conv_terms, FS)
-    conv_total = added_up(conv_copies) * scale
+    conv_total = conv_terms
+    for axis in ("x", "z"):
+        bit = 1
+        while bit < lax.axis_size(axis):
+            conv_total = conv_total + swapped(conv_total, axis, bit)
+            bit *= 2
+    conv_total = conv_total * scale
 
     gate_terms = contract_rows(whole_tokens, gate_grad).astype(narrow)
     value_terms = contract_rows(whole_tokens, value_grad).astype(narrow)

time: 231 us -> 243 us (1.052)
  waiting for transfers between devices: 90.3 us -> 100 us
  starting transfers between devices: 45.1 us -> 51.9 us
  local copies, waits for them, and re-layouts: 35.8 us -> 32.8 us
    ppermute x2 -> x7, waiting for transfers between devices: 0.01 us -> 18.3 us  [swapped(): return lax.ppermute(block, axis, [(i, i ^ bit) for i in range(size)])]
    ppermute x2 -> x7, starting transfers between devices: 0.1 us -> 10.8 us  [swapped(): return lax.ppermute(block, axis, [(i, i ^ bit) for i in range(size)])]
    ppermute x18, waiting for transfers between devices: 83.9 us -> 77.5 us  [shifted(): lax.ppermute(block, axis, [(i, (i + by) % size) for i in range(size)])]
    all_to_all x3 -> x2, starting transfers between devices: 18 us -> 12 us  [exchanged(): return lax.all_to_all(blocks, axis, 0, 0, tiled=True)]
    all_to_all x3 -> x2, waiting for transfers between devices: 6.36 us -> 4.29 us  [exchanged(): return lax.all_to_all(blocks, axis, 0, 0, tiled=True)]
    unnamed x43 -> x41, local copies, waits for them, and re-layouts: 15 us -> 14.3 us
  transfers between devices with their start and end apart: 25 -> 29, of which waited for: 14 -> 17; matrix products, arithmetic and copies ran while one was open for 25% -> 22% of each run, Pallas kernels for 4% -> 3%
where the time goes in v7:
time: 243 us; the launch traced here: 242 us
  waiting for transfers between devices  100 us (41%)
  starting transfers between devices  51.9 us (21%)
  local copies, waits for them, and re-layouts  32.8 us (13%)
  other arithmetic  23.1 us (10%)
  between operations  14.4 us (6%)
  matrix products  11.2 us (5%)
  Pallas kernels  8.43 us (3%)
    ppermute x18, waiting for transfers between devices, shifted(): lax.ppermute(block, axis, [(i, (i + by) % size) for i in range(size)])  77.5 us
    ppermute x18, starting transfers between devices, shifted(): lax.ppermute(block, axis, [(i, (i + by) % size) for i in range(size)])  29 us
    ppermute x7, waiting for transfers between devices, swapped(): return lax.ppermute(block, axis, [(i, i ^ bit) for i in range(size)])  18.3 us
    unnamed x41, local copies, waits for them, and re-layouts  14.3 us
    all_to_all x2, starting transfers between devices, exchanged(): return lax.all_to_all(blocks, axis, 0, 0, tiled=True)  12 us
    dot_general x2, matrix products, contract_rows(): lax.dot_general(left, right, (((0,), (0,)), ((), ())), preferred_element_...  11.2 us
    ppermute x7, starting transfers between devices, swapped(): return lax.ppermute(block, axis, [(i, i ^ bit) for i in range(size)])  10.8 us
    pallas_call x1, Pallas kernels, back_parts(): pl.pallas_call(back_kernel, grid=(steps,), in_specs=[pl.BlockSpec(memory_...  8.43 us
  transfers between devices with their start and end apart: 29, of which 17 were waited for; matrix products, arithmetic and copies ran while one was open for 22% of the time, Pallas kernels for 3%

profile of v7, /device:TPU:8, one launch (start us, length us, event | category | flops | bytes accessed | tf_op | source)
XLA Modules:
  0.0 241.9 jit_solution(5537749710487321679)
XLA Ops:
  17.6 2.2 collective-permute-start.4
  20.8 6.7 %collective-permute-done.3 = bf16[1,128,2048]{2,1,0:T(8,128)(2,1)} collective-permute-done((bf16[1,128,2048]{2,1,0:T(8,128)(2,1)}, bf16[1,128,2048]{2,1,0:T(8,128)(2,1)}, u32[]{:S(2)}, u32[]{:S(2)}) %collective-permute-start.3) | collective-permute-done | bytes 524320 | tf_op jit(solution)/shard_map/ppermute | solution.py:17
  30.0 2.5 %collective-permute-done.4 = bf16[1,128,2048]{2,1,0:T(8,128)(2,1)} collective-permute-done((bf16[1,128,2048]{2,1,0:T(8,128)(2,1)}, bf16[1,128,2048]{2,1,0:T(8,128)(2,1)}, u32[]{:S(2)}, u32[]{:S(2)}) %collective-permute-start.4) | collective-permute-done | bytes 524320 | tf_op jit(solution)/shard_map/ppermute | solution.py:17
  33.6 8.8 %collective-permute-done.5 = bf16[1,128,2048]{2,1,0:T(8,128)(2,1)} collective-permute-done((bf16[1,128,2048]{2,1,0:T(8,128)(2,1)}, bf16[1,128,2048]{2,1,0:T(8,128)(2,1)}, u32[]{:S(2)}, u32[]{:S(2)}) %collective-permute-start.5) | collective-permute-done | bytes 524320 | tf_op jit(solution)/shard_map/ppermute | solution.py:17
  44.6 8.5 %all-to-all-start = ((bf16[8,64,704]{2,1,0:T(8,128)(2,1)}), bf16[8,64,704]{2,1,0:T(8,128)(2,1)}, u32[]{:S(2)}, u32[]{:S(2)}) async-start(bf16[8,64,704]{2,1,0:T(8,128)(2,1)} %broadcast_in_dim.46), calls=%async_computation | async-start | bytes 1572864 | tf_op jit(solution)/shard_map/all_to_all | solution.py:45
  55.0 7.8 %multiply_reduce_fusion.2 = (f32[704]{0:T(1024)}, f32[704]{0:T(1024)}, f32[704]{0:T(1024)}, f32[704]{0:T(1024)S(1)}, f32[1024,704]{0,1:T(8,128)}, /*index=5*/f32[1024,704]{0,1:T(8,128)S(1)}) fusion(f32[1024,704]{0,1:T(8,128)S(1)} %convert_element_type.123, bf16[1024,704]{0,1:T(8,128)(2,1)S(1)} %copy-done.9, bf16[1024,704]{0,1:T(8,128)(2,1)S(1)} %copy-done.14, ...), kind=kLoop, calls=%fused_computation.25 | loop fusion | flops 25949440 | bytes 12998656 | tf_op jit(solution)/shard_map/reduce_sum | solution.py:179
  64.4 1.9 constant_dynamic-update-slice_fusion
  66.3 1.9 copy-done.11
  68.3 4.5 %convolution_convert_fusion = bf16[2048,704]{0,1:T(8,128)(2,1)} fusion(bf16[1024,704]{0,1:T(8,128)(2,1)S(1)} %fusion.5, bf16[1024,2048]{1,0:T(8,128)(2,1)S(1)} %bitcast.48), kind=kOutput, calls=%fused_computation.5 | convolution fusion | flops 2954231808 | bytes 8519680 | tf_op jit(solution)/shard_map/dot_general | solution.py:83
  72.9 6.0 %fusion.3 = bf16[1024,704]{0,1:T(8,128)(2,1)S(1)} fusion(f32[1024,704]{0,1:T(8,128)} %get-tuple-element.36, f32[704]{0:T(1024)S(1)} %get-tuple-element.34, f32[704]{0:T(1024)S(1)} %get-tuple-element.35, f32[704]{0:T(1024)S(1)} %get-tuple-element.33), kind=kLoop, calls=%fused_computation.14 | loop fusion | flops 4325376 | bytes 4333824 | tf_op jit(solution)/shard_map/convert_element_type | solution.py:176
  78.9 4.3 %all-to-all-done.own = bf16[8,64,704]{2,1,0:T(8,128)(2,1)} async-done(((bf16[8,64,704]{2,1,0:T(8,128)(2,1)}), bf16[8,64,704]{2,1,0:T(8,128)(2,1)}, u32[]{:S(2)}, u32[]{:S(2)}) %all-to-all-start) | async-done | bytes 720928 | tf_op jit(solution)/shard_map/all_to_all | solution.py:45
  88.2 6.7 %convolution_convert_fusion.1 = bf16[2048,704]{0,1:T(8,128)(2,1)} fusion(bf16[1024,704]{0,1:T(8,128)(2,1)S(1)} %fusion.3, bf16[1024,2048]{1,0:T(8,128)(2,1)} %bitcast.49), kind=kOutput, calls=%fused_computation.6 | convolution fusion | flops 2954231808 | bytes 8519680 | tf_op jit(solution)/shard_map/dot_general | solution.py:83
  94.9 9.2 %collective-permute-done.7.rest_0_ = bf16[8,64,704]{2,1,0:T(8,128)(2,1)S(1)} collective-permute-done((bf16[8,64,704]{2,1,0:T(8,128)(2,1)}, bf16[8,64,704]{2,1,0:T(8,128)(2,1)S(1)}, u32[]{:S(2)}, u32[]{:S(2)}) %collective-permute-start.7) | collective-permute-done | bytes 720928 | tf_op jit(solution)/shard_map/ppermute | solution.py:17
  105.1 15.3 %collective-permute-done.8.rest_1_ = bf16[8,64,704]{2,1,0:T(8,128)(2,1)S(1)} collective-permute-done((bf16[8,64,704]{2,1,0:T(8,128)(2,1)}, bf16[8,64,704]{2,1,0:T(8,128)(2,1)S(1)}, u32[]{:S(2)}, u32[]{:S(2)}) %collective-permute-start.8) | collective-permute-done | bytes 720928 | tf_op jit(solution)/shard_map/ppermute | solution.py:17
  122.7 1.9 copy-done.2
  128.1 8.4 %shard_map.119 = bf16[8,2048,128]{2,1,0:T(8,128)(2,1)S(1)} custom-call(s32[4]{0:T(128)S(1)} %pad_add_fusion.place, bf16[704,1024]{1,0:T(8,128)(2,1)S(1)} %bitcast.44, bf16[704,1024]{1,0:T(8,128)(2,1)S(1)} %bitcast.45, bf16[2048,704]{1,0:T(8,128)(2,1)S(1)} %copy-done.2, bf16[8,64,704]{2,1,0:T(8,128)(2,1)} %all-to-all-done.own, ...), custom_call_target="tpu_custom_call" | custom-call | flops 5905580032 | bytes 12845056 | tf_op jit(solution)/shard_map/pallas_call | solution.py:109
  136.5 1.9 copy-done
  141.2 3.1 %copy.18 = bf16[2048,704]{1,0:T(8,128)(2,1)S(1)} copy(bf16[2048,704]{0,1:T(8,128)(2,1)} %convolution_convert_fusion.1) | data formatting | bytes 5767168 | tf_op jit(solution)/shard_map/convert_element_type | solution.py:193
  145.7 2.4 collective-permute-start.15
  148.0 2.1 collective-permute-start.16
  151.7 2.1 add_convert_fusion
  153.8 12.0 %collective-permute-done.14 = bf16[8,1,64,704]{3,2,1,0:T(8,128)(2,1)S(1)} collective-permute-done((bf16[8,1,64,704]{3,2,1,0:T(8,128)(2,1)S(1)}, bf16[8,1,64,704]{3,2,1,0:T(8,128)(2,1)S(1)}, u32[]{:S(2)}, u32[]{:S(2)}) %collective-permute-start.14) | collective-permute-done | bytes 720928 | tf_op jit(solution)/shard_map/ppermute | solution.py:17
  166.4 16.6 %collective-permute-done.16 = bf16[8,1,64,704]{3,2,1,0:T(8,128)(2,1)S(1)} collective-permute-done((bf16[8,1,64,704]{3,2,1,0:T(8,128)(2,1)S(1)}, bf16[8,1,64,704]{3,2,1,0:T(8,128)(2,1)S(1)}, u32[]{:S(2)}, u32[]{:S(2)}) %collective-permute-start.16) | collective-permute-done | bytes 720928 | tf_op jit(solution)/shard_map/ppermute | solution.py:17
  185.5 3.5 %all-to-all-start.1 = ((bf16[8,64,704]{2,1,0:T(8,128)(2,1)}), bf16[8,64,704]{2,1,0:T(8,128)(2,1)S(1)}, u32[]{:S(2)}, u32[]{:S(2)}) async-start(bf16[8,64,704]{2,1,0:T(8,128)(2,1)} %fusion.15), calls=%async_computation.1 | async-start | bytes 1572864 | tf_op jit(solution)/shard_map/all_to_all | solution.py:45
  191.1 3.0 %collective-permute-start.13 = (bf16[1,2048,128]{2,1,0:T(8,128)(2,1)}, bf16[1,2048,128]{2,1,0:T(8,128)(2,1)}, u32[]{:S(2)}, u32[]{:S(2)}) collective-permute-start(bf16[1,2048,128]{2,1,0:T(8,128)(2,1)} %get-tuple-element.43), channel_id=1, source_target_pairs={{0,4},{2,6},{4,0},{6,2},{1,5},{3,7},{5,1},{7,3},{8,12},{10,14},{12... | collective-permute-start | bytes 1572872 | tf_op jit(solution)/shard_map/ppermute | solution.py:17
  194.2 2.3 collective-permute-start.22
  196.6 11.7 %collective-permute-done.22 = f32[4,704]{1,0:T(4,128)S(1)} collective-permute-done((f32[4,704]{1,0:T(4,128)S(1)}, f32[4,704]{1,0:T(4,128)S(1)}, u32[]{:S(2)}, u32[]{:S(2)}) %collective-permute-start.22) | collective-permute-done | bytes 11296 | tf_op jit(solution)/shard_map/ppermute | solution.py:22
  209.2 3.6 %collective-permute-done.23 = f32[4,704]{1,0:T(4,128)S(1)} collective-permute-done((f32[4,704]{1,0:T(4,128)S(1)}, f32[4,704]{1,0:T(4,128)S(1)}, u32[]{:S(2)}, u32[]{:S(2)}) %collective-permute-start.23) | collective-permute-done | bytes 11296 | tf_op jit(solution)/shard_map/ppermute | solution.py:22
  212.9 4.6 %collective-permute-start.24 = (f32[4,704]{1,0:T(4,128)S(1)}, f32[4,704]{1,0:T(4,128)S(1)}, u32[]{:S(2)}, u32[]{:S(2)}) collective-permute-start(f32[4,704]{1,0:T(4,128)S(1)} %add.153), channel_id=1, source_target_pairs={{0,128},{32,160},{64,192},{96,224},{128,0},{160,32},{192,64},{224,... | collective-permute-start | bytes 33800 | tf_op jit(solution)/shard_map/ppermute | solution.py:22
  217.5 3.0 %collective-permute-done.24 = f32[4,704]{1,0:T(4,128)S(1)} collective-permute-done((f32[4,704]{1,0:T(4,128)S(1)}, f32[4,704]{1,0:T(4,128)S(1)}, u32[]{:S(2)}, u32[]{:S(2)}) %collective-permute-start.24) | collective-permute-done | bytes 11296 | tf_op jit(solution)/shard_map/ppermute | solution.py:22
  223.6 2.7 %collective-permute-start.18 = (bf16[1,64,704]{2,1,0:T(8,128)(2,1)}, bf16[1,64,704]{2,1,0:T(8,128)(2,1)}, u32[]{:S(2)}, u32[]{:S(2)}) collective-permute-start(bf16[1,64,704]{2,1,0:T(8,128)(2,1)} %get-tuple-element.47), channel_id=1, source_target_pairs={{0,24},{8,0},{16,8},{24,16},{1,25},{9,1},{17,9},{25,17},{2,26},{10... | collective-permute-start | bytes 270344 | tf_op jit(solution)/shard_map/ppermute | solution.py:17
  229.8 2.7 %collective-permute-done.19 = bf16[1,64,704]{2,1,0:T(8,128)(2,1)} collective-permute-done((bf16[1,64,704]{2,1,0:T(8,128)(2,1)S(1)}, bf16[1,64,704]{2,1,0:T(8,128)(2,1)}, u32[]{:S(2)}, u32[]{:S(2)}) %collective-permute-start.19) | collective-permute-done | bytes 90144 | tf_op jit(solution)/shard_map/ppermute | solution.py:17
  (112 shorter events, 53.4 us)
Async XLA Ops:
  7.2 115.6 %all-gather.2.cloned.1.call-start = ((), (), s32[]{:S(2)}) async-start(), calls=%async_computation.3 | async-start | bytes 3538944 | tf_op jit(solution)/shard_map/all_gather | solution.py:147
  7.2 6.7 %collective-permute-start = (bf16[1,64,704]{2,1,0:T(8,128)(2,1)}, bf16[1,64,704]{2,1,0:T(8,128)(2,1)S(1)}, u32[]{:S(2)}, u32[]{:S(2)}) collective-permute-start(bf16[1,64,704]{2,1,0:T(8,128)(2,1)} %bitcast.56), channel_id=1, source_target_pairs={{0,8},{8,16},{16,24},{24,0},{1,9},{9,17},{17,25},{25,1},{2,10},{10... | collective-permute-start | bytes 270344 | tf_op jit(solution)/shard_map/ppermute | solution.py:17
  8.8 6.3 %collective-permute-start.1 = (bf16[1,64,704]{2,1,0:T(8,128)(2,1)}, bf16[1,64,704]{2,1,0:T(8,128)(2,1)S(1)}, u32[]{:S(2)}, u32[]{:S(2)}) collective-permute-start(bf16[1,64,704]{2,1,0:T(8,128)(2,1)} %bitcast.57), channel_id=1, source_target_pairs={{0,24},{8,0},{16,8},{24,16},{1,25},{9,1},{17,9},{25,17},{2,26},{10... | collective-permute-start | bytes 270344 | tf_op jit(solution)/shard_map/ppermute | solution.py:17
  10.5 6.3 %collective-permute-start.2 = (bf16[1,64,704]{2,1,0:T(8,128)(2,1)}, bf16[1,64,704]{2,1,0:T(8,128)(2,1)S(1)}, u32[]{:S(2)}, u32[]{:S(2)}) collective-permute-start(bf16[1,64,704]{2,1,0:T(8,128)(2,1)} %bitcast.58), channel_id=1, source_target_pairs={{0,16},{8,24},{16,0},{24,8},{1,17},{9,25},{17,1},{25,9},{2,18},{10... | collective-permute-start | bytes 270344 | tf_op jit(solution)/shard_map/ppermute | solution.py:17
  12.3 15.1 %collective-permute-start.3 = (bf16[1,128,2048]{2,1,0:T(8,128)(2,1)}, bf16[1,128,2048]{2,1,0:T(8,128)(2,1)}, u32[]{:S(2)}, u32[]{:S(2)}) collective-permute-start(bf16[1,128,2048]{2,1,0:T(8,128)(2,1)} %bitcast.53), channel_id=1, source_target_pairs={{0,2},{2,4},{4,6},{6,0},{1,3},{3,5},{5,7},{7,1},{8,10},{10,12},{12... | collective-permute-start | bytes 1572872 | tf_op jit(solution)/shard_map/ppermute | solution.py:17
  17.6 14.9 %collective-permute-start.4 = (bf16[1,128,2048]{2,1,0:T(8,128)(2,1)}, bf16[1,128,2048]{2,1,0:T(8,128)(2,1)}, u32[]{:S(2)}, u32[]{:S(2)}) collective-permute-start(bf16[1,128,2048]{2,1,0:T(8,128)(2,1)} %bitcast.54), channel_id=1, source_target_pairs={{0,6},{2,0},{4,2},{6,4},{1,7},{3,1},{5,3},{7,5},{8,14},{10,8},{12,... | collective-permute-start | bytes 1572872 | tf_op jit(solution)/shard_map/ppermute | solution.py:17
  19.9 22.6 %collective-permute-start.5 = (bf16[1,128,2048]{2,1,0:T(8,128)(2,1)}, bf16[1,128,2048]{2,1,0:T(8,128)(2,1)}, u32[]{:S(2)}, u32[]{:S(2)}) collective-permute-start(bf16[1,128,2048]{2,1,0:T(8,128)(2,1)} %bitcast.55), channel_id=1, source_target_pairs={{0,4},{2,6},{4,0},{6,2},{1,5},{3,7},{5,1},{7,3},{8,12},{10,14},{12... | collective-permute-start | bytes 1572872 | tf_op jit(solution)/shard_map/ppermute | solution.py:17
  20.8 22.9 %copy-start.15 = (bf16[64,704]{1,0:T(8,128)(2,1)S(1)}, bf16[64,704]{1,0:T(8,128)(2,1)}, u32[]{:S(2)}) copy-start(bf16[64,704]{1,0:T(8,128)(2,1)} %param.11) | copy-start | bytes 270340
  28.8 25.3 %copy-start.9 = (bf16[1024,704]{0,1:T(8,128)(2,1)S(1)}, bf16[1024,704]{0,1:T(8,128)(2,1)}, u32[]{:S(2)}) copy-start(bf16[1024,704]{0,1:T(8,128)(2,1)} %param.9) | copy-start | bytes 4325380
  43.5 20.4 %collective-permute-start.6 = (bf16[4,1,128,2048]{3,2,1,0:T(8,128)(2,1)S(1)}, bf16[4,1,128,2048]{3,2,1,0:T(8,128)(2,1)}, u32[]{:S(2)}, u32[]{:S(2)}) collective-permute-start(bf16[4,1,128,2048]{3,2,1,0:T(8,128)(2,1)S(1)} %bitcast_dynamic-update-slice_fusion), channel_id=1, source_target_pairs={{0,1},{1,0},{2,3},{3,2},{4,5},{5,4},{6,7},{7,6},{8,9},{9,8},{10,11... | collective-permute-start | bytes 6291464 | tf_op jit(solution)/shard_map/ppermute | solution.py:22
  44.6 38.6 %all-to-all-start = ((bf16[8,64,704]{2,1,0:T(8,128)(2,1)}), bf16[8,64,704]{2,1,0:T(8,128)(2,1)}, u32[]{:S(2)}, u32[]{:S(2)}) async-start(bf16[8,64,704]{2,1,0:T(8,128)(2,1)} %broadcast_in_dim.46), calls=%async_computation | async-start | bytes 1572864 | tf_op jit(solution)/shard_map/all_to_all | solution.py:45
  53.1 168.0 %reduce-scatter.2.cloned.1.call-start = ((), (), s32[]{:S(2)}) async-start(), calls=%async_computation.4 | async-start | bytes 3244032 | tf_op jit(solution)/shard_map/reduce_scatter | solution.py:199
  83.2 21.0 %collective-permute-start.7 = (bf16[8,64,704]{2,1,0:T(8,128)(2,1)}, bf16[8,64,704]{2,1,0:T(8,128)(2,1)S(1)}, u32[]{:S(2)}, u32[]{:S(2)}) collective-permute-start(bf16[8,64,704]{2,1,0:T(8,128)(2,1)} %all-to-all-done.own), channel_id=1, source_target_pairs={{0,8},{8,16},{16,24},{24,0},{1,9},{9,17},{17,25},{25,1},{2,10},{10... | collective-permute-start | bytes 2162696 | tf_op jit(solution)/shard_map/ppermute | solution.py:17
  84.7 35.7 %collective-permute-start.8 = (bf16[8,64,704]{2,1,0:T(8,128)(2,1)}, bf16[8,64,704]{2,1,0:T(8,128)(2,1)S(1)}, u32[]{:S(2)}, u32[]{:S(2)}) collective-permute-start(bf16[8,64,704]{2,1,0:T(8,128)(2,1)} %all-to-all-done.own), channel_id=1, source_target_pairs={{0,24},{8,0},{16,8},{24,16},{1,25},{9,1},{17,9},{25,17},{2,26},{10... | collective-permute-start | bytes 2162696 | tf_op jit(solution)/shard_map/ppermute | solution.py:17
  86.4 35.4 %collective-permute-start.9 = (bf16[8,64,704]{2,1,0:T(8,128)(2,1)}, bf16[8,64,704]{2,1,0:T(8,128)(2,1)S(1)}, u32[]{:S(2)}, u32[]{:S(2)}) collective-permute-start(bf16[8,64,704]{2,1,0:T(8,128)(2,1)} %all-to-all-done.own), channel_id=1, source_target_pairs={{0,16},{8,24},{16,0},{24,8},{1,17},{9,25},{17,1},{25,9},{2,18},{10... | collective-permute-start | bytes 2162696 | tf_op jit(solution)/shard_map/ppermute | solution.py:17
  139.9 11.8 %collective-permute-start.10 = (bf16[4,1,2048,128]{3,2,1,0:T(8,128)(2,1)}, bf16[4,1,2048,128]{3,2,1,0:T(8,128)(2,1)}, u32[]{:S(2)}, u32[]{:S(2)}) collective-permute-start(bf16[4,1,2048,128]{3,2,1,0:T(8,128)(2,1)} %constant_dynamic-slice_fusion.7), channel_id=1, source_target_pairs={{0,1},{1,0},{2,3},{3,2},{4,5},{5,4},{6,7},{7,6},{8,9},{9,8},{10,11... | collective-permute-start | bytes 6291464 | tf_op jit(solution)/shard_map/ppermute | solution.py:22
  140.0 10.1 %collective-permute-start.20 = (f32[4,704]{1,0:T(4,128)S(1)}, f32[4,704]{1,0:T(4,128)S(1)}, u32[]{:S(2)}, u32[]{:S(2)}) collective-permute-start(f32[4,704]{1,0:T(4,128)S(1)} %pad_maximum_fusion), channel_id=1, source_target_pairs={{0,8},{8,0},{16,24},{24,16},{1,9},{9,1},{17,25},{25,17},{2,10},{10... | collective-permute-start | bytes 33800 | tf_op jit(solution)/shard_map/ppermute | solution.py:22
  144.7 21.1 %collective-permute-start.14 = (bf16[8,1,64,704]{3,2,1,0:T(8,128)(2,1)S(1)}, bf16[8,1,64,704]{3,2,1,0:T(8,128)(2,1)S(1)}, u32[]{:S(2)}, u32[]{:S(2)}) collective-permute-start(bf16[8,1,64,704]{3,2,1,0:T(8,128)(2,1)S(1)} %get-tuple-element.40), channel_id=1, source_target_pairs={{0,8},{8,16},{16,24},{24,0},{1,9},{9,17},{17,25},{25,1},{2,10},{10... | collective-permute-start | bytes 2162696 | tf_op jit(solution)/shard_map/ppermute | solution.py:17
  145.7 20.8 %collective-permute-start.15 = (bf16[8,1,64,704]{3,2,1,0:T(8,128)(2,1)S(1)}, bf16[8,1,64,704]{3,2,1,0:T(8,128)(2,1)S(1)}, u32[]{:S(2)}, u32[]{:S(2)}) collective-permute-start(bf16[8,1,64,704]{3,2,1,0:T(8,128)(2,1)S(1)} %get-tuple-element.39), channel_id=1, source_target_pairs={{0,24},{8,0},{16,8},{24,16},{1,25},{9,1},{17,9},{25,17},{2,26},{10... | collective-permute-start | bytes 2162696 | tf_op jit(solution)/shard_map/ppermute | solution.py:17
  148.0 35.0 %collective-permute-start.16 = (bf16[8,1,64,704]{3,2,1,0:T(8,128)(2,1)S(1)}, bf16[8,1,64,704]{3,2,1,0:T(8,128)(2,1)S(1)}, u32[]{:S(2)}, u32[]{:S(2)}) collective-permute-start(bf16[8,1,64,704]{3,2,1,0:T(8,128)(2,1)S(1)} %get-tuple-element.38), channel_id=1, source_target_pairs={{0,16},{8,24},{16,0},{24,8},{1,17},{9,25},{17,1},{25,9},{2,18},{10... | collective-permute-start | bytes 2162696 | tf_op jit(solution)/shard_map/ppermute | solution.py:17
  150.1 44.1 %collective-permute-start.21 = (f32[4,704]{1,0:T(4,128)S(1)}, f32[4,704]{1,0:T(4,128)S(1)}, u32[]{:S(2)}, u32[]{:S(2)}) collective-permute-start(f32[4,704]{1,0:T(4,128)S(1)} %fusion.17), channel_id=1, source_target_pairs={{0,16},{8,24},{16,0},{24,8},{1,17},{9,25},{17,1},{25,9},{2,18},{10... | collective-permute-start | bytes 33800 | tf_op jit(solution)/shard_map/ppermute | solution.py:22
  185.5 48.8 %all-to-all-start.1 = ((bf16[8,64,704]{2,1,0:T(8,128)(2,1)}), bf16[8,64,704]{2,1,0:T(8,128)(2,1)S(1)}, u32[]{:S(2)}, u32[]{:S(2)}) async-start(bf16[8,64,704]{2,1,0:T(8,128)(2,1)} %fusion.15), calls=%async_computation.1 | async-start | bytes 1572864 | tf_op jit(solution)/shard_map/all_to_all | solution.py:45
  189.0 37.2 %collective-permute-start.11 = (bf16[1,2048,128]{2,1,0:T(8,128)(2,1)}, bf16[1,2048,128]{2,1,0:T(8,128)(2,1)}, u32[]{:S(2)}, u32[]{:S(2)}) collective-permute-start(bf16[1,2048,128]{2,1,0:T(8,128)(2,1)} %get-tuple-element.42), channel_id=1, source_target_pairs={{0,2},{2,4},{4,6},{6,0},{1,3},{3,5},{5,7},{7,1},{8,10},{10,12},{12... | collective-permute-start | bytes 1572872 | tf_op jit(solution)/shard_map/ppermute | solution.py:17
  190.6 36.1 %collective-permute-start.12 = (bf16[1,2048,128]{2,1,0:T(8,128)(2,1)}, bf16[1,2048,128]{2,1,0:T(8,128)(2,1)}, u32[]{:S(2)}, u32[]{:S(2)}) collective-permute-start(bf16[1,2048,128]{2,1,0:T(8,128)(2,1)} %get-tuple-element.44), channel_id=1, source_target_pairs={{0,6},{2,0},{4,2},{6,4},{1,7},{3,1},{5,3},{7,5},{8,14},{10,8},{12,... | collective-permute-start | bytes 1572872 | tf_op jit(solution)/shard_map/ppermute | solution.py:17
  191.1 35.5 %collective-permute-start.13 = (bf16[1,2048,128]{2,1,0:T(8,128)(2,1)}, bf16[1,2048,128]{2,1,0:T(8,128)(2,1)}, u32[]{:S(2)}, u32[]{:S(2)}) collective-permute-start(bf16[1,2048,128]{2,1,0:T(8,128)(2,1)} %get-tuple-element.43), channel_id=1, source_target_pairs={{0,4},{2,6},{4,0},{6,2},{1,5},{3,7},{5,1},{7,3},{8,12},{10,14},{12... | collective-permute-start | bytes 1572872 | tf_op jit(solution)/shard_map/ppermute | solution.py:17
  194.2 14.0 %collective-permute-start.22 = (f32[4,704]{1,0:T(4,128)S(1)}, f32[4,704]{1,0:T(4,128)S(1)}, u32[]{:S(2)}, u32[]{:S(2)}) collective-permute-start(f32[4,704]{1,0:T(4,128)S(1)} %fusion.23), channel_id=1, source_target_pairs={{0,32},{32,0},{64,96},{96,64},{128,160},{160,128},{192,224},{224,1... | collective-permute-start | bytes 33800 | tf_op jit(solution)/shard_map/ppermute | solution.py:22
  208.3 4.6 %collective-permute-start.23 = (f32[4,704]{1,0:T(4,128)S(1)}, f32[4,704]{1,0:T(4,128)S(1)}, u32[]{:S(2)}, u32[]{:S(2)}) collective-permute-start(f32[4,704]{1,0:T(4,128)S(1)} %add.152), channel_id=1, source_target_pairs={{0,64},{32,96},{64,0},{96,32},{128,192},{160,224},{192,128},{224,1... | collective-permute-start | bytes 33800 | tf_op jit(solution)/shard_map/ppermute | solution.py:22
  212.9 7.6 %collective-permute-start.24 = (f32[4,704]{1,0:T(4,128)S(1)}, f32[4,704]{1,0:T(4,128)S(1)}, u32[]{:S(2)}, u32[]{:S(2)}) collective-permute-start(f32[4,704]{1,0:T(4,128)S(1)} %add.153), channel_id=1, source_target_pairs={{0,128},{32,160},{64,192},{96,224},{128,0},{160,32},{192,64},{224,... | collective-permute-start | bytes 33800 | tf_op jit(solution)/shard_map/ppermute | solution.py:22
  220.5 13.9 %copy-start.16 = (f32[4,704]{1,0:T(4,128)}, f32[4,704]{1,0:T(4,128)S(1)}, u32[]{:S(2)}) copy-start(f32[4,704]{1,0:T(4,128)S(1)} %add_multiply_fusion) | copy-start | bytes 33796
  223.0 6.3 %collective-permute-start.17 = (bf16[1,64,704]{2,1,0:T(8,128)(2,1)}, bf16[1,64,704]{2,1,0:T(8,128)(2,1)}, u32[]{:S(2)}, u32[]{:S(2)}) collective-permute-start(bf16[1,64,704]{2,1,0:T(8,128)(2,1)} %get-tuple-element.45), channel_id=1, source_target_pairs={{0,8},{8,16},{16,24},{24,0},{1,9},{9,17},{17,25},{25,1},{2,10},{10... | collective-permute-start | bytes 270344 | tf_op jit(solution)/shard_map/ppermute | solution.py:17
  223.6 6.2 %collective-permute-start.18 = (bf16[1,64,704]{2,1,0:T(8,128)(2,1)}, bf16[1,64,704]{2,1,0:T(8,128)(2,1)}, u32[]{:S(2)}, u32[]{:S(2)}) collective-permute-start(bf16[1,64,704]{2,1,0:T(8,128)(2,1)} %get-tuple-element.47), channel_id=1, source_target_pairs={{0,24},{8,0},{16,8},{24,16},{1,25},{9,1},{17,9},{25,17},{2,26},{10... | collective-permute-start | bytes 270344 | tf_op jit(solution)/shard_map/ppermute | solution.py:17
  226.3 6.2 %collective-permute-start.19 = (bf16[1,64,704]{2,1,0:T(8,128)(2,1)S(1)}, bf16[1,64,704]{2,1,0:T(8,128)(2,1)}, u32[]{:S(2)}, u32[]{:S(2)}) collective-permute-start(bf16[1,64,704]{2,1,0:T(8,128)(2,1)S(1)} %get-tuple-element.46), channel_id=1, source_target_pairs={{0,16},{8,24},{16,0},{24,8},{1,17},{9,25},{17,1},{25,9},{2,18},{10... | collective-permute-start | bytes 270344 | tf_op jit(solution)/shard_map/ppermute | solution.py:17
  (17 other events, 37.9 us)
Sparse Core Ops, SparseCore 0:
  17.8 59.5 all-gather.1
  80.0 47.9 reduce-scatter.1

commit v8 on v6

--- a/solution.py
+++ b/solution.py
@@ -79,10 +79,53 @@
     return blocks.astype(jnp.float32).sum(axis=0)
 
 
-def contract_rows(left, right):
-    return lax.dot_general(
-        left, right, (((0,), (0,)), ((), ())), preferred_element_type=jnp.float32
-    )
+def terms_kernel(place, own, other, gate_t, value_t, gate_out, value_out, tokens):
+    groups, rows, _ = own.shape
+    for k, piece in enumerate((own, other)):
+        for group in range(groups):
+            start = pl.multiple_of(group * 2 * rows + place[k] * rows, rows)
+            tokens[pl.ds(start, rows), :] = piece[group]
+    block = tokens[...]
+    value = jnp.dot(value_t[...], block, preferred_element_type=jnp.float32)
+    value_out[...] = value.astype(value_out.dtype)
+    gate = lax.dot_general(
+        block, gate_t[...], (((0,), (1,)), ((), ())), preferred_element_type=jnp.float32
+    ).astype(gate_out.dtype)
+    peers, tall, share, _ = gate_out.shape
+    for far in range(tall):
+        for near in range(peers):
+            start = (far * peers + near) * share
+            gate_out[near, far] = gate[start : start + share]
+
+
+def grad_terms(place, own, other, gate_t, value_t, far, near, steps):
+    groups, rows, width = own.shape
+    cols, length = gate_t.shape
+    wide, share = width // steps, width // (far * near)
+    whole = pl.BlockSpec((cols, length), lambda i: (0, 0))
+    piece = pl.BlockSpec((groups, rows, wide), lambda i: (0, 0, i))
+    return pl.pallas_call(
+        terms_kernel,
+        grid=(steps,),
+        in_specs=[pl.BlockSpec(memory_space=pltpu.SMEM), piece, piece, whole, whole],
+        out_specs=[
+            pl.BlockSpec((near, far // steps, share, cols), lambda i: (0, i, 0, 0)),
+            pl.BlockSpec((cols, wide), lambda i: (0, i)),
+        ],
+        out_shape=[
+            jax.ShapeDtypeStruct((near, far, share, cols), own.dtype),
+            jax.ShapeDtypeStruct((cols, width), own.dtype),
+        ],
+        scratch_shapes=[pltpu.VMEM((length, wide), own.dtype)],
+        compiler_params=pltpu.CompilerParams(
+            dimension_semantics=("arbitrary",), vmem_limit_bytes=58 * 2**20
+        ),
+        cost_estimate=pl.CostEstimate(
+            flops=4 * width * cols * length,
+            bytes_accessed=4 * (cols * length + width * cols) + 2 * width * length,
+            transcendentals=0,
+        ),
+    )(place, own, other, gate_t, value_t)
 
 
 def back_kernel(place, gate_t, value_t, value_w, own, *rest):
@@ -120,7 +163,7 @@
         out_shape=jax.ShapeDtypeStruct((peers, width, length // peers), value_w.dtype),
         scratch_shapes=[pltpu.VMEM((tall, cols), value_w.dtype)],
         compiler_params=pltpu.CompilerParams(
-            dimension_semantics=("arbitrary",), vmem_limit_bytes=40 * 2**20
+            dimension_semantics=("arbitrary",), vmem_limit_bytes=58 * 2**20
         ),
         cost_estimate=pl.CostEstimate(
             flops=4 * width * cols * length,
@@ -141,7 +184,10 @@
     scale = float(length * nz * nx) ** (-0.5)
     narrow = jnp.bfloat16
 
-    token_blocks = gathered_four(tokens[None], "y", 0)[:, None]
+    token_blocks = gathered_four(tokens[None], "y", 0)
+    other_blocks = swapped(token_blocks, "c", 1)
+    core = lax.axis_index("c")
+    token_places = jnp.stack([core, nc - 1 - core]).astype(jnp.int32)
     gate_part = copies_of_all(up_gate_w, "z")
     value_part = gathered_four(up_value_w[None], "x", 0).reshape(nx * share, cols)
     full_value = lax.all_gather(value_part, "z", axis=0, tiled=True)
@@ -150,10 +196,6 @@
     gate_places = jnp.stack(
         [(lax.axis_index("x") + nx - k) & (nx - 1) for k in (0, *steps)]
     ).astype(jnp.int32)
-    whole_tokens = jnp.broadcast_to(token_blocks, (ny, nc, rows, width))
-    other_blocks = swapped(token_blocks, "c", 1)
-    whole_tokens = put(whole_tokens, other_blocks, "c", 1, 1)
-    whole_tokens = whole_tokens.reshape(length, width)
 
     gate_pre, value_part = lax.optimization_barrier((gate_pre, value_part))
     gate_float = gate_pre.astype(jnp.float32)
@@ -182,16 +224,19 @@
             jnp.sum(conv_grad, axis=0),
         ]
     )
-    conv_copies = copies_of_all(conv_terms, FS)
-    conv_total = added_up(conv_copies) * scale
-
-    gate_terms = contract_rows(whole_tokens, gate_grad).astype(narrow)
-    value_terms = contract_rows(whole_tokens, value_grad).astype(narrow)
+    conv_total = conv_terms
+    for axis, bit in (("z", 1), ("z", 2), ("z", 4), ("x", 1), ("x", 2)):
+        conv_total = conv_total + swapped(conv_total, axis, bit)
+    conv_total = conv_total * scale
+
+    gate_terms, value_terms = grad_terms(
+        token_places, token_blocks, other_blocks, gate_grad.T, value_grad.T, nz, nx, 4
+    )
     gate_grad, value_grad, _, _ = lax.optimization_barrier(
         (gate_grad, value_grad, gate_terms, value_terms)
     )
-    gate_blocks = sent_four(gate_terms.reshape(nz, nx, share, cols), "x", 1)
-    value_sums = lax.psum_scatter(value_terms, "z", scatter_dimension=0, tiled=True)
+    gate_blocks = sent_four(gate_terms, "x", 0)
+    value_sums = lax.psum_scatter(value_terms.T, "z", scatter_dimension=0, tiled=True)
 
     part = back_parts(
         gate_places, gate_grad.T, value_grad.T, full_value, gate_pieces, ny * nc, 4
@@ -205,7 +250,7 @@
 
     gate_blocks, _ = lax.optimization_barrier((gate_blocks, pair))
     gate_sums = total_of(gate_blocks).astype(narrow)
-    gate_sums = exchanged(gate_sums[:, 0], "z")
+    gate_sums = exchanged(gate_sums[0], "z")
     gate_out = added_up(gate_sums) * scale
     value_blocks = sent_four(value_sums.reshape(nx, share, cols), "x", 0)
     value_out = total_of(value_blocks)[0] * scale

time: 231 us -> 236 us (1.022)
  waiting for transfers between devices: 90.3 us -> 112 us
  local copies, waits for them, and re-layouts: 35.8 us -> 16 us
  Pallas kernels: 8.43 us -> 21.6 us
  matrix products: 11.3 us -> 0 us
    ppermute x2 -> x7, waiting for transfers between devices: 0.01 us -> 20.4 us  [swapped(): return lax.ppermute(block, axis, [(i, i ^ bit) for i in range(size)])]
    unnamed x43 -> x21, local copies, waits for them, and re-layouts: 15 us -> 1.79 us
    dot_general x2 -> x0, matrix products: 11.3 us -> none  [contract_rows(): lax.dot_general(left, right, (((0,), (0,)), ((), ())), preferred_element_...]
    pallas_call x0 -> x1, Pallas kernels: none -> 10.7 us  [grad_terms(): pl.pallas_call(terms_kernel, grid=(steps,), in_specs=[pl.BlockSpec(memory...]
    ppermute x2 -> x7, starting transfers between devices: 0.1 us -> 9.35 us  [swapped(): return lax.ppermute(block, axis, [(i, i ^ bit) for i in range(size)])]
    all_to_all x3 -> x2, starting transfers between devices: 18 us -> 12.1 us  [exchanged(): return lax.all_to_all(blocks, axis, 0, 0, tiled=True)]
    convert_element_type x1 -> x0, local copies, waits for them, and re-layouts: 3.13 us -> none  [on_device(): gate_terms = contract_rows(whole_tokens, gate_grad).astype(narrow)]
    convert_element_type x1, other arithmetic: 6.06 us -> 2.93 us  [on_device(): gate_grad = (conv_weight[2] * conv_grad + conv_weight[1] * late[1:length...]
  transfers between devices with their start and end apart: 25 -> 29, of which waited for: 14 -> 17; matrix products, arithmetic and copies ran while one was open for 25% -> 17% of each run, Pallas kernels for 4% -> 9%
where the time goes in v8:
time: 236 us; the launch traced here: 235 us
  waiting for transfers between devices  112 us (47%)
  starting transfers between devices  47.1 us (20%)
  other arithmetic  24.4 us (10%)
  Pallas kernels  21.6 us (9%)
  local copies, waits for them, and re-layouts  16 us (7%)
  between operations  14.3 us (6%)
    ppermute x18, waiting for transfers between devices, shifted(): lax.ppermute(block, axis, [(i, (i + by) % size) for i in range(size)])  85.7 us
    ppermute x18, starting transfers between devices, shifted(): lax.ppermute(block, axis, [(i, (i + by) % size) for i in range(size)])  25.5 us
    ppermute x7, waiting for transfers between devices, swapped(): return lax.ppermute(block, axis, [(i, i ^ bit) for i in range(size)])  20.4 us
    all_to_all x2, starting transfers between devices, exchanged(): return lax.all_to_all(blocks, axis, 0, 0, tiled=True)  12.1 us
    pallas_call x1, Pallas kernels, back_parts(): pl.pallas_call(back_kernel, grid=(steps,), in_specs=[pl.BlockSpec(memory_...  10.9 us
    pallas_call x1, Pallas kernels, grad_terms(): pl.pallas_call(terms_kernel, grid=(steps,), in_specs=[pl.BlockSpec(memory...  10.7 us
    ppermute x7, starting transfers between devices, swapped(): return lax.ppermute(block, axis, [(i, i ^ bit) for i in range(size)])  9.35 us
    reduce_sum x1, other arithmetic, on_device(): jnp.sum(conv_grad * padded[:length], axis=0)  7.1 us
  transfers between devices with their start and end apart: 29, of which 17 were waited for; matrix products, arithmetic and copies ran while one was open for 17% of the time, Pallas kernels for 9%

profile of v8, /device:TPU:8, one launch (start us, length us, event | category | flops | bytes accessed | tf_op | source)
XLA Modules:
  0.0 234.9 jit_solution(4657589756366809673)
XLA Ops:
  8.8 1.7 collective-permute-start.1
  10.5 1.8 collective-permute-start.2
  20.0 2.1 collective-permute-start.5
  22.0 10.8 %collective-permute-done.3 = bf16[1,128,2048]{2,1,0:T(8,128)(2,1)S(1)} collective-permute-done((bf16[1,128,2048]{2,1,0:T(8,128)(2,1)}, bf16[1,128,2048]{2,1,0:T(8,128)(2,1)S(1)}, u32[]{:S(2)}, u32[]{:S(2)}) %collective-permute-start.3) | collective-permute-done | bytes 524320 | tf_op jit(solution)/shard_map/ppermute | solution.py:17
  32.9 2.6 %broadcast_in_dim.12 = bf16[4,128,2048]{2,1,0:T(8,128)(2,1)} broadcast(bf16[128,2048]{1,0:T(8,128)(2,1)} %param.8), dimensions={1,2} | broadcast | bytes 2621440 | tf_op jit(solution)/shard_map/broadcast_in_dim | solution.py:58
  37.1 6.2 %collective-permute-done.5 = bf16[1,128,2048]{2,1,0:T(8,128)(2,1)S(1)} collective-permute-done((bf16[1,128,2048]{2,1,0:T(8,128)(2,1)}, bf16[1,128,2048]{2,1,0:T(8,128)(2,1)S(1)}, u32[]{:S(2)}, u32[]{:S(2)}) %collective-permute-start.5) | collective-permute-done | bytes 524320 | tf_op jit(solution)/shard_map/ppermute | solution.py:17
  45.1 8.6 %all-to-all-start = ((bf16[8,64,704]{2,1,0:T(8,128)(2,1)}), bf16[8,64,704]{2,1,0:T(8,128)(2,1)}, u32[]{:S(2)}, u32[]{:S(2)}) async-start(bf16[8,64,704]{2,1,0:T(8,128)(2,1)} %broadcast_in_dim.27), calls=%async_computation | async-start | bytes 1572864 | tf_op jit(solution)/shard_map/all_to_all | solution.py:45
  54.8 7.1 %multiply_reduce_fusion.2 = (f32[704]{0:T(1024)S(1)}, f32[704]{0:T(1024)S(1)}, f32[704]{0:T(1024)S(1)}, f32[704]{0:T(1024)S(1)}, f32[1024,704]{0,1:T(8,128)S(1)}, /*index=5*/f32[1024,704]{0,1:T(8,128)S(1)}) fusion(f32[1024,704]{0,1:T(8,128)S(1)} %convert_element_type.116, bf16[1024,704]{0,1:T(8,128)(2,1)} %param.9, bf16[1024,704]{0,1:T(8,128)(2,1)} %param.10, ...), kind=kLoop, calls=%fused_computation.23 | loop fusion | flops 25949440 | bytes 12998656 | tf_op jit(solution)/shard_map/reduce_sum | solution.py:221
  61.9 2.2 fusion.5
  64.1 2.9 %fusion.20.gate_t = bf16[704,1024]{1,0:T(8,128)(2,1)} fusion(f32[704]{0:T(1024)S(1)} %get-tuple-element.39, f32[1024,704]{0,1:T(8,128)S(1)} %get-tuple-element.40, f32[704]{0:T(1024)S(1)} %get-tuple-element.38, f32[704]{0:T(1024)S(1)} %get-tuple-element.37), kind=kLoop, calls=%fused_computation.62 | loop fusion | flops 4325376 | bytes 4333824 | tf_op jit(solution)/shard_map/transpose | solution.py:233
  67.0 10.7 %shard_map.119 = (bf16[4,8,64,704]{3,2,1,0:T(8,128)(2,1)}, bf16[704,2048]{1,0:T(8,128)(2,1)}) custom-call(s32[2]{0:T(128)} %pad_add_fusion.1.place, bf16[4,128,2048]{2,1,0:T(8,128)(2,1)} %constant_dynamic-update-slice_fusion.own, bf16[4,128,2048]{2,1,0:T(8,128)(2,1)} %collective-permute-done.6.other, bf16[704,1024]{1,0:T(8,128)(2,1)} %fusion.20.gate_t, ...), custom_call_target="tpu_custom_call" | custom-call | flops 5905580032 | bytes 12845056 | tf_op jit(solution)/shard_map/pallas_call | solution.py:107
  77.8 5.4 %all-to-all-done.own = bf16[8,64,704]{2,1,0:T(8,128)(2,1)} async-done(((bf16[8,64,704]{2,1,0:T(8,128)(2,1)}), bf16[8,64,704]{2,1,0:T(8,128)(2,1)}, u32[]{:S(2)}, u32[]{:S(2)}) %all-to-all-start) | async-done | bytes 720928 | tf_op jit(solution)/shard_map/all_to_all | solution.py:45
  84.7 1.8 collective-permute-start.8
  86.4 1.8 collective-permute-start.9
  88.8 2.9 %fusion.3 = bf16[1024,704]{0,1:T(8,128)(2,1)} fusion(f32[1024,704]{0,1:T(8,128)S(1)} %get-tuple-element.40, f32[704]{0:T(1024)S(1)} %get-tuple-element.38, f32[704]{0:T(1024)S(1)} %get-tuple-element.39, f32[704]{0:T(1024)S(1)} %get-tuple-element.37), kind=kLoop, calls=%fused_computation.12 | loop fusion | flops 4325376 | bytes 4333824 | tf_op jit(solution)/shard_map/convert_element_type | solution.py:218
  91.8 12.5 %collective-permute-done.7.rest_0_ = bf16[8,64,704]{2,1,0:T(8,128)(2,1)} collective-permute-done((bf16[8,64,704]{2,1,0:T(8,128)(2,1)}, bf16[8,64,704]{2,1,0:T(8,128)(2,1)}, u32[]{:S(2)}, u32[]{:S(2)}) %collective-permute-start.7) | collective-permute-done | bytes 720928 | tf_op jit(solution)/shard_map/ppermute | solution.py:17
  104.2 16.1 %collective-permute-done.8.rest_1_ = bf16[8,64,704]{2,1,0:T(8,128)(2,1)} collective-permute-done((bf16[8,64,704]{2,1,0:T(8,128)(2,1)}, bf16[8,64,704]{2,1,0:T(8,128)(2,1)}, u32[]{:S(2)}, u32[]{:S(2)}) %collective-permute-start.8) | collective-permute-done | bytes 720928 | tf_op jit(solution)/shard_map/ppermute | solution.py:17
  122.0 10.9 %shard_map.120 = bf16[8,2048,128]{2,1,0:T(8,128)(2,1)} custom-call(s32[4]{0:T(128)} %pad_add_fusion.place, bf16[704,1024]{1,0:T(8,128)(2,1)} %bitcast.41, bf16[704,1024]{1,0:T(8,128)(2,1)} %bitcast.43, bf16[2048,704]{1,0:T(8,128)(2,1)} %all-gather.2.cloned.1.call-done.value_w, bf16[8,64,704]{2,1,0:T(8,128)(2,1)} %all-to-all-done.own, ...), custom_call_target="tpu_custom_call" | custom-call | flops 5905580032 | bytes 12845056 | tf_op jit(solution)/shard_map/pallas_call | solution.py:152
  132.8 3.2 %constant_dynamic-slice_fusion.7 = bf16[4,1,2048,128]{3,2,1,0:T(8,128)(2,1)} fusion(bf16[4,2,2048,128]{3,2,1,0:T(8,128)(2,1)} %bitcast.35, u32[]{:T(128)S(6)} %and.66), kind=kLoop, calls=%fused_computation.47 | loop fusion | bytes 4194308 | tf_op jit(solution)/shard_map/dynamic_slice | solution.py:41
  137.8 2.1 collective-permute-start.15
  141.5 2.1 add_convert_fusion
  143.6 14.4 %collective-permute-done.14 = bf16[1,8,64,704]{3,2,1,0:T(8,128)(2,1)S(1)} collective-permute-done((bf16[1,8,64,704]{3,2,1,0:T(8,128)(2,1)S(1)}, bf16[1,8,64,704]{3,2,1,0:T(8,128)(2,1)S(1)}, u32[]{:S(2)}, u32[]{:S(2)}) %collective-permute-start.14) | collective-permute-done | bytes 720928 | tf_op jit(solution)/shard_map/ppermute | solution.py:17
  158.0 16.0 %collective-permute-done.15 = bf16[1,8,64,704]{3,2,1,0:T(8,128)(2,1)S(1)} collective-permute-done((bf16[1,8,64,704]{3,2,1,0:T(8,128)(2,1)S(1)}, bf16[1,8,64,704]{3,2,1,0:T(8,128)(2,1)S(1)}, u32[]{:S(2)}, u32[]{:S(2)}) %collective-permute-start.15) | collective-permute-done | bytes 720928 | tf_op jit(solution)/shard_map/ppermute | solution.py:17
  177.4 3.5 %all-to-all-start.1 = ((bf16[8,64,704]{2,1,0:T(8,128)(2,1)}), bf16[8,64,704]{2,1,0:T(8,128)(2,1)S(1)}, u32[]{:S(2)}, u32[]{:S(2)}) async-start(bf16[8,64,704]{2,1,0:T(8,128)(2,1)} %fusion.15), calls=%async_computation.1 | async-start | bytes 1572864 | tf_op jit(solution)/shard_map/all_to_all | solution.py:45
  180.9 2.5 %collective-permute-start.11 = (bf16[1,2048,128]{2,1,0:T(8,128)(2,1)}, bf16[1,2048,128]{2,1,0:T(8,128)(2,1)}, u32[]{:S(2)}, u32[]{:S(2)}) collective-permute-start(bf16[1,2048,128]{2,1,0:T(8,128)(2,1)} %get-tuple-element.46), channel_id=1, source_target_pairs={{0,2},{2,4},{4,6},{6,0},{1,3},{3,5},{5,7},{7,1},{8,10},{10,12},{12... | collective-permute-start | bytes 1572872 | tf_op jit(solution)/shard_map/ppermute | solution.py:17
  185.2 5.9 %collective-permute-start.22 = (f32[4,704]{1,0:T(4,128)S(1)}, f32[4,704]{1,0:T(4,128)S(1)}, u32[]{:S(2)}, u32[]{:S(2)}) collective-permute-start(f32[4,704]{1,0:T(4,128)S(1)} %fusion.19), channel_id=1, source_target_pairs={{0,128},{32,160},{64,192},{96,224},{128,0},{160,32},{192,64},{224,... | collective-permute-start | bytes 33800 | tf_op jit(solution)/shard_map/ppermute | solution.py:22
  191.0 13.5 %collective-permute-done.22 = f32[4,704]{1,0:T(4,128)S(1)} collective-permute-done((f32[4,704]{1,0:T(4,128)S(1)}, f32[4,704]{1,0:T(4,128)S(1)}, u32[]{:S(2)}, u32[]{:S(2)}) %collective-permute-start.22) | collective-permute-done | bytes 11296 | tf_op jit(solution)/shard_map/ppermute | solution.py:22
  205.4 2.8 %collective-permute-done.23 = f32[4,704]{1,0:T(4,128)S(1)} collective-permute-done((f32[4,704]{1,0:T(4,128)S(1)}, f32[4,704]{1,0:T(4,128)S(1)}, u32[]{:S(2)}, u32[]{:S(2)}) %collective-permute-start.23) | collective-permute-done | bytes 11296 | tf_op jit(solution)/shard_map/ppermute | solution.py:22
  209.5 4.0 %collective-permute-done.24 = f32[4,704]{1,0:T(4,128)S(1)} collective-permute-done((f32[4,704]{1,0:T(4,128)S(1)}, f32[4,704]{1,0:T(4,128)S(1)}, u32[]{:S(2)}, u32[]{:S(2)}) %collective-permute-start.24) | collective-permute-done | bytes 11296 | tf_op jit(solution)/shard_map/ppermute | solution.py:22
  216.9 2.4 %collective-permute-start.18 = (bf16[1,64,704]{2,1,0:T(8,128)(2,1)}, bf16[1,64,704]{2,1,0:T(8,128)(2,1)}, u32[]{:S(2)}, u32[]{:S(2)}) collective-permute-start(bf16[1,64,704]{2,1,0:T(8,128)(2,1)} %get-tuple-element.51), channel_id=1, source_target_pairs={{0,24},{8,0},{16,8},{24,16},{1,25},{9,1},{17,9},{25,17},{2,26},{10... | collective-permute-start | bytes 270344 | tf_op jit(solution)/shard_map/ppermute | solution.py:17
  223.1 2.3 collective-permute-done.19
  225.5 1.8 multiply_bitcast_fusion
  (90 shorter events, 36.0 us)
Async XLA Ops:
  7.2 114.8 %all-gather.2.cloned.1.call-start = ((), (), s32[]{:S(2)}) async-start(), calls=%async_computation.3 | async-start | bytes 3538944 | tf_op jit(solution)/shard_map/all_gather | solution.py:193
  7.2 6.1 %collective-permute-start = (bf16[1,64,704]{2,1,0:T(8,128)(2,1)}, bf16[1,64,704]{2,1,0:T(8,128)(2,1)S(1)}, u32[]{:S(2)}, u32[]{:S(2)}) collective-permute-start(bf16[1,64,704]{2,1,0:T(8,128)(2,1)} %bitcast.47), channel_id=1, source_target_pairs={{0,8},{8,16},{16,24},{24,0},{1,9},{9,17},{17,25},{25,1},{2,10},{10... | collective-permute-start | bytes 270344 | tf_op jit(solution)/shard_map/ppermute | solution.py:17
  8.8 6.3 %collective-permute-start.1 = (bf16[1,64,704]{2,1,0:T(8,128)(2,1)}, bf16[1,64,704]{2,1,0:T(8,128)(2,1)S(1)}, u32[]{:S(2)}, u32[]{:S(2)}) collective-permute-start(bf16[1,64,704]{2,1,0:T(8,128)(2,1)} %bitcast.48), channel_id=1, source_target_pairs={{0,24},{8,0},{16,8},{24,16},{1,25},{9,1},{17,9},{25,17},{2,26},{10... | collective-permute-start | bytes 270344 | tf_op jit(solution)/shard_map/ppermute | solution.py:17
  10.5 6.3 %collective-permute-start.2 = (bf16[1,64,704]{2,1,0:T(8,128)(2,1)}, bf16[1,64,704]{2,1,0:T(8,128)(2,1)S(1)}, u32[]{:S(2)}, u32[]{:S(2)}) collective-permute-start(bf16[1,64,704]{2,1,0:T(8,128)(2,1)} %bitcast.49), channel_id=1, source_target_pairs={{0,16},{8,24},{16,0},{24,8},{1,17},{9,25},{17,1},{25,9},{2,18},{10... | collective-permute-start | bytes 270344 | tf_op jit(solution)/shard_map/ppermute | solution.py:17
  17.6 15.2 %collective-permute-start.3 = (bf16[1,128,2048]{2,1,0:T(8,128)(2,1)}, bf16[1,128,2048]{2,1,0:T(8,128)(2,1)S(1)}, u32[]{:S(2)}, u32[]{:S(2)}) collective-permute-start(bf16[1,128,2048]{2,1,0:T(8,128)(2,1)} %bitcast.44), channel_id=1, source_target_pairs={{0,2},{2,4},{4,6},{6,0},{1,3},{3,5},{5,7},{7,1},{8,10},{10,12},{12... | collective-permute-start | bytes 1572872 | tf_op jit(solution)/shard_map/ppermute | solution.py:17
  19.3 17.0 %collective-permute-start.4 = (bf16[1,128,2048]{2,1,0:T(8,128)(2,1)}, bf16[1,128,2048]{2,1,0:T(8,128)(2,1)S(1)}, u32[]{:S(2)}, u32[]{:S(2)}) collective-permute-start(bf16[1,128,2048]{2,1,0:T(8,128)(2,1)} %bitcast.45), channel_id=1, source_target_pairs={{0,6},{2,0},{4,2},{6,4},{1,7},{3,1},{5,3},{7,5},{8,14},{10,8},{12,... | collective-permute-start | bytes 1572872 | tf_op jit(solution)/shard_map/ppermute | solution.py:17
  20.0 23.4 %collective-permute-start.5 = (bf16[1,128,2048]{2,1,0:T(8,128)(2,1)}, bf16[1,128,2048]{2,1,0:T(8,128)(2,1)S(1)}, u32[]{:S(2)}, u32[]{:S(2)}) collective-permute-start(bf16[1,128,2048]{2,1,0:T(8,128)(2,1)} %bitcast.46), channel_id=1, source_target_pairs={{0,4},{2,6},{4,0},{6,2},{1,5},{3,7},{5,1},{7,3},{8,12},{10,14},{12... | collective-permute-start | bytes 1572872 | tf_op jit(solution)/shard_map/ppermute | solution.py:17
  22.0 22.1 %copy-start.6 = (bf16[64,704]{1,0:T(8,128)(2,1)S(1)}, bf16[64,704]{1,0:T(8,128)(2,1)}, u32[]{:S(2)}) copy-start(bf16[64,704]{1,0:T(8,128)(2,1)} %param.11) | copy-start | bytes 270340
  35.5 18.9 %copy-start.8 = (f32[3,704]{1,0:T(4,128)S(1)}, f32[3,704]{1,0:T(4,128)}, u32[]{:S(2)}) copy-start(f32[3,704]{1,0:T(4,128)} %param.13) | copy-start | bytes 25348
  35.5 18.9 %copy-start = (bf16[1024,704]{0,1:T(8,128)(2,1)S(1)}, bf16[1024,704]{0,1:T(8,128)(2,1)}, u32[]{:S(2)}) copy-start(bf16[1024,704]{0,1:T(8,128)(2,1)} %param.9) | copy-start | bytes 4325380
  44.2 22.9 %collective-permute-start.6 = (bf16[4,128,2048]{2,1,0:T(8,128)(2,1)}, bf16[4,128,2048]{2,1,0:T(8,128)(2,1)}, u32[]{:S(2)}, u32[]{:S(2)}) collective-permute-start(bf16[4,128,2048]{2,1,0:T(8,128)(2,1)} %constant_dynamic-update-slice_fusion.own), channel_id=1, source_target_pairs={{0,1},{1,0},{2,3},{3,2},{4,5},{5,4},{6,7},{7,6},{8,9},{9,8},{10,11... | collective-permute-start | bytes 6291464 | tf_op jit(solution)/shard_map/ppermute | solution.py:22
  45.1 38.1 %all-to-all-start = ((bf16[8,64,704]{2,1,0:T(8,128)(2,1)}), bf16[8,64,704]{2,1,0:T(8,128)(2,1)}, u32[]{:S(2)}, u32[]{:S(2)}) async-start(bf16[8,64,704]{2,1,0:T(8,128)(2,1)} %broadcast_in_dim.27), calls=%async_computation | async-start | bytes 1572864 | tf_op jit(solution)/shard_map/all_to_all | solution.py:45
  53.7 160.4 %reduce-scatter.2.cloned.1.call-start = ((), (), s32[]{:S(2)}) async-start(), calls=%async_computation.4 | async-start | bytes 3244032 | tf_op jit(solution)/shard_map/reduce_scatter | solution.py:239
  83.2 21.0 %collective-permute-start.7 = (bf16[8,64,704]{2,1,0:T(8,128)(2,1)}, bf16[8,64,704]{2,1,0:T(8,128)(2,1)}, u32[]{:S(2)}, u32[]{:S(2)}) collective-permute-start(bf16[8,64,704]{2,1,0:T(8,128)(2,1)} %all-to-all-done.own), channel_id=1, source_target_pairs={{0,8},{8,16},{16,24},{24,0},{1,9},{9,17},{17,25},{25,1},{2,10},{10... | collective-permute-start | bytes 2162696 | tf_op jit(solution)/shard_map/ppermute | solution.py:17
  84.7 35.7 %collective-permute-start.8 = (bf16[8,64,704]{2,1,0:T(8,128)(2,1)}, bf16[8,64,704]{2,1,0:T(8,128)(2,1)}, u32[]{:S(2)}, u32[]{:S(2)}) collective-permute-start(bf16[8,64,704]{2,1,0:T(8,128)(2,1)} %all-to-all-done.own), channel_id=1, source_target_pairs={{0,24},{8,0},{16,8},{24,16},{1,25},{9,1},{17,9},{25,17},{2,26},{10... | collective-permute-start | bytes 2162696 | tf_op jit(solution)/shard_map/ppermute | solution.py:17
  86.4 35.5 %collective-permute-start.9 = (bf16[8,64,704]{2,1,0:T(8,128)(2,1)}, bf16[8,64,704]{2,1,0:T(8,128)(2,1)}, u32[]{:S(2)}, u32[]{:S(2)}) collective-permute-start(bf16[8,64,704]{2,1,0:T(8,128)(2,1)} %all-to-all-done.own), channel_id=1, source_target_pairs={{0,16},{8,24},{16,0},{24,8},{1,17},{9,25},{17,1},{25,9},{2,18},{10... | collective-permute-start | bytes 2162696 | tf_op jit(solution)/shard_map/ppermute | solution.py:17
  136.0 5.4 %collective-permute-start.10 = (bf16[4,1,2048,128]{3,2,1,0:T(8,128)(2,1)}, bf16[4,1,2048,128]{3,2,1,0:T(8,128)(2,1)}, u32[]{:S(2)}, u32[]{:S(2)}) collective-permute-start(bf16[4,1,2048,128]{3,2,1,0:T(8,128)(2,1)} %constant_dynamic-slice_fusion.7), channel_id=1, source_target_pairs={{0,1},{1,0},{2,3},{3,2},{4,5},{5,4},{6,7},{7,6},{8,9},{9,8},{10,11... | collective-permute-start | bytes 6291464 | tf_op jit(solution)/shard_map/ppermute | solution.py:22
  136.1 4.0 %collective-permute-start.20 = (f32[4,704]{1,0:T(4,128)S(1)}, f32[4,704]{1,0:T(4,128)S(1)}, u32[]{:S(2)}, u32[]{:S(2)}) collective-permute-start(f32[4,704]{1,0:T(4,128)S(1)} %pad_maximum_fusion), channel_id=1, source_target_pairs={{0,32},{32,0},{64,96},{96,64},{128,160},{160,128},{192,224},{224,1... | collective-permute-start | bytes 33800 | tf_op jit(solution)/shard_map/ppermute | solution.py:22
  136.6 21.4 %collective-permute-start.14 = (bf16[1,8,64,704]{3,2,1,0:T(8,128)(2,1)S(1)}, bf16[1,8,64,704]{3,2,1,0:T(8,128)(2,1)S(1)}, u32[]{:S(2)}, u32[]{:S(2)}) collective-permute-start(bf16[1,8,64,704]{3,2,1,0:T(8,128)(2,1)S(1)} %get-tuple-element.44), channel_id=1, source_target_pairs={{0,8},{8,16},{16,24},{24,0},{1,9},{9,17},{17,25},{25,1},{2,10},{10... | collective-permute-start | bytes 2162696 | tf_op jit(solution)/shard_map/ppermute | solution.py:17
  137.8 36.1 %collective-permute-start.15 = (bf16[1,8,64,704]{3,2,1,0:T(8,128)(2,1)S(1)}, bf16[1,8,64,704]{3,2,1,0:T(8,128)(2,1)S(1)}, u32[]{:S(2)}, u32[]{:S(2)}) collective-permute-start(bf16[1,8,64,704]{3,2,1,0:T(8,128)(2,1)S(1)} %get-tuple-element.43), channel_id=1, source_target_pairs={{0,24},{8,0},{16,8},{24,16},{1,25},{9,1},{17,9},{25,17},{2,26},{10... | collective-permute-start | bytes 2162696 | tf_op jit(solution)/shard_map/ppermute | solution.py:17
  139.9 35.0 %collective-permute-start.16 = (bf16[1,8,64,704]{3,2,1,0:T(8,128)(2,1)S(1)}, bf16[1,8,64,704]{3,2,1,0:T(8,128)(2,1)S(1)}, u32[]{:S(2)}, u32[]{:S(2)}) collective-permute-start(bf16[1,8,64,704]{3,2,1,0:T(8,128)(2,1)S(1)} %get-tuple-element.42), channel_id=1, source_target_pairs={{0,16},{8,24},{16,0},{24,8},{1,17},{9,25},{17,1},{25,9},{2,18},{10... | collective-permute-start | bytes 2162696 | tf_op jit(solution)/shard_map/ppermute | solution.py:17
  140.2 45.0 %collective-permute-start.21 = (f32[4,704]{1,0:T(4,128)S(1)}, f32[4,704]{1,0:T(4,128)S(1)}, u32[]{:S(2)}, u32[]{:S(2)}) collective-permute-start(f32[4,704]{1,0:T(4,128)S(1)} %fusion.17), channel_id=1, source_target_pairs={{0,64},{32,96},{64,0},{96,32},{128,192},{160,224},{192,128},{224,1... | collective-permute-start | bytes 33800 | tf_op jit(solution)/shard_map/ppermute | solution.py:22
  177.4 49.9 %all-to-all-start.1 = ((bf16[8,64,704]{2,1,0:T(8,128)(2,1)}), bf16[8,64,704]{2,1,0:T(8,128)(2,1)S(1)}, u32[]{:S(2)}, u32[]{:S(2)}) async-start(bf16[8,64,704]{2,1,0:T(8,128)(2,1)} %fusion.15), calls=%async_computation.1 | async-start | bytes 1572864 | tf_op jit(solution)/shard_map/all_to_all | solution.py:45
  180.9 38.3 %collective-permute-start.11 = (bf16[1,2048,128]{2,1,0:T(8,128)(2,1)}, bf16[1,2048,128]{2,1,0:T(8,128)(2,1)}, u32[]{:S(2)}, u32[]{:S(2)}) collective-permute-start(bf16[1,2048,128]{2,1,0:T(8,128)(2,1)} %get-tuple-element.46), channel_id=1, source_target_pairs={{0,2},{2,4},{4,6},{6,0},{1,3},{3,5},{5,7},{7,1},{8,10},{10,12},{12... | collective-permute-start | bytes 1572872 | tf_op jit(solution)/shard_map/ppermute | solution.py:17
  183.4 35.9 %collective-permute-start.12 = (bf16[1,2048,128]{2,1,0:T(8,128)(2,1)}, bf16[1,2048,128]{2,1,0:T(8,128)(2,1)}, u32[]{:S(2)}, u32[]{:S(2)}) collective-permute-start(bf16[1,2048,128]{2,1,0:T(8,128)(2,1)} %get-tuple-element.48), channel_id=1, source_target_pairs={{0,6},{2,0},{4,2},{6,4},{1,7},{3,1},{5,3},{7,5},{8,14},{10,8},{12,... | collective-permute-start | bytes 1572872 | tf_op jit(solution)/shard_map/ppermute | solution.py:17
  183.4 35.9 %collective-permute-start.13 = (bf16[1,2048,128]{2,1,0:T(8,128)(2,1)}, bf16[1,2048,128]{2,1,0:T(8,128)(2,1)}, u32[]{:S(2)}, u32[]{:S(2)}) collective-permute-start(bf16[1,2048,128]{2,1,0:T(8,128)(2,1)} %get-tuple-element.47), channel_id=1, source_target_pairs={{0,4},{2,6},{4,0},{6,2},{1,5},{3,7},{5,1},{7,3},{8,12},{10,14},{12... | collective-permute-start | bytes 1572872 | tf_op jit(solution)/shard_map/ppermute | solution.py:17
  185.2 19.4 %collective-permute-start.22 = (f32[4,704]{1,0:T(4,128)S(1)}, f32[4,704]{1,0:T(4,128)S(1)}, u32[]{:S(2)}, u32[]{:S(2)}) collective-permute-start(f32[4,704]{1,0:T(4,128)S(1)} %fusion.19), channel_id=1, source_target_pairs={{0,128},{32,160},{64,192},{96,224},{128,0},{160,32},{192,64},{224,... | collective-permute-start | bytes 33800 | tf_op jit(solution)/shard_map/ppermute | solution.py:22
  204.6 3.7 %collective-permute-start.23 = (f32[4,704]{1,0:T(4,128)S(1)}, f32[4,704]{1,0:T(4,128)S(1)}, u32[]{:S(2)}, u32[]{:S(2)}) collective-permute-start(f32[4,704]{1,0:T(4,128)S(1)} %add.151), channel_id=1, source_target_pairs={{0,8},{8,0},{16,24},{24,16},{1,9},{9,1},{17,25},{25,17},{2,10},{10... | collective-permute-start | bytes 33800 | tf_op jit(solution)/shard_map/ppermute | solution.py:22
  208.3 5.2 %collective-permute-start.24 = (f32[4,704]{1,0:T(4,128)S(1)}, f32[4,704]{1,0:T(4,128)S(1)}, u32[]{:S(2)}, u32[]{:S(2)}) collective-permute-start(f32[4,704]{1,0:T(4,128)S(1)} %add.152), channel_id=1, source_target_pairs={{0,16},{8,24},{16,0},{24,8},{1,17},{9,25},{17,1},{25,9},{2,18},{10... | collective-permute-start | bytes 33800 | tf_op jit(solution)/shard_map/ppermute | solution.py:22
  216.0 7.1 %collective-permute-start.17 = (bf16[1,64,704]{2,1,0:T(8,128)(2,1)}, bf16[1,64,704]{2,1,0:T(8,128)(2,1)}, u32[]{:S(2)}, u32[]{:S(2)}) collective-permute-start(bf16[1,64,704]{2,1,0:T(8,128)(2,1)} %get-tuple-element.49), channel_id=1, source_target_pairs={{0,8},{8,16},{16,24},{24,0},{1,9},{9,17},{17,25},{25,1},{2,10},{10... | collective-permute-start | bytes 270344 | tf_op jit(solution)/shard_map/ppermute | solution.py:17
  216.9 6.3 %collective-permute-start.18 = (bf16[1,64,704]{2,1,0:T(8,128)(2,1)}, bf16[1,64,704]{2,1,0:T(8,128)(2,1)}, u32[]{:S(2)}, u32[]{:S(2)}) collective-permute-start(bf16[1,64,704]{2,1,0:T(8,128)(2,1)} %get-tuple-element.51), channel_id=1, source_target_pairs={{0,24},{8,0},{16,8},{24,16},{1,25},{9,1},{17,9},{25,17},{2,26},{10... | collective-permute-start | bytes 270344 | tf_op jit(solution)/shard_map/ppermute | solution.py:17
  219.3 6.2 %collective-permute-start.19 = (bf16[1,64,704]{2,1,0:T(8,128)(2,1)S(1)}, bf16[1,64,704]{2,1,0:T(8,128)(2,1)}, u32[]{:S(2)}, u32[]{:S(2)}) collective-permute-start(bf16[1,64,704]{2,1,0:T(8,128)(2,1)S(1)} %get-tuple-element.50), channel_id=1, source_target_pairs={{0,16},{8,24},{16,0},{24,8},{1,17},{9,25},{17,1},{25,9},{2,18},{10... | collective-permute-start | bytes 270344 | tf_op jit(solution)/shard_map/ppermute | solution.py:17
  (7 other events, 44.3 us)
Sparse Core Ops, SparseCore 0:
  17.8 59.0 all-gather.1
  79.5 47.8 reduce-scatter.1

commit v9 on v8

--- a/solution.py
+++ b/solution.py
@@ -79,12 +79,12 @@
     return blocks.astype(jnp.float32).sum(axis=0)
 
 
-def terms_kernel(place, own, other, gate_t, value_t, gate_out, value_out, tokens):
-    groups, rows, _ = own.shape
-    for k, piece in enumerate((own, other)):
-        for group in range(groups):
-            start = pl.multiple_of(group * 2 * rows + place[k] * rows, rows)
-            tokens[pl.ds(start, rows), :] = piece[group]
+def terms_kernel(place, gate_t, value_t, *rest):
+    pieces, gate_out, value_out, tokens = rest[:-3], rest[-3], rest[-2], rest[-1]
+    for k, piece in enumerate(pieces):
+        rows = piece.shape[0]
+        start = pl.multiple_of(place[k] * rows, rows)
+        tokens[pl.ds(start, rows), :] = piece[...]
     block = tokens[...]
     value = jnp.dot(value_t[...], block, preferred_element_type=jnp.float32)
     value_out[...] = value.astype(value_out.dtype)
@@ -98,25 +98,26 @@
             gate_out[near, far] = gate[start : start + share]
 
 
-def grad_terms(place, own, other, gate_t, value_t, far, near, steps):
-    groups, rows, width = own.shape
+def grad_terms(place, pieces, gate_t, value_t, far, near, steps):
+    rows, width = pieces[0].shape
+    kind = pieces[0].dtype
     cols, length = gate_t.shape
     wide, share = width // steps, width // (far * near)
     whole = pl.BlockSpec((cols, length), lambda i: (0, 0))
-    piece = pl.BlockSpec((groups, rows, wide), lambda i: (0, 0, i))
+    piece = pl.BlockSpec((rows, wide), lambda i: (0, i))
     return pl.pallas_call(
         terms_kernel,
         grid=(steps,),
-        in_specs=[pl.BlockSpec(memory_space=pltpu.SMEM), piece, piece, whole, whole],
+        in_specs=[pl.BlockSpec(memory_space=pltpu.SMEM), whole, whole] + [piece] * len(pieces),
         out_specs=[
             pl.BlockSpec((near, far // steps, share, cols), lambda i: (0, i, 0, 0)),
             pl.BlockSpec((cols, wide), lambda i: (0, i)),
         ],
         out_shape=[
-            jax.ShapeDtypeStruct((near, far, share, cols), own.dtype),
-            jax.ShapeDtypeStruct((cols, width), own.dtype),
+            jax.ShapeDtypeStruct((near, far, share, cols), kind),
+            jax.ShapeDtypeStruct((cols, width), kind),
         ],
-        scratch_shapes=[pltpu.VMEM((length, wide), own.dtype)],
+        scratch_shapes=[pltpu.VMEM((length, wide), kind)],
         compiler_params=pltpu.CompilerParams(
             dimension_semantics=("arbitrary",), vmem_limit_bytes=58 * 2**20
         ),
@@ -125,7 +126,7 @@
             bytes_accessed=4 * (cols * length + width * cols) + 2 * width * length,
             transcendentals=0,
         ),
-    )(place, own, other, gate_t, value_t)
+    )(place, gate_t, value_t, *pieces)
 
 
 def back_kernel(place, gate_t, value_t, value_w, own, *rest):
@@ -184,14 +185,17 @@
     scale = float(length * nz * nx) ** (-0.5)
     narrow = jnp.bfloat16
 
-    token_blocks = gathered_four(tokens[None], "y", 0)
-    other_blocks = swapped(token_blocks, "c", 1)
+    steps = (1, nx - 1, 2)
+    pieces = [tokens] + [shifted(tokens, "y", k) for k in steps]
+    pieces = pieces + [swapped(piece, "c", 1) for piece in pieces]
     core = lax.axis_index("c")
-    token_places = jnp.stack([core, nc - 1 - core]).astype(jnp.int32)
+    chips = [(lax.axis_index("y") + ny - k) & (ny - 1) for k in (0, *steps)]
+    token_places = jnp.stack(
+        [chip * nc + core for chip in chips] + [chip * nc + nc - 1 - core for chip in chips]
+    ).astype(jnp.int32)
     gate_part = copies_of_all(up_gate_w, "z")
     value_part = gathered_four(up_value_w[None], "x", 0).reshape(nx * share, cols)
     full_value = lax.all_gather(value_part, "z", axis=0, tiled=True)
-    steps = (1, nx - 1, 2)
     gate_pieces = [gate_part] + [shifted(gate_part, "x", k) for k in steps]
     gate_places = jnp.stack(
         [(lax.axis_index("x") + nx - k) & (nx - 1) for k in (0, *steps)]
@@ -229,17 +233,15 @@
         conv_total = conv_total + swapped(conv_total, axis, bit)
     conv_total = conv_total * scale
 
+    gate_t, value_t = gate_grad.T, value_grad.T
     gate_terms, value_terms = grad_terms(
-        token_places, token_blocks, other_blocks, gate_grad.T, value_grad.T, nz, nx, 4
-    )
-    gate_grad, value_grad, _, _ = lax.optimization_barrier(
-        (gate_grad, value_grad, gate_terms, value_terms)
+        token_places, pieces, gate_t, value_t, nz, nx, 4
     )
     gate_blocks = sent_four(gate_terms, "x", 0)
     value_sums = lax.psum_scatter(value_terms.T, "z", scatter_dimension=0, tiled=True)
 
     part = back_parts(
-        gate_places, gate_grad.T, value_grad.T, full_value, gate_pieces, ny * nc, 4
+        gate_places, gate_t, value_t, full_value, gate_pieces, ny * nc, 4
     )
     part = part.reshape(ny, nc, width, rows)
     partner = swapped(take(part, "c", 1, 1), "c", 1)

time: 236 us -> 245 us (1.038)
  blocking collectives: 0 us -> 37.5 us
  waiting for transfers between devices: 112 us -> 95.9 us
  starting transfers between devices: 47.1 us -> 34.9 us
  other arithmetic: 24.4 us -> 21.4 us
    all_to_all x0 -> x1, blocking collectives: none -> 37.5 us  [exchanged(): return lax.all_to_all(blocks, axis, 0, 0, tiled=True)]
    ppermute x18, waiting for transfers between devices: 85.7 us -> 64.2 us  [shifted(): lax.ppermute(block, axis, [(i, (i + by) % size) for i in range(size)])]
    ppermute x7 -> x10, waiting for transfers between devices: 20.4 us -> 31.6 us  [swapped(): return lax.ppermute(block, axis, [(i, i ^ bit) for i in range(size)])]
    all_to_all x2 -> x1, starting transfers between devices: 12.1 us -> 4.06 us  [exchanged(): return lax.all_to_all(blocks, axis, 0, 0, tiled=True)]
    all_to_all x2 -> x1, waiting for transfers between devices: 5.41 us -> 0.01 us  [exchanged(): return lax.all_to_all(blocks, axis, 0, 0, tiled=True)]
    convert_element_type x2 -> x0, other arithmetic: 5.13 us -> none  [the longest x1 2.93 us: on_device(): gate_grad = (conv_weight[2] * conv_grad + conv_weight[1] * late[1:length...]
    unnamed x21 -> x33, local copies, waits for them, and re-layouts: 1.79 us -> 5.27 us
    ppermute x18, starting transfers between devices: 25.5 us -> 22.7 us  [shifted(): lax.ppermute(block, axis, [(i, (i + by) % size) for i in range(size)])]
  transfers between devices with their start and end apart: 29 -> 31, of which waited for: 17 -> 15; matrix products, arithmetic and copies ran while one was open for 17% -> 13% of each run, Pallas kernels for 9% -> 9%
where the time goes in v9:
time: 245 us; the launch traced here: 242 us
  waiting for transfers between devices  95.9 us (39%)
  blocking collectives  37.5 us (15%)
  starting transfers between devices  34.9 us (14%)
  Pallas kernels  22 us (9%)
  other arithmetic  21.4 us (9%)
  local copies, waits for them, and re-layouts  16.3 us (7%)
  between operations  14.3 us (6%)
    ppermute x18, waiting for transfers between devices, shifted(): lax.ppermute(block, axis, [(i, (i + by) % size) for i in range(size)])  64.2 us
    all_to_all x1, blocking collectives, exchanged(): return lax.all_to_all(blocks, axis, 0, 0, tiled=True)  37.5 us
    ppermute x10, waiting for transfers between devices, swapped(): return lax.ppermute(block, axis, [(i, i ^ bit) for i in range(size)])  31.6 us
    ppermute x18, starting transfers between devices, shifted(): lax.ppermute(block, axis, [(i, (i + by) % size) for i in range(size)])  22.7 us
    pallas_call x1, Pallas kernels, grad_terms(): pl.pallas_call(terms_kernel, grid=(steps,), in_specs=[pl.BlockSpec(memory...  11.1 us
    pallas_call x1, Pallas kernels, back_parts(): pl.pallas_call(back_kernel, grid=(steps,), in_specs=[pl.BlockSpec(memory_...  10.9 us
    ppermute x10, starting transfers between devices, swapped(): return lax.ppermute(block, axis, [(i, i ^ bit) for i in range(size)])  8.06 us
    dynamic_slice x4, local copies, waits for them, and re-layouts, take(): return lax.dynamic_slice(terms, at, lengths)  5.82 us
  transfers between devices with their start and end apart: 31, of which 15 were waited for; matrix products, arithmetic and copies ran while one was open for 13% of the time, Pallas kernels for 9%

profile of v9, /device:TPU:8, one launch (start us, length us, event | category | flops | bytes accessed | tf_op | source)
XLA Modules:
  0.0 242.3 jit_solution(8233794886064605080)
XLA Ops:
  8.8 1.7 collective-permute-start.1
  10.5 1.8 collective-permute-start.2
  17.7 1.7 collective-permute-start.10
  20.0 2.1 collective-permute-start.12
  23.6 1.7 convert_element_type.113
  25.4 5.6 %multiply_reduce_fusion.2 = (f32[704]{0:T(1024)S(1)}, f32[704]{0:T(1024)S(1)}, f32[704]{0:T(1024)S(1)}, f32[704]{0:T(1024)S(1)}, f32[1024,704]{0,1:T(8,128)S(1)}, /*index=5*/f32[1024,704]{0,1:T(8,128)S(1)}) fusion(f32[1024,704]{0,1:T(8,128)S(1)} %convert_element_type.113, bf16[1024,704]{0,1:T(8,128)(2,1)S(1)} %copy-done, bf16[1024,704]{0,1:T(8,128)(2,1)S(1)} %copy-done.5, ...), kind=kLoop, calls=%fused_computation.23 | loop fusion | flops 25949440 | bytes 12998656 | tf_op jit(solution)/shard_map/reduce_sum | solution.py:225
  31.0 2.0 collective-permute-done.10.rest_1_
  33.7 9.8 %collective-permute-done.12.rest_3_ = bf16[128,2048]{1,0:T(8,128)(2,1)} collective-permute-done((bf16[128,2048]{1,0:T(8,128)(2,1)}, bf16[128,2048]{1,0:T(8,128)(2,1)}, u32[]{:S(2)}, u32[]{:S(2)}) %collective-permute-start.12) | collective-permute-done | bytes 524320 | tf_op jit(solution)/shard_map/ppermute | solution.py:17
  43.5 3.0 %fusion.13.gate_t = bf16[704,1024]{1,0:T(8,128)(2,1)} fusion(f32[1024,704]{0,1:T(8,128)S(1)} %get-tuple-element.36, f32[704]{0:T(1024)S(1)} %get-tuple-element.35, f32[704]{0:T(1024)S(1)} %get-tuple-element.34, f32[704]{0:T(1024)S(1)} %get-tuple-element.33), kind=kLoop, calls=%fused_computation.28 | loop fusion | flops 4325376 | bytes 4333824 | tf_op jit(solution)/shard_map/transpose | solution.py:236
  46.5 2.3 fusion.12.value_t
  50.5 11.1 %shard_map.120 = (bf16[4,8,64,704]{3,2,1,0:T(8,128)(2,1)}, bf16[704,2048]{1,0:T(8,128)(2,1)}) custom-call(s32[8]{0:T(128)} %stack.70.place, bf16[704,1024]{1,0:T(8,128)(2,1)} %fusion.13.gate_t, bf16[704,1024]{1,0:T(8,128)(2,1)} %fusion.12.value_t, bf16[128,2048]{1,0:T(8,128)(2,1)} %rest_0_.1, bf16[128,2048]{1,0:T(8,128)(2,1)} %collective-permute-done.10.rest_1_, ...), custom_call_target="tpu_custom_call" | custom-call | flops 5905580032 | bytes 12845056 | tf_op jit(solution)/shard_map/pallas_call | solution.py:108
  62.6 37.5 %all_to_all.10.own = bf16[8,64,704]{2,1,0:T(8,128)(2,1)S(1)} all-to-all(bf16[8,64,704]{2,1,0:T(8,128)(2,1)S(1)} %broadcast_in_dim.8), channel_id=1, replica_groups=mesh['z'=8,'x'=4,'y'=4,'c'=2] {'z'}, dimensions={0} | all-to-all | bytes 1441792 | tf_op jit(solution)/shard_map/all_to_all | solution.py:45
  101.0 2.3 collective-permute-start.4
  104.3 17.1 %collective-permute-done.3.rest_0_ = bf16[8,64,704]{2,1,0:T(8,128)(2,1)S(1)} collective-permute-done((bf16[8,64,704]{2,1,0:T(8,128)(2,1)S(1)}, bf16[8,64,704]{2,1,0:T(8,128)(2,1)S(1)}, u32[]{:S(2)}, u32[]{:S(2)}) %collective-permute-start.3) | collective-permute-done | bytes 720928 | tf_op jit(solution)/shard_map/ppermute | solution.py:17
  121.4 15.4 %collective-permute-done.4.rest_1_ = bf16[8,64,704]{2,1,0:T(8,128)(2,1)S(1)} collective-permute-done((bf16[8,64,704]{2,1,0:T(8,128)(2,1)S(1)}, bf16[8,64,704]{2,1,0:T(8,128)(2,1)S(1)}, u32[]{:S(2)}, u32[]{:S(2)}) %collective-permute-start.4) | collective-permute-done | bytes 720928 | tf_op jit(solution)/shard_map/ppermute | solution.py:17
  138.7 10.9 %shard_map.119 = bf16[8,2048,128]{2,1,0:T(8,128)(2,1)} custom-call(s32[4]{0:T(128)} %pad_add_fusion.place, bf16[704,1024]{1,0:T(8,128)(2,1)} %fusion.13.gate_t, bf16[704,1024]{1,0:T(8,128)(2,1)} %fusion.12.value_t, bf16[2048,704]{1,0:T(8,128)(2,1)} %all-gather.2.cloned.1.call-done.value_w, bf16[8,64,704]{2,1,0:T(8,128)(2,1)} %copy-done.6, ...), custom_call_target="tpu_custom_call" | custom-call | flops 5905580032 | bytes 12845056 | tf_op jit(solution)/shard_map/pallas_call | solution.py:153
  149.5 3.2 %constant_dynamic-slice_fusion.7 = bf16[4,1,2048,128]{3,2,1,0:T(8,128)(2,1)} fusion(bf16[4,2,2048,128]{3,2,1,0:T(8,128)(2,1)} %bitcast.39, u32[]{:T(128)S(6)} %and.72), kind=kLoop, calls=%fused_computation.49 | loop fusion | bytes 4194308 | tf_op jit(solution)/shard_map/dynamic_slice | solution.py:41
  152.9 3.7 %collective-permute-done.23 = f32[4,704]{1,0:T(4,128)S(1)} collective-permute-done((f32[4,704]{1,0:T(4,128)S(1)}, f32[4,704]{1,0:T(4,128)S(1)}, u32[]{:S(2)}, u32[]{:S(2)}) %collective-permute-start.23) | collective-permute-done | bytes 11296 | tf_op jit(solution)/shard_map/ppermute | solution.py:22
  156.7 1.9 constant_dynamic-slice_fusion.3
  159.7 2.1 collective-permute-start.18
  162.9 3.3 %collective-permute-start.25 = (f32[4,704]{1,0:T(4,128)S(1)}, f32[4,704]{1,0:T(4,128)S(1)}, u32[]{:S(2)}, u32[]{:S(2)}) collective-permute-start(f32[4,704]{1,0:T(4,128)S(1)} %fusion.21), channel_id=1, source_target_pairs={{0,128},{32,160},{64,192},{96,224},{128,0},{160,32},{192,64},{224,... | collective-permute-start | bytes 33800 | tf_op jit(solution)/shard_map/ppermute | solution.py:22
  166.2 4.4 %collective-permute-done.25 = f32[4,704]{1,0:T(4,128)S(1)} collective-permute-done((f32[4,704]{1,0:T(4,128)S(1)}, f32[4,704]{1,0:T(4,128)S(1)}, u32[]{:S(2)}, u32[]{:S(2)}) %collective-permute-start.25) | collective-permute-done | bytes 11296 | tf_op jit(solution)/shard_map/ppermute | solution.py:22
  172.0 23.6 %collective-permute-done.26 = f32[4,704]{1,0:T(4,128)S(1)} collective-permute-done((f32[4,704]{1,0:T(4,128)S(1)}, f32[4,704]{1,0:T(4,128)S(1)}, u32[]{:S(2)}, u32[]{:S(2)}) %collective-permute-start.26) | collective-permute-done | bytes 11296 | tf_op jit(solution)/shard_map/ppermute | solution.py:22
  195.6 3.1 %collective-permute-start.27 = (f32[4,704]{1,0:T(4,128)S(1)}, f32[4,704]{1,0:T(4,128)S(1)}, u32[]{:S(2)}, u32[]{:S(2)}) collective-permute-start(f32[4,704]{1,0:T(4,128)S(1)} %add.197), channel_id=1, source_target_pairs={{0,16},{8,24},{16,0},{24,8},{1,17},{9,25},{17,1},{25,9},{2,18},{10... | collective-permute-start | bytes 33800 | tf_op jit(solution)/shard_map/ppermute | solution.py:22
  201.0 2.8 %add_convert_fusion = bf16[4,1,2048,128]{3,2,1,0:T(8,128)(2,1)S(1)} fusion(bf16[4,1,2048,128]{3,2,1,0:T(8,128)(2,1)} %collective-permute-done.6, bf16[4,2,2048,128]{3,2,1,0:T(8,128)(2,1)} %bitcast.40, u32[]{:T(128)S(6)} %and.71), kind=kLoop, calls=%fused_computation | loop fusion | flops 4194304 | bytes 6291460 | tf_op jit(solution)/shard_map/convert_element_type | solution.py:248
  203.8 2.7 %fusion.17 = bf16[8,64,704]{2,1,0:T(8,128)(2,1)} fusion(bf16[1,8,64,704]{3,2,1,0:T(8,128)(2,1)} %collective-permute-done.19, bf16[1,8,64,704]{3,2,1,0:T(8,128)(2,1)} %collective-permute-done.18, bf16[1,8,64,704]{3,2,1,0:T(8,128)(2,1)S(1)} %collective-permute-done.17, bf16[1,8,64,704]{3,2,1,0:T(8,128)(2,1)S(1)} %copy-done.3), kind=kLoop, calls=%fused_computation.33 | loop fusion | flops 2883584 | bytes 3604480 | tf_op jit(solution)/shard_map/squeeze | solution.py:255
  206.5 4.1 %all-to-all-start.1 = ((bf16[8,64,704]{2,1,0:T(8,128)(2,1)}), bf16[8,64,704]{2,1,0:T(8,128)(2,1)S(1)}, u32[]{:S(2)}, u32[]{:S(2)}) async-start(bf16[8,64,704]{2,1,0:T(8,128)(2,1)} %fusion.17), calls=%async_computation.1 | async-start | bytes 1572864 | tf_op jit(solution)/shard_map/all_to_all | solution.py:45
  213.3 2.2 collective-permute-start.21
  216.1 1.9 collective-permute-done.21
  218.0 3.3 %collective-permute-done.20 = bf16[1,64,704]{2,1,0:T(8,128)(2,1)S(1)} collective-permute-done((bf16[1,64,704]{2,1,0:T(8,128)(2,1)S(1)}, bf16[1,64,704]{2,1,0:T(8,128)(2,1)S(1)}, u32[]{:S(2)}, u32[]{:S(2)}) %collective-permute-start.20) | collective-permute-done | bytes 90144 | tf_op jit(solution)/shard_map/ppermute | solution.py:17
  223.0 4.0 %collective-permute-done.9 = bf16[1,2048,128]{2,1,0:T(8,128)(2,1)S(1)} collective-permute-done((bf16[1,2048,128]{2,1,0:T(8,128)(2,1)S(1)}, bf16[1,2048,128]{2,1,0:T(8,128)(2,1)S(1)}, u32[]{:S(2)}, u32[]{:S(2)}) %collective-permute-start.9) | collective-permute-done | bytes 524320 | tf_op jit(solution)/shard_map/ppermute | solution.py:17
  227.0 6.4 %collective-permute-done.8 = bf16[1,2048,128]{2,1,0:T(8,128)(2,1)S(1)} collective-permute-done((bf16[1,2048,128]{2,1,0:T(8,128)(2,1)S(1)}, bf16[1,2048,128]{2,1,0:T(8,128)(2,1)S(1)}, u32[]{:S(2)}, u32[]{:S(2)}) %collective-permute-start.8) | collective-permute-done | bytes 524320 | tf_op jit(solution)/shard_map/ppermute | solution.py:17
  (102 shorter events, 29.7 us)
Async XLA Ops:
  7.2 130.6 %all-gather.2.cloned.1.call-start = ((), (), s32[]{:S(2)}) async-start(), calls=%async_computation.3 | async-start | bytes 3538944 | tf_op jit(solution)/shard_map/all_gather | solution.py:198
  7.2 6.2 %collective-permute-start = (bf16[1,64,704]{2,1,0:T(8,128)(2,1)}, bf16[1,64,704]{2,1,0:T(8,128)(2,1)}, u32[]{:S(2)}, u32[]{:S(2)}) collective-permute-start(bf16[1,64,704]{2,1,0:T(8,128)(2,1)} %bitcast.45), channel_id=1, source_target_pairs={{0,8},{8,16},{16,24},{24,0},{1,9},{9,17},{17,25},{25,1},{2,10},{10... | collective-permute-start | bytes 270344 | tf_op jit(solution)/shard_map/ppermute | solution.py:17
  8.8 6.5 %collective-permute-start.1 = (bf16[1,64,704]{2,1,0:T(8,128)(2,1)}, bf16[1,64,704]{2,1,0:T(8,128)(2,1)S(1)}, u32[]{:S(2)}, u32[]{:S(2)}) collective-permute-start(bf16[1,64,704]{2,1,0:T(8,128)(2,1)} %bitcast.46), channel_id=1, source_target_pairs={{0,24},{8,0},{16,8},{24,16},{1,25},{9,1},{17,9},{25,17},{2,26},{10... | collective-permute-start | bytes 270344 | tf_op jit(solution)/shard_map/ppermute | solution.py:17
  10.5 6.3 %collective-permute-start.2 = (bf16[1,64,704]{2,1,0:T(8,128)(2,1)}, bf16[1,64,704]{2,1,0:T(8,128)(2,1)S(1)}, u32[]{:S(2)}, u32[]{:S(2)}) collective-permute-start(bf16[1,64,704]{2,1,0:T(8,128)(2,1)} %bitcast.47), channel_id=1, source_target_pairs={{0,16},{8,24},{16,0},{24,8},{1,17},{9,25},{17,1},{25,9},{2,18},{10... | collective-permute-start | bytes 270344 | tf_op jit(solution)/shard_map/ppermute | solution.py:17
  17.6 181.1 %reduce-scatter.2.cloned.1.call-start = ((), (), s32[]{:S(2)}) async-start(), calls=%async_computation.4 | async-start | bytes 3244032 | tf_op jit(solution)/shard_map/reduce_scatter | solution.py:241
  17.7 15.3 %collective-permute-start.10 = (bf16[128,2048]{1,0:T(8,128)(2,1)}, bf16[128,2048]{1,0:T(8,128)(2,1)}, u32[]{:S(2)}, u32[]{:S(2)}) collective-permute-start(bf16[128,2048]{1,0:T(8,128)(2,1)} %rest_0_.1), channel_id=1, source_target_pairs={{0,2},{2,4},{4,6},{6,0},{1,3},{3,5},{5,7},{7,1},{8,10},{10,12},{12... | collective-permute-start | bytes 1572872 | tf_op jit(solution)/shard_map/ppermute | solution.py:17
  19.3 14.4 %collective-permute-start.11 = (bf16[128,2048]{1,0:T(8,128)(2,1)}, bf16[128,2048]{1,0:T(8,128)(2,1)}, u32[]{:S(2)}, u32[]{:S(2)}) collective-permute-start(bf16[128,2048]{1,0:T(8,128)(2,1)} %rest_0_.1), channel_id=1, source_target_pairs={{0,6},{2,0},{4,2},{6,4},{1,7},{3,1},{5,3},{7,5},{8,14},{10,8},{12,... | collective-permute-start | bytes 1572872 | tf_op jit(solution)/shard_map/ppermute | solution.py:17
  20.0 23.5 %collective-permute-start.12 = (bf16[128,2048]{1,0:T(8,128)(2,1)}, bf16[128,2048]{1,0:T(8,128)(2,1)}, u32[]{:S(2)}, u32[]{:S(2)}) collective-permute-start(bf16[128,2048]{1,0:T(8,128)(2,1)} %rest_0_.1), channel_id=1, source_target_pairs={{0,4},{2,6},{4,0},{6,2},{1,5},{3,7},{5,1},{7,3},{8,12},{10,14},{12... | collective-permute-start | bytes 1572872 | tf_op jit(solution)/shard_map/ppermute | solution.py:17
  22.1 26.7 %collective-permute-start.13 = (bf16[128,2048]{1,0:T(8,128)(2,1)}, bf16[128,2048]{1,0:T(8,128)(2,1)}, u32[]{:S(2)}, u32[]{:S(2)}) collective-permute-start(bf16[128,2048]{1,0:T(8,128)(2,1)} %rest_0_.1), channel_id=1, source_target_pairs={{0,1},{1,0},{2,3},{3,2},{4,5},{5,4},{6,7},{7,6},{8,9},{9,8},{10,11... | collective-permute-start | bytes 1572872 | tf_op jit(solution)/shard_map/ppermute | solution.py:22
  33.0 15.7 %collective-permute-start.14 = (bf16[128,2048]{1,0:T(8,128)(2,1)}, bf16[128,2048]{1,0:T(8,128)(2,1)S(1)}, u32[]{:S(2)}, u32[]{:S(2)}) collective-permute-start(bf16[128,2048]{1,0:T(8,128)(2,1)} %collective-permute-done.10.rest_1_), channel_id=1, source_target_pairs={{0,1},{1,0},{2,3},{3,2},{4,5},{5,4},{6,7},{7,6},{8,9},{9,8},{10,11... | collective-permute-start | bytes 1572872 | tf_op jit(solution)/shard_map/ppermute | solution.py:22
  33.7 15.0 %collective-permute-start.15 = (bf16[128,2048]{1,0:T(8,128)(2,1)}, bf16[128,2048]{1,0:T(8,128)(2,1)S(1)}, u32[]{:S(2)}, u32[]{:S(2)}) collective-permute-start(bf16[128,2048]{1,0:T(8,128)(2,1)} %collective-permute-done.11.rest_2_), channel_id=1, source_target_pairs={{0,1},{1,0},{2,3},{3,2},{4,5},{5,4},{6,7},{7,6},{8,9},{9,8},{10,11... | collective-permute-start | bytes 1572872 | tf_op jit(solution)/shard_map/ppermute | solution.py:22
  43.5 5.3 %collective-permute-start.16 = (bf16[128,2048]{1,0:T(8,128)(2,1)}, bf16[128,2048]{1,0:T(8,128)(2,1)S(1)}, u32[]{:S(2)}, u32[]{:S(2)}) collective-permute-start(bf16[128,2048]{1,0:T(8,128)(2,1)} %collective-permute-done.12.rest_3_), channel_id=1, source_target_pairs={{0,1},{1,0},{2,3},{3,2},{4,5},{5,4},{6,7},{7,6},{8,9},{9,8},{10,11... | collective-permute-start | bytes 1572872 | tf_op jit(solution)/shard_map/ppermute | solution.py:22
  100.1 37.7 %copy-start.6 = (bf16[8,64,704]{2,1,0:T(8,128)(2,1)}, bf16[8,64,704]{2,1,0:T(8,128)(2,1)S(1)}, u32[]{:S(2)}) copy-start(bf16[8,64,704]{2,1,0:T(8,128)(2,1)S(1)} %all_to_all.10.own) | copy-start | bytes 2162692
  100.1 21.3 %collective-permute-start.3 = (bf16[8,64,704]{2,1,0:T(8,128)(2,1)S(1)}, bf16[8,64,704]{2,1,0:T(8,128)(2,1)S(1)}, u32[]{:S(2)}, u32[]{:S(2)}) collective-permute-start(bf16[8,64,704]{2,1,0:T(8,128)(2,1)S(1)} %all_to_all.10.own), channel_id=1, source_target_pairs={{0,8},{8,16},{16,24},{24,0},{1,9},{9,17},{17,25},{25,1},{2,10},{10... | collective-permute-start | bytes 2162696 | tf_op jit(solution)/shard_map/ppermute | solution.py:17
  101.0 35.7 %collective-permute-start.4 = (bf16[8,64,704]{2,1,0:T(8,128)(2,1)S(1)}, bf16[8,64,704]{2,1,0:T(8,128)(2,1)S(1)}, u32[]{:S(2)}, u32[]{:S(2)}) collective-permute-start(bf16[8,64,704]{2,1,0:T(8,128)(2,1)S(1)} %all_to_all.10.own), channel_id=1, source_target_pairs={{0,24},{8,0},{16,8},{24,16},{1,25},{9,1},{17,9},{25,17},{2,26},{10... | collective-permute-start | bytes 2162696 | tf_op jit(solution)/shard_map/ppermute | solution.py:17
  103.3 34.5 %collective-permute-start.5 = (bf16[8,64,704]{2,1,0:T(8,128)(2,1)S(1)}, bf16[8,64,704]{2,1,0:T(8,128)(2,1)S(1)}, u32[]{:S(2)}, u32[]{:S(2)}) collective-permute-start(bf16[8,64,704]{2,1,0:T(8,128)(2,1)S(1)} %all_to_all.10.own), channel_id=1, source_target_pairs={{0,16},{8,24},{16,0},{24,8},{1,17},{9,25},{17,1},{25,9},{2,18},{10... | collective-permute-start | bytes 2162696 | tf_op jit(solution)/shard_map/ppermute | solution.py:17
  152.7 47.8 %collective-permute-start.6 = (bf16[4,1,2048,128]{3,2,1,0:T(8,128)(2,1)}, bf16[4,1,2048,128]{3,2,1,0:T(8,128)(2,1)}, u32[]{:S(2)}, u32[]{:S(2)}) collective-permute-start(bf16[4,1,2048,128]{3,2,1,0:T(8,128)(2,1)} %constant_dynamic-slice_fusion.7), channel_id=1, source_target_pairs={{0,1},{1,0},{2,3},{3,2},{4,5},{5,4},{6,7},{7,6},{8,9},{9,8},{10,11... | collective-permute-start | bytes 6291464 | tf_op jit(solution)/shard_map/ppermute | solution.py:22
  152.8 3.8 %collective-permute-start.23 = (f32[4,704]{1,0:T(4,128)S(1)}, f32[4,704]{1,0:T(4,128)S(1)}, u32[]{:S(2)}, u32[]{:S(2)}) collective-permute-start(f32[4,704]{1,0:T(4,128)S(1)} %pad_maximum_fusion), channel_id=1, source_target_pairs={{0,32},{32,0},{64,96},{96,64},{128,160},{160,128},{192,224},{224,1... | collective-permute-start | bytes 33800 | tf_op jit(solution)/shard_map/ppermute | solution.py:22
  156.6 6.3 %collective-permute-start.24 = (f32[4,704]{1,0:T(4,128)S(1)}, f32[4,704]{1,0:T(4,128)S(1)}, u32[]{:S(2)}, u32[]{:S(2)}) collective-permute-start(f32[4,704]{1,0:T(4,128)S(1)} %fusion.19), channel_id=1, source_target_pairs={{0,64},{32,96},{64,0},{96,32},{128,192},{160,224},{192,128},{224,1... | collective-permute-start | bytes 33800 | tf_op jit(solution)/shard_map/ppermute | solution.py:22
  158.6 45.2 %collective-permute-start.17 = (bf16[1,8,64,704]{3,2,1,0:T(8,128)(2,1)}, bf16[1,8,64,704]{3,2,1,0:T(8,128)(2,1)S(1)}, u32[]{:S(2)}, u32[]{:S(2)}) collective-permute-start(bf16[1,8,64,704]{3,2,1,0:T(8,128)(2,1)} %get-tuple-element.40), channel_id=1, source_target_pairs={{0,8},{8,16},{16,24},{24,0},{1,9},{9,17},{17,25},{25,1},{2,10},{10... | collective-permute-start | bytes 2162696 | tf_op jit(solution)/shard_map/ppermute | solution.py:17
  159.7 44.0 %collective-permute-start.18 = (bf16[1,8,64,704]{3,2,1,0:T(8,128)(2,1)}, bf16[1,8,64,704]{3,2,1,0:T(8,128)(2,1)}, u32[]{:S(2)}, u32[]{:S(2)}) collective-permute-start(bf16[1,8,64,704]{3,2,1,0:T(8,128)(2,1)} %get-tuple-element.39), channel_id=1, source_target_pairs={{0,24},{8,0},{16,8},{24,16},{1,25},{9,1},{17,9},{25,17},{2,26},{10... | collective-permute-start | bytes 2162696 | tf_op jit(solution)/shard_map/ppermute | solution.py:17
  161.8 42.0 %collective-permute-start.19 = (bf16[1,8,64,704]{3,2,1,0:T(8,128)(2,1)}, bf16[1,8,64,704]{3,2,1,0:T(8,128)(2,1)}, u32[]{:S(2)}, u32[]{:S(2)}) collective-permute-start(bf16[1,8,64,704]{3,2,1,0:T(8,128)(2,1)} %get-tuple-element.38), channel_id=1, source_target_pairs={{0,16},{8,24},{16,0},{24,8},{1,17},{9,25},{17,1},{25,9},{2,18},{10... | collective-permute-start | bytes 2162696 | tf_op jit(solution)/shard_map/ppermute | solution.py:17
  162.9 7.7 %collective-permute-start.25 = (f32[4,704]{1,0:T(4,128)S(1)}, f32[4,704]{1,0:T(4,128)S(1)}, u32[]{:S(2)}, u32[]{:S(2)}) collective-permute-start(f32[4,704]{1,0:T(4,128)S(1)} %fusion.21), channel_id=1, source_target_pairs={{0,128},{32,160},{64,192},{96,224},{128,0},{160,32},{192,64},{224,... | collective-permute-start | bytes 33800 | tf_op jit(solution)/shard_map/ppermute | solution.py:22
  170.6 25.0 %collective-permute-start.26 = (f32[4,704]{1,0:T(4,128)S(1)}, f32[4,704]{1,0:T(4,128)S(1)}, u32[]{:S(2)}, u32[]{:S(2)}) collective-permute-start(f32[4,704]{1,0:T(4,128)S(1)} %add.196), channel_id=1, source_target_pairs={{0,8},{8,0},{16,24},{24,16},{1,9},{9,1},{17,25},{25,17},{2,10},{10... | collective-permute-start | bytes 33800 | tf_op jit(solution)/shard_map/ppermute | solution.py:22
  195.6 17.7 %collective-permute-start.27 = (f32[4,704]{1,0:T(4,128)S(1)}, f32[4,704]{1,0:T(4,128)S(1)}, u32[]{:S(2)}, u32[]{:S(2)}) collective-permute-start(f32[4,704]{1,0:T(4,128)S(1)} %add.197), channel_id=1, source_target_pairs={{0,16},{8,24},{16,0},{24,8},{1,17},{9,25},{17,1},{25,9},{2,18},{10... | collective-permute-start | bytes 33800 | tf_op jit(solution)/shard_map/ppermute | solution.py:22
  200.6 14.9 %collective-permute-start.22 = (bf16[1,64,704]{2,1,0:T(8,128)(2,1)}, bf16[1,64,704]{2,1,0:T(8,128)(2,1)}, u32[]{:S(2)}, u32[]{:S(2)}) collective-permute-start(bf16[1,64,704]{2,1,0:T(8,128)(2,1)} %get-tuple-element.46), channel_id=1, source_target_pairs={{0,16},{8,24},{16,0},{24,8},{1,17},{9,25},{17,1},{25,9},{2,18},{10... | collective-permute-start | bytes 270344 | tf_op jit(solution)/shard_map/ppermute | solution.py:17
  206.5 28.2 %all-to-all-start.1 = ((bf16[8,64,704]{2,1,0:T(8,128)(2,1)}), bf16[8,64,704]{2,1,0:T(8,128)(2,1)S(1)}, u32[]{:S(2)}, u32[]{:S(2)}) async-start(bf16[8,64,704]{2,1,0:T(8,128)(2,1)} %fusion.17), calls=%async_computation.1 | async-start | bytes 1572864 | tf_op jit(solution)/shard_map/all_to_all | solution.py:45
  210.6 16.4 %collective-permute-start.9 = (bf16[1,2048,128]{2,1,0:T(8,128)(2,1)S(1)}, bf16[1,2048,128]{2,1,0:T(8,128)(2,1)S(1)}, u32[]{:S(2)}, u32[]{:S(2)}) collective-permute-start(bf16[1,2048,128]{2,1,0:T(8,128)(2,1)S(1)} %get-tuple-element.43), channel_id=1, source_target_pairs={{0,4},{2,6},{4,0},{6,2},{1,5},{3,7},{5,1},{7,3},{8,12},{10,14},{12... | collective-permute-start | bytes 1572872 | tf_op jit(solution)/shard_map/ppermute | solution.py:17
  211.3 22.1 %collective-permute-start.8 = (bf16[1,2048,128]{2,1,0:T(8,128)(2,1)S(1)}, bf16[1,2048,128]{2,1,0:T(8,128)(2,1)S(1)}, u32[]{:S(2)}, u32[]{:S(2)}) collective-permute-start(bf16[1,2048,128]{2,1,0:T(8,128)(2,1)S(1)} %get-tuple-element.44), channel_id=1, source_target_pairs={{0,6},{2,0},{4,2},{6,4},{1,7},{3,1},{5,3},{7,5},{8,14},{10,8},{12,... | collective-permute-start | bytes 1572872 | tf_op jit(solution)/shard_map/ppermute | solution.py:17
  211.7 21.6 %collective-permute-start.7 = (bf16[1,2048,128]{2,1,0:T(8,128)(2,1)S(1)}, bf16[1,2048,128]{2,1,0:T(8,128)(2,1)S(1)}, u32[]{:S(2)}, u32[]{:S(2)}) collective-permute-start(bf16[1,2048,128]{2,1,0:T(8,128)(2,1)S(1)} %get-tuple-element.42), channel_id=1, source_target_pairs={{0,2},{2,4},{4,6},{6,0},{1,3},{3,5},{5,7},{7,1},{8,10},{10,12},{12... | collective-permute-start | bytes 1572872 | tf_op jit(solution)/shard_map/ppermute | solution.py:17
  213.3 4.7 %collective-permute-start.21 = (bf16[1,64,704]{2,1,0:T(8,128)(2,1)S(1)}, bf16[1,64,704]{2,1,0:T(8,128)(2,1)S(1)}, u32[]{:S(2)}, u32[]{:S(2)}) collective-permute-start(bf16[1,64,704]{2,1,0:T(8,128)(2,1)S(1)} %get-tuple-element.47), channel_id=1, source_target_pairs={{0,24},{8,0},{16,8},{24,16},{1,25},{9,1},{17,9},{25,17},{2,26},{10... | collective-permute-start | bytes 270344 | tf_op jit(solution)/shard_map/ppermute | solution.py:17
  215.5 5.8 %collective-permute-start.20 = (bf16[1,64,704]{2,1,0:T(8,128)(2,1)S(1)}, bf16[1,64,704]{2,1,0:T(8,128)(2,1)S(1)}, u32[]{:S(2)}, u32[]{:S(2)}) collective-permute-start(bf16[1,64,704]{2,1,0:T(8,128)(2,1)S(1)} %get-tuple-element.45), channel_id=1, source_target_pairs={{0,8},{8,16},{16,24},{24,0},{1,9},{9,17},{17,25},{25,1},{2,10},{10... | collective-permute-start | bytes 270344 | tf_op jit(solution)/shard_map/ppermute | solution.py:17
  (15 other events, 97.0 us)
Sparse Core Ops, SparseCore 0:
  17.8 46.6 all-gather.1
  67.0 54.2 reduce-scatter.1
